TPU v7x, 256 devices: a whole 4x4x8 slice. The times are simulated.
256 devices in a mesh: ep: 16 (over y, x), tp: 16 (over z, core).
Axes of the slice: x: 4, y: 4, z: 8, core: 2. Of those that a mesh axis runs over, the one named last changes fastest.
Arguments:
- tokens: bfloat16 [512, 4096], P('ep'), may hold values from -6 to 6
- state_matrix: float32 [512, 16, 128, 128], P('ep', 'tp'), may hold values from -1.5 to 1.5
- state_norm: float32 [512, 16, 128], P('ep', 'tp'), may hold values from -4 to 4
- state_max: float32 [512, 16], P('ep', 'tp'), may hold values from -5 to 5
- mixer_gain: float32 [4096], replicated, may hold values from 0.1 to 1.9
- w_query: bfloat16 [4096, 2048], P('ep', 'tp'), may hold values from -0.09375 to 0.09375
- w_key: bfloat16 [4096, 2048], P('ep', 'tp'), may hold values from -0.09375 to 0.09375
- w_value: bfloat16 [4096, 2048], P('ep', 'tp'), may hold values from -0.09375 to 0.09375
- w_outgate: bfloat16 [4096, 2048], P('ep', 'tp'), may hold values from -0.09375 to 0.09375
- w_ingate: bfloat16 [4096, 16], replicated, may hold values from -0.09375 to 0.09375
- w_forget: bfloat16 [4096, 16], replicated, may hold values from -0.09375 to 0.09375
- forget_bias: float32 [16], replicated, may hold values from -2 to 4
- w_proj: bfloat16 [2048, 4096], P('tp', 'ep'), may hold values from -0.125 to 0.125
- ffn_gain: float32 [4096], replicated, may hold values from 0.1 to 1.9
- w_branch: bfloat16 [4096], replicated, may hold values from -0.09375 to 0.09375
- routes: int32 [512, 2], P('ep'), may hold values from 0 to 15, all different within a row; in each aligned block of 32 rows (0 to 31, 32 to 63, ...) at most 6 rows name the same one
- route_weight: float32 [512, 2], P('ep'), may hold values from 0.2 to 1
- expert_gate: bfloat16 [16, 4096, 4096], P('ep', None, 'tp'), may hold values from -0.09375 to 0.09375
- expert_up: bfloat16 [16, 4096, 4096], P('ep', None, 'tp'), may hold values from -0.09375 to 0.09375
- expert_down: bfloat16 [16, 4096, 4096], P('ep', 'tp'), may hold values from -0.09375 to 0.09375
- dense_gate: bfloat16 [4096, 8192], P('ep', 'tp'), may hold values from -0.09375 to 0.09375
- dense_up: bfloat16 [4096, 8192], P('ep', 'tp'), may hold values from -0.09375 to 0.09375
- dense_down: bfloat16 [8192, 4096], P('tp', 'ep'), may hold values from -0.0625 to 0.0625
Outputs:
- layer_out: bfloat16 [512, 4096], P('ep')
- new_matrix: float32 [512, 16, 128, 128], P('ep', 'tp')
- new_norm: float32 [512, 16, 128], P('ep', 'tp')
- new_max: float32 [512, 16], P('ep', 'tp')
Inputs may be any that keep to these rules, and one draw needn't show every extreme that they name: `routes`: each row names 2 different experts. Among the rows of one index of ep (32 sequences) no expert is named more than 6 times, and in some such group one expert is named exactly 6 times.
All inputs are finite; a program needn't handle non-finite values.
Results may differ from a plain program's by a relative error of at most 0.012.
Values may be sent and summed in bfloat16 or wider, within the bound.
No kernel may reach another device: no remote copies, remote signals or barrier semaphores. Data moves between devices by JAX's collectives and lax.ppermute only.
A program may use at most 64 MiB of HBM per device.

v0:
```python
import jax
import jax.numpy as jnp
from jax import lax
from jax.sharding import PartitionSpec as P

EPS = 1e-06


def side_by_side(arrays, axis, dim, along):
    ends, at = ([], 0)
    for a in arrays[:-1]:
        at += a.shape[along]
        ends.append(at)
    both = jnp.concatenate(arrays, axis=along)
    return tuple(jnp.split(lax.all_gather(both, axis, axis=dim, tiled=True), ends, axis=along))


def from_everyone(shard, axis):
    devices = lax.axis_size(axis)
    return lax.all_to_all(
        jnp.broadcast_to(shard[None], (devices, *shard.shape)), axis, 0, 0, tiled=True
    )


def laid_out(parts, dim):
    parts = jnp.moveaxis(parts, 0, dim)
    shape = parts.shape
    return parts.reshape(*shape[:dim], shape[dim] * shape[dim + 1], *shape[dim + 2 :])


def collect(shard, axis, dim):
    parts = from_everyone(shard, axis)
    return laid_out(parts, dim)


def total_of_pieces(shard, axis):
    return lax.all_gather(shard, axis).sum(0)


def in_blocks(shard, dim, devices):
    shape = shard.shape
    parts = shard.reshape(*shape[:dim], devices, shape[dim] // devices, *shape[dim + 1 :])
    return jnp.moveaxis(parts, dim, 0)


def sum_at_owner(shard, axis, dim):
    parts = in_blocks(shard, dim, lax.axis_size(axis))
    arrived = lax.all_to_all(parts, axis, split_axis=0, concat_axis=0, tiled=True)
    return arrived.astype(jnp.float32).sum(axis=0)


def in_one_piece(arrays, axis, dim, along):
    both = jnp.concatenate(arrays, axis=along)
    out, at, finished = (sum_at_owner(both, axis, dim), 0, [])
    for a in arrays:
        finished.append(lax.slice_in_dim(out, at, at + a.shape[along], axis=along))
        at += a.shape[along]
    return tuple(finished)


def rms_scale(values, gain):
    wide = values.astype(jnp.float32)
    return wide * lax.rsqrt(jnp.mean(wide * wide, axis=-1, keepdims=True) + EPS) * gain


def slot_numbers(flat_routes, experts_all):
    onehot = (flat_routes[:, None] == jnp.arange(experts_all, dtype=jnp.int32)[None, :]).astype(
        jnp.int32
    )
    before = jnp.cumsum(onehot, axis=0) - onehot
    return jnp.sum(before * onehot, axis=1)


def memory_step(
    query_all,
    key_all,
    value_all,
    outgate,
    gate_in,
    gate_forget,
    state_matrix,
    state_norm,
    state_max,
):
    row_count, head_count = gate_in.shape
    head_size = state_matrix.shape[-1]
    heads_q = query_all.reshape(row_count, head_count, head_size)
    heads_k = key_all.reshape(row_count, head_count, head_size) * head_size ** (-0.5)
    heads_v = value_all.reshape(row_count, head_count, head_size)
    log_keep = jax.nn.log_sigmoid(gate_forget)
    new_max = jnp.maximum(log_keep + state_max, gate_in)
    keep_factor = jnp.exp(log_keep + state_max - new_max)
    write_factor = jnp.exp(gate_in - new_max)
    new_matrix = (
        keep_factor[:, :, None, None] * state_matrix
        + write_factor[:, :, None, None] * heads_k[:, :, :, None] * heads_v[:, :, None, :]
    )
    new_norm = keep_factor[:, :, None] * state_norm + write_factor[:, :, None] * heads_k
    numer = jnp.einsum("bhk,bhkv->bhv", heads_q, new_matrix, precision=lax.Precision.HIGHEST)
    denom = jnp.sum(heads_q * new_norm, axis=-1)
    cell = numer / jnp.maximum(jnp.abs(denom), 1.0)[:, :, None]
    gated = jax.nn.sigmoid(outgate.reshape(row_count, head_count, head_size)) * cell
    mixed_heads = gated.reshape(row_count, head_count * head_size).astype(jnp.bfloat16)
    return (mixed_heads, new_matrix, new_norm, new_max)


def on_device(
    tokens,
    state_matrix,
    state_norm,
    state_max,
    mixer_gain,
    w_query,
    w_key,
    w_value,
    w_outgate,
    w_ingate,
    w_forget,
    forget_bias,
    w_proj,
    ffn_gain,
    w_branch,
    routes,
    route_weight,
    expert_gate,
    expert_up,
    expert_down,
    dense_gate,
    dense_up,
    dense_down,
):
    row_count = tokens.shape[0]
    head_count = state_matrix.shape[1]
    model_width = tokens.shape[1]
    normed = rms_scale(tokens, mixer_gain).astype(jnp.bfloat16)
    head_start = lax.axis_index("tp") * head_count
    gate_in = lax.dynamic_slice_in_dim(
        jnp.dot(normed, w_ingate, preferred_element_type=jnp.float32), head_start, head_count, 1
    )
    forget_all = jnp.dot(normed, w_forget, preferred_element_type=jnp.float32) + forget_bias
    gate_forget = lax.dynamic_slice_in_dim(forget_all, head_start, head_count, 1)
    pieces = side_by_side((w_query, w_key, w_value, w_outgate), "ep", 0, 1)
    projected = tuple(
        (jnp.dot(normed, shard_w, preferred_element_type=jnp.float32) for shard_w in pieces)
    )
    mixed_heads, new_matrix, new_norm, new_max = memory_step(
        projected[0],
        projected[1],
        projected[2],
        projected[3],
        gate_in,
        gate_forget,
        state_matrix,
        state_norm,
        state_max,
    )
    spread_out = jnp.dot(collect(mixed_heads, "ep", 0), w_proj, preferred_element_type=jnp.float32)
    mix_back = lax.all_to_all(spread_out, "ep", split_axis=0, concat_axis=1, tiled=True)
    mixer_out = total_of_pieces(mix_back, "tp")
    residual = (tokens.astype(jnp.float32) + mixer_out).astype(jnp.bfloat16)
    ffn_in = rms_scale(residual, ffn_gain).astype(jnp.bfloat16)
    branch_share = jax.nn.sigmoid(jnp.dot(ffn_in, w_branch, preferred_element_type=jnp.float32))
    dense_spread = lax.all_to_all(ffn_in, "ep", split_axis=1, concat_axis=0, tiled=True)
    dense_g, dense_u = in_one_piece(
        (
            jnp.dot(dense_spread, dense_gate, preferred_element_type=jnp.float32).astype(
                jnp.bfloat16
            ),
            jnp.dot(dense_spread, dense_up, preferred_element_type=jnp.float32).astype(
                jnp.bfloat16
            ),
        ),
        "ep",
        0,
        1,
    )
    dense_hidden = (jax.nn.silu(dense_g) * dense_u).astype(jnp.bfloat16)
    dense_spread_out = jnp.dot(
        collect(dense_hidden, "ep", 0), dense_down, preferred_element_type=jnp.float32
    )
    dense_back = lax.all_to_all(dense_spread_out, "ep", split_axis=0, concat_axis=1, tiled=True)
    ep_count = lax.axis_size("ep")
    local_experts = expert_gate.shape[0]
    experts_all = local_experts * ep_count
    top_count = routes.shape[1]
    capacity = max(2, (row_count * top_count * 4 + 3 * experts_all - 1) // (3 * experts_all))
    flat_routes = routes.reshape(-1)
    slots = slot_numbers(flat_routes, experts_all)
    outbound = (
        jnp.zeros((experts_all, capacity, model_width), jnp.bfloat16)
        .at[flat_routes, slots]
        .set(jnp.repeat(ffn_in, top_count, axis=0))
    )
    arrived = lax.all_to_all(outbound, "ep", split_axis=0, concat_axis=0, tiled=True)
    slot_count = arrived.shape[1]
    grid = arrived.reshape(ep_count, local_experts, slot_count, model_width)
    gate_part = jnp.einsum("secd,edf->secf", grid, expert_gate, preferred_element_type=jnp.float32)
    up_part = jnp.einsum("secd,edf->secf", grid, expert_up, preferred_element_type=jnp.float32)
    hidden = (jax.nn.silu(gate_part) * up_part).astype(jnp.bfloat16)
    partial_out = jnp.einsum(
        "secf,efd->secd", hidden, expert_down, preferred_element_type=jnp.float32
    )
    partial_out = sum_at_owner(partial_out.astype(jnp.bfloat16), "tp", 3)
    partial_out = partial_out.reshape(ep_count * local_experts, slot_count, partial_out.shape[3])
    returned = lax.all_to_all(
        partial_out.astype(jnp.bfloat16), "ep", split_axis=0, concat_axis=0, tiled=True
    ).astype(partial_out.dtype)
    picked = returned[flat_routes, slots].reshape(row_count, top_count, returned.shape[2])
    shares = route_weight / jnp.sum(route_weight, axis=1, keepdims=True)
    expert_rows = jnp.sum(shares[:, :, None] * picked, axis=1)
    dense_slice = sum_at_owner((branch_share[:, None] * dense_back).astype(jnp.bfloat16), "tp", 1)
    width_part = dense_slice.shape[1]
    resid_slice = lax.dynamic_slice_in_dim(
        residual, lax.axis_index("tp") * width_part, width_part, 1
    )
    out_slice = (resid_slice.astype(jnp.float32) + expert_rows + dense_slice).astype(jnp.bfloat16)
    layer_out = collect(out_slice, "tp", 1)
    return (layer_out, new_matrix, new_norm, new_max)


def solution(mesh):
    in_specs = (
        P("ep", None),
        P("ep", "tp", None, None),
        P("ep", "tp", None),
        P("ep", "tp"),
        P(),
        P("ep", "tp"),
        P("ep", "tp"),
        P("ep", "tp"),
        P("ep", "tp"),
        P(),
        P(),
        P(),
        P("tp", "ep"),
        P(),
        P(),
        P("ep", None),
        P("ep", None),
        P("ep", None, "tp"),
        P("ep", None, "tp"),
        P("ep", "tp", None),
        P("ep", "tp"),
        P("ep", "tp"),
        P("tp", "ep"),
    )
    out_specs = (P("ep", None), P("ep", "tp", None, None), P("ep", "tp", None), P("ep", "tp"))
    return jax.shard_map(
        on_device, mesh=mesh, in_specs=in_specs, out_specs=out_specs, check_vma=False
    )
```

profile of v0, /device:TPU:1, one launch (start us, length us, event | category | flops | bytes accessed | tf_op | source)
XLA Modules:
  0.0 338.2 jit_solution(3360213346436248407)
XLA Ops:
  14.8 56.3 %all-gather.3.cloned.1.call-done = bf16[4096,512]{1,0:T(8,128)(2,1)} async-done(((bf16[256,512]{1,0:T(8,128)(2,1)}), bf16[4096,512]{1,0:T(8,128)(2,1)}) %all-gather.3.cloned.1.call-update) | async-done | bytes 4194320 | tf_op jit(solution)/shard_map/all_gather | solution.py:15
  72.8 2.2 fusion.61
  80.9 11.6 %all_to_all.82 = bf16[16,32,128]{2,1,0:T(8,128)(2,1)S(1)} all-to-all(bf16[16,32,128]{2,1,0:T(8,128)(2,1)S(1)} %broadcast_in_dim.10), channel_id=1, replica_groups=mesh['ep'=16,'tp'=16] {'ep'}, dimensions={0} | all-to-all | bytes 262144 | tf_op jit(solution)/shard_map/all_to_all | solution.py:20
  92.8 12.5 %all_to_all.83 = f32[16,32,256]{2,1,0:T(8,128)S(1)} all-to-all(f32[16,32,256]{2,1,0:T(8,128)S(1)} %fusion.57), channel_id=1, replica_groups=mesh['ep'=16,'tp'=16] {'ep'}, dimensions={0} | all-to-all | bytes 1048576 | tf_op jit(solution)/shard_map/all_to_all | solution.py:158
  106.6 56.4 %all-gather.5.cloned.1.call-done = f32[16,32,4096]{2,1,0:T(8,128)} async-done(((f32[1,32,4096]{2,1,0:T(8,128)}), f32[16,32,4096]{2,1,0:T(8,128)}) %all-gather.5.cloned.1.call-update) | async-done | bytes 8388624 | tf_op jit(solution)/shard_map/all_gather | solution.py:37
  163.0 3.8 %reduce_sum.97 = f32[32,4096]{1,0:T(8,128)S(1)} reduce(f32[16,32,4096]{2,1,0:T(8,128)} %all-gather.5.cloned.1.call-done, f32[]{:T(128)} %constant.13.clone.1), dimensions={0}, to_apply=%region_2.3 | reduce | flops 1966080 | bytes 8912900 | tf_op jit(solution)/shard_map/reduce_sum | solution.py:37
  167.2 14.6 %all_to_all.84 = bf16[32,16,256]{2,0,1:T(8,128)(2,1)S(1)} all-to-all(bf16[32,16,256]{2,0,1:T(8,128)(2,1)S(1)} %bitcast.138), channel_id=1, replica_groups=mesh['ep'=16,'tp'=16] {'ep'}, dimensions={1} | all-to-all | bytes 524288 | tf_op jit(solution)/shard_map/all_to_all | solution.py:163
  183.9 4.3 %all-to-all-start.6 = ((bf16[16,32,1024]{2,1,0:T(8,128)(2,1)}), bf16[16,32,1024]{2,1,0:T(8,128)(2,1)}, u32[]{:S(2)}, u32[]{:S(2)}) async-start(bf16[16,32,1024]{2,1,0:T(8,128)(2,1)} %bitcast.38), calls=%async_computation.6 | async-start | bytes 2097152 | tf_op jit(solution)/shard_map/all_to_all | solution.py:48
  190.5 13.4 %scatter_fusion = bf16[16,6,4096]{2,0,1:T(8,128)(2,1)S(1)} fusion(bf16[16,6,4096]{2,0,1:T(8,128)(2,1)S(1)} %broadcast_in_dim.11, s32[64]{0:T(128)S(1)} %get-tuple-element.28, bf16[64,4096]{1,0:T(8,128)(2,1)} %reshape.229), kind=kCustom, calls=%fused_computation.1 | custom fusion | bytes 1573376 | tf_op jit(solution)/shard_map/scatter | solution.py:192
  205.3 6.5 %all-to-all-start.2 = ((bf16[16,6,4096]{2,1,0:T(8,128)(2,1)}), bf16[16,6,4096]{2,1,0:T(8,128)(2,1)S(1)}, u32[]{:S(2)}, u32[]{:S(2)}) async-start(bf16[16,6,4096]{2,1,0:T(8,128)(2,1)} %copy.79), calls=%async_computation.2 | async-start | bytes 2097152 | tf_op jit(solution)/shard_map/all_to_all | solution.py:194
  213.3 13.7 %all-to-all-done.2 = bf16[16,6,4096]{2,1,0:T(8,128)(2,1)S(1)} async-done(((bf16[16,6,4096]{2,1,0:T(8,128)(2,1)}), bf16[16,6,4096]{2,1,0:T(8,128)(2,1)S(1)}, u32[]{:S(2)}, u32[]{:S(2)}) %all-to-all-start.2) | async-done | bytes 786464 | tf_op jit(solution)/shard_map/all_to_all | solution.py:194
  227.9 4.9 %all-to-all-start.7 = ((bf16[16,32,512]{2,1,0:T(8,128)(2,1)}), bf16[16,32,512]{2,1,0:T(8,128)(2,1)}, u32[]{:S(2)}, u32[]{:S(2)}) async-start(bf16[16,32,512]{2,1,0:T(8,128)(2,1)} %broadcast_in_dim.13), calls=%async_computation.7 | async-start | bytes 1048576 | tf_op jit(solution)/shard_map/all_to_all | solution.py:20
  232.8 2.3 fusion.7
  235.1 3.8 %convolution_convert_fusion = bf16[16,6,4096]{2,0,1:T(8,128)(2,1)} fusion(bf16[1,256,4096]{2,1,0:T(8,128)(2,1)S(1)} %copy-done, bf16[1,4096,256]{2,1,0:T(8,128)(2,1)} %param.41, bf16[16,6,4096]{2,1,0:T(8,128)(2,1)S(1)} %all-to-all-done.2, f32[16,1,6,256]{3,0,2,1:T(8,128)S(1)} %fusion.7), kind=kOutput, calls=%fused_computation.2 | convolution fusion | flops 403193856 | bytes 5865472 | tf_op jit(solution)/shard_map/secf,efd->secd/dot_general | solution.py:200
  238.9 2.1 copy.102
  242.2 7.5 %all-to-all-start.3 = ((bf16[16,16,1,6,256]{4,1,3,2,0:T(8,128)(2,1)}), bf16[16,16,1,6,256]{4,1,3,2,0:T(8,128)(2,1)S(1)}, u32[]{:S(2)}, u32[]{:S(2)}) async-start(bf16[16,16,1,6,256]{4,1,3,2,0:T(8,128)(2,1)} %bitcast.130), calls=%async_computation.3 | async-start | bytes 1572864 | tf_op jit(solution)/shard_map/all_to_all | solution.py:48
  251.8 20.6 %all-to-all-done.3 = bf16[16,16,1,6,256]{4,1,3,2,0:T(8,128)(2,1)S(1)} async-done(((bf16[16,16,1,6,256]{4,1,3,2,0:T(8,128)(2,1)}), bf16[16,16,1,6,256]{4,1,3,2,0:T(8,128)(2,1)S(1)}, u32[]{:S(2)}, u32[]{:S(2)}) %all-to-all-start.3) | async-done | bytes 786464 | tf_op jit(solution)/shard_map/all_to_all | solution.py:48
  272.4 5.2 %all-to-all-start.8 = ((f32[16,32,256]{2,1,0:T(8,128)}), f32[16,32,256]{2,1,0:T(8,128)}, u32[]{:S(2)}, u32[]{:S(2)}) async-start(f32[16,32,256]{2,1,0:T(8,128)} %fusion.49), calls=%async_computation.8 | async-start | bytes 1048576 | tf_op jit(solution)/shard_map/all_to_all | solution.py:181
  278.6 9.5 %all-to-all-done.8 = f32[16,32,256]{2,1,0:T(8,128)} async-done(((f32[16,32,256]{2,1,0:T(8,128)}), f32[16,32,256]{2,1,0:T(8,128)}, u32[]{:S(2)}, u32[]{:S(2)}) %all-to-all-start.8) | async-done | bytes 524320 | tf_op jit(solution)/shard_map/all_to_all | solution.py:181
  288.1 3.5 %all-to-all-start.4 = ((bf16[16,6,256]{2,1,0:T(8,128)(2,1)}), bf16[16,6,256]{2,1,0:T(8,128)(2,1)S(1)}, u32[]{:S(2)}, u32[]{:S(2)}) async-start(bf16[16,6,256]{2,1,0:T(8,128)(2,1)} %copy.83), calls=%async_computation.4 | async-start | bytes 131072 | tf_op jit(solution)/shard_map/all_to_all | solution.py:205
  293.5 5.0 %all-to-all-done.4 = bf16[16,6,256]{2,1,0:T(8,128)(2,1)S(1)} async-done(((bf16[16,6,256]{2,1,0:T(8,128)(2,1)}), bf16[16,6,256]{2,1,0:T(8,128)(2,1)S(1)}, u32[]{:S(2)}, u32[]{:S(2)}) %all-to-all-start.4) | async-done | bytes 49184 | tf_op jit(solution)/shard_map/all_to_all | solution.py:205
  298.4 5.4 %all-to-all-start.9 = ((bf16[16,32,256]{2,1,0:T(8,128)(2,1)}), bf16[16,32,256]{2,1,0:T(8,128)(2,1)S(1)}, u32[]{:S(2)}, u32[]{:S(2)}) async-start(bf16[16,32,256]{2,1,0:T(8,128)(2,1)} %multiply_convert_fusion), calls=%async_computation.9 | async-start | bytes 524288 | tf_op jit(solution)/shard_map/all_to_all | solution.py:48
  305.1 10.4 %all-to-all-done.9 = bf16[16,32,256]{2,1,0:T(8,128)(2,1)S(1)} async-done(((bf16[16,32,256]{2,1,0:T(8,128)(2,1)}), bf16[16,32,256]{2,1,0:T(8,128)(2,1)S(1)}, u32[]{:S(2)}, u32[]{:S(2)}) %all-to-all-start.9) | async-done | bytes 262176 | tf_op jit(solution)/shard_map/all_to_all | solution.py:48
  316.3 14.4 %all_to_all.85 = bf16[16,32,256]{2,1,0:T(8,128)(2,1)S(1)} all-to-all(bf16[16,32,256]{2,1,0:T(8,128)(2,1)S(1)} %broadcast_in_dim.14), channel_id=1, replica_groups=mesh['ep'=16,'tp'=16] {'tp'}, dimensions={0} | all-to-all | bytes 524288 | tf_op jit(solution)/shard_map/all_to_all | solution.py:20
  (97 shorter events, 33.7 us)
Async XLA Ops:
  7.2 227.9 %copy-start = (bf16[1,256,4096]{2,1,0:T(8,128)(2,1)S(1)}, bf16[1,256,4096]{2,1,0:T(8,128)(2,1)}, u32[]{:S(2)}) copy-start(bf16[1,256,4096]{2,1,0:T(8,128)(2,1)} %param.42) | copy-start | bytes 6291460
  7.2 63.9 %copy-start.4 = (bf16[32,4096]{1,0:T(8,128)(2,1)S(1)}, bf16[32,4096]{1,0:T(8,128)(2,1)}, u32[]{:S(2)}) copy-start(bf16[32,4096]{1,0:T(8,128)(2,1)} %param.23) | copy-start | bytes 786436
  7.2 63.9 %copy-start.16 = (f32[4096]{0:T(1024)S(1)}, f32[4096]{0:T(1024)}, u32[]{:S(2)}) copy-start(f32[4096]{0:T(1024)} %param.27) | copy-start | bytes 49156
  7.2 6.8 %copy-start.14 = (f32[32,1]{0,1:T(1,128)S(1)}, f32[32,1]{0,1:T(1,128)}, u32[]{:S(2)}) copy-start(f32[32,1]{0,1:T(1,128)} %param.26) | copy-start | bytes 388
  7.2 65.6 %copy-start.15 = (f32[32,1,128]{2,1,0:T(1,128)S(1)}, f32[32,1,128]{2,1,0:T(1,128)}, u32[]{:S(2)}) copy-start(f32[32,1,128]{2,1,0:T(1,128)} %param.25) | copy-start | bytes 49156
  7.2 63.9 %all-gather.3.cloned.1.call-start = ((), (), s32[]{:S(2)}) async-start(), calls=%async_computation.11 | async-start | bytes 4456448 | tf_op jit(solution)/shard_map/all_gather | solution.py:15
  9.1 153.8 %all-gather.5.cloned.1.call-start = ((), (), s32[]{:S(2)}) async-start(), calls=%async_computation.12 | async-start | bytes 8912896 | tf_op jit(solution)/shard_map/all_gather | solution.py:37
  14.7 61.9 %copy-start.12 = (f32[32,1]{0,1:T(1,128)}, f32[32,1]{0,1:T(1,128)S(1)}, u32[]{:S(2)}) copy-start(f32[32,1]{0,1:T(1,128)S(1)} %get-tuple-element.35) | copy-start | bytes 388
  77.4 15.1 %copy-start.1 = (f32[32,1,128,128]{3,2,1,0:T(8,128)}, f32[32,1,128,128]{3,2,1,0:T(8,128)S(1)}, u32[]{:S(2)}) copy-start(f32[32,1,128,128]{3,2,1,0:T(8,128)S(1)} %multiply_add_fusion) | copy-start | bytes 6291460
  77.4 15.1 %copy-start.8 = (bf16[128,256]{1,0:T(8,128)(2,1)S(1)}, bf16[128,256]{1,0:T(8,128)(2,1)}, u32[]{:S(2)}) copy-start(bf16[128,256]{1,0:T(8,128)(2,1)} %param.35) | copy-start | bytes 196612
  106.5 60.5 %copy-start.9 = (f32[4096]{0:T(1024)S(1)}, f32[4096]{0:T(1024)}, u32[]{:S(2)}) copy-start(f32[4096]{0:T(1024)} %param.36) | copy-start | bytes 49156
  166.8 15.0 %copy-start.6 = (bf16[256,512]{1,0:T(8,128)(2,1)S(1)}, bf16[256,512]{1,0:T(8,128)(2,1)}, u32[]{:S(2)}) copy-start(bf16[256,512]{1,0:T(8,128)(2,1)} %param.44) | copy-start | bytes 786436
  166.8 15.3 %copy-start.7 = (bf16[256,512]{1,0:T(8,128)(2,1)S(1)}, bf16[256,512]{1,0:T(8,128)(2,1)}, u32[]{:S(2)}) copy-start(bf16[256,512]{1,0:T(8,128)(2,1)} %param.43) | copy-start | bytes 786436
  167.0 15.1 %copy-start.3 = (bf16[32,4096]{1,0:T(8,128)(2,1)}, bf16[32,4096]{1,0:T(8,128)(2,1)S(1)}, u32[]{:S(2)}) copy-start(bf16[32,4096]{1,0:T(8,128)(2,1)S(1)} %get-tuple-element.31) | copy-start | bytes 786436
  183.9 21.4 %all-to-all-start.6 = ((bf16[16,32,1024]{2,1,0:T(8,128)(2,1)}), bf16[16,32,1024]{2,1,0:T(8,128)(2,1)}, u32[]{:S(2)}, u32[]{:S(2)}) async-start(bf16[16,32,1024]{2,1,0:T(8,128)(2,1)} %bitcast.38), calls=%async_computation.6 | async-start | bytes 2097152 | tf_op jit(solution)/shard_map/all_to_all | solution.py:48
  205.3 21.7 %all-to-all-start.2 = ((bf16[16,6,4096]{2,1,0:T(8,128)(2,1)}), bf16[16,6,4096]{2,1,0:T(8,128)(2,1)S(1)}, u32[]{:S(2)}, u32[]{:S(2)}) async-start(bf16[16,6,4096]{2,1,0:T(8,128)(2,1)} %copy.79), calls=%async_computation.2 | async-start | bytes 2097152 | tf_op jit(solution)/shard_map/all_to_all | solution.py:194
  227.9 14.3 %all-to-all-start.7 = ((bf16[16,32,512]{2,1,0:T(8,128)(2,1)}), bf16[16,32,512]{2,1,0:T(8,128)(2,1)}, u32[]{:S(2)}, u32[]{:S(2)}) async-start(bf16[16,32,512]{2,1,0:T(8,128)(2,1)} %broadcast_in_dim.13), calls=%async_computation.7 | async-start | bytes 1048576 | tf_op jit(solution)/shard_map/all_to_all | solution.py:20
  238.9 10.8 %copy-start.5 = (bf16[512,256]{1,0:T(8,128)(2,1)S(1)}, bf16[512,256]{1,0:T(8,128)(2,1)}, u32[]{:S(2)}) copy-start(bf16[512,256]{1,0:T(8,128)(2,1)} %param.45) | copy-start | bytes 786436
  241.0 36.5 %copy-start.11 = (f32[32,2]{0,1:T(2,128)S(1)}, f32[32,2]{0,1:T(2,128)}, u32[]{:S(2)}) copy-start(f32[32,2]{0,1:T(2,128)} %param.39) | copy-start | bytes 772
  241.1 36.5 %copy-start.10 = (bf16[4096]{0:T(1024)(128)(2,1)S(1)}, bf16[4096]{0:T(1024)(128)(2,1)}, u32[]{:S(2)}) copy-start(bf16[4096]{0:T(1024)(128)(2,1)} %param.37) | copy-start | bytes 24580
  242.2 30.2 %all-to-all-start.3 = ((bf16[16,16,1,6,256]{4,1,3,2,0:T(8,128)(2,1)}), bf16[16,16,1,6,256]{4,1,3,2,0:T(8,128)(2,1)S(1)}, u32[]{:S(2)}, u32[]{:S(2)}) async-start(bf16[16,16,1,6,256]{4,1,3,2,0:T(8,128)(2,1)} %bitcast.130), calls=%async_computation.3 | async-start | bytes 1572864 | tf_op jit(solution)/shard_map/all_to_all | solution.py:48
  272.4 15.7 %all-to-all-start.8 = ((f32[16,32,256]{2,1,0:T(8,128)}), f32[16,32,256]{2,1,0:T(8,128)}, u32[]{:S(2)}, u32[]{:S(2)}) async-start(f32[16,32,256]{2,1,0:T(8,128)} %fusion.49), calls=%async_computation.8 | async-start | bytes 1048576 | tf_op jit(solution)/shard_map/all_to_all | solution.py:181
  288.1 10.3 %all-to-all-start.4 = ((bf16[16,6,256]{2,1,0:T(8,128)(2,1)}), bf16[16,6,256]{2,1,0:T(8,128)(2,1)S(1)}, u32[]{:S(2)}, u32[]{:S(2)}) async-start(bf16[16,6,256]{2,1,0:T(8,128)(2,1)} %copy.83), calls=%async_computation.4 | async-start | bytes 131072 | tf_op jit(solution)/shard_map/all_to_all | solution.py:205
  298.4 17.0 %all-to-all-start.9 = ((bf16[16,32,256]{2,1,0:T(8,128)(2,1)}), bf16[16,32,256]{2,1,0:T(8,128)(2,1)S(1)}, u32[]{:S(2)}, u32[]{:S(2)}) async-start(bf16[16,32,256]{2,1,0:T(8,128)(2,1)} %multiply_convert_fusion), calls=%async_computation.9 | async-start | bytes 524288 | tf_op jit(solution)/shard_map/all_to_all | solution.py:48
  (2 other events, 11.2 us)
Sparse Core Ops, SparseCore 0:
  11.0 60.0 all-gather.2
  106.7 56.2 all-gather.4
where the time goes:
time: 340 us; the launch traced here: 338 us
  waiting for transfers between devices  173 us (51%)
  blocking collectives  53.1 us (16%)
  starting transfers between devices  37.5 us (11%)
  local copies, waits for them, and re-layouts  26 us (8%)
  matrix products  20.7 us (6%)
  between operations  14.5 us (4%)
  other arithmetic  13.4 us (4%)
    all_gather x1, waiting for transfers between devices, total_of_pieces(): return lax.all_gather(shard, axis).sum(0)  56.4 us
    all_gather x1, waiting for transfers between devices, side_by_side(): lax.all_gather(both, axis, axis=dim, tiled=True)  56.3 us
    all_to_all x3, waiting for transfers between devices, sum_at_owner(): lax.all_to_all(parts, axis, split_axis=0, concat_axis=0, tiled=True)  31 us
    all_to_all x2, blocking collectives, from_everyone(): lax.all_to_all(jnp.broadcast_to(shard[None], (devices, *shard.shape)), ax...  26 us
    all_to_all x3, starting transfers between devices, sum_at_owner(): lax.all_to_all(parts, axis, split_axis=0, concat_axis=0, tiled=True)  17.3 us
    scatter x2, local copies, waits for them, and re-layouts, on_device(): outbound = jnp.zeros((experts_all, capacity, model_width), jnp.bfloat16)....  14.8 us
    all_to_all x1, blocking collectives, on_device(): lax.all_to_all(ffn_in, 'ep', split_axis=1, concat_axis=0, tiled=True)  14.6 us
    all_to_all x1, waiting for transfers between devices, on_device(): lax.all_to_all(outbound, 'ep', split_axis=0, concat_axis=0, tiled=True)  13.7 us
  transfers between devices with their start and end apart: 9, of which 8 were waited for; matrix products, arithmetic and copies ran while one was open for 11% of the time, Pallas kernels for 0%

commit v1 on v0

v1 whole, which is shorter than its diff:
```python
import jax
import jax.numpy as jnp
from jax import lax
from jax.sharding import PartitionSpec as P

EPS = 1e-06
BF = jnp.bfloat16
F32 = jnp.float32


def swap(parts, axis):
    return lax.all_to_all(parts, axis, 0, 0, tiled=True)


def copies(shard, axis):
    return swap(jnp.broadcast_to(shard[None], (lax.axis_size(axis), *shard.shape)), axis)


def split_exact(x):
    high = lax.reduce_precision(x, 8, 7)
    return high.astype(BF), (x - high).astype(BF)


def slot_numbers(flat_routes, experts_all):
    onehot = (flat_routes[:, None] == jnp.arange(experts_all, dtype=jnp.int32)[None, :]).astype(
        jnp.int32
    )
    before = jnp.cumsum(onehot, axis=0) - onehot
    return jnp.sum(before * onehot, axis=1)


def on_device(
    tokens,
    state_matrix,
    state_norm,
    state_max,
    mixer_gain,
    w_query,
    w_key,
    w_value,
    w_outgate,
    w_ingate,
    w_forget,
    forget_bias,
    w_proj,
    ffn_gain,
    w_branch,
    routes,
    route_weight,
    expert_gate,
    expert_up,
    expert_down,
    dense_gate,
    dense_up,
    dense_down,
):
    rows, width = tokens.shape
    n_ep, n_tp = lax.axis_size("ep"), lax.axis_size("tp")
    my_e, my_t = lax.axis_index("ep"), lax.axis_index("tp")
    cols = width // n_ep
    everyone = rows * n_ep
    cap = 6
    dot = lambda a, b: jnp.dot(a, b, preferred_element_type=F32)

    token_cols = swap(jnp.moveaxis(tokens.reshape(rows, n_ep, cols), 1, 0), "ep")

    wide = tokens.astype(F32)
    scale = lax.rsqrt(jnp.mean(wide * wide, axis=-1, keepdims=True) + EPS)
    normed = (wide * scale * mixer_gain).astype(BF)
    gate_in = lax.dynamic_slice_in_dim(dot(normed, w_ingate), my_t, 1, 1)
    gate_forget = lax.dynamic_slice_in_dim(dot(normed, w_forget) + forget_bias, my_t, 1, 1)

    flat_routes = routes.reshape(-1)
    slots = slot_numbers(flat_routes, n_ep)
    code = (flat_routes * 8 + slots).reshape(rows, 2)

    gain_cols = lax.dynamic_slice_in_dim(mixer_gain, my_e * cols, cols, 0)
    scaled = (token_cols.reshape(everyone, cols).astype(F32) * gain_cols).astype(BF)
    partial = jnp.concatenate(
        [dot(scaled, w).astype(BF) for w in (w_query, w_key, w_value, w_outgate)], axis=1
    )
    projected = swap(partial.reshape(n_ep, rows, -1), "ep").astype(F32).sum(0) * scale
    head = projected.shape[1] // 4
    query, key, value, outgate = (projected[:, i * head : (i + 1) * head] for i in range(4))

    key = key * head ** (-0.5)
    log_keep = jax.nn.log_sigmoid(gate_forget)
    new_max = jnp.maximum(log_keep + state_max, gate_in)
    keep = jnp.exp(log_keep + state_max - new_max)
    write = jnp.exp(gate_in - new_max)
    new_matrix = (
        keep[:, :, None] * state_matrix[:, 0]
        + write[:, :, None] * key[:, :, None] * value[:, None, :]
    )
    new_norm = keep * state_norm[:, 0] + write * key
    numer = jnp.einsum("bk,bkv->bv", query, new_matrix, precision=lax.Precision.HIGHEST)
    denom = jnp.sum(query * new_norm, axis=-1, keepdims=True)
    cell = numer / jnp.maximum(jnp.abs(denom), 1.0)
    mixed = (jax.nn.sigmoid(outgate) * cell).astype(BF)

    extra = jnp.pad(code.reshape(1, -1).astype(BF), ((0, 7), (0, head - 2 * rows)))
    mixed_all = copies(jnp.concatenate([mixed, extra], axis=0), "ep")
    codes_all = mixed_all[:, rows, : 2 * rows].reshape(everyone, 2).astype(jnp.int32)
    mixed_all = mixed_all[:, :rows].reshape(everyone, head)

    spread = dot(mixed_all, w_proj).astype(BF).reshape(n_tp, rows, cols)
    mixer_out = swap(spread, "tp").astype(F32).sum(0)
    token_block = lax.dynamic_index_in_dim(token_cols, my_t, 0, keepdims=False)
    resid_block = (token_block.astype(F32) + mixer_out).astype(BF)
    resid_turned = lax.ppermute(
        resid_block, ("ep", "tp"), [(a * n_tp + b, b * n_tp + a) for a in range(n_ep) for b in range(n_tp)]
    )
    resid = copies(resid_block, "tp").reshape(everyone, cols)

    resid_wide = resid.astype(F32)
    ffn_gain_cols = lax.dynamic_slice_in_dim(ffn_gain, my_e * cols, cols, 0)
    branch_cols = lax.dynamic_slice_in_dim(w_branch, my_e * cols, cols, 0)
    gained_wide = resid_wide * ffn_gain_cols
    gained = gained_wide.astype(BF)
    squares = split_exact(jnp.sum(resid_wide * resid_wide, axis=1, keepdims=True))
    branch = split_exact(jnp.sum(gained_wide * branch_cols.astype(F32), axis=1, keepdims=True))
    side = jnp.pad(jnp.concatenate([*squares, *branch], axis=1), ((0, 0), (0, 124)))
    gate_up = jnp.concatenate(
        [dot(gained, dense_gate).astype(BF), dot(gained, dense_up).astype(BF), side], axis=1
    )
    at = jnp.arange(n_ep * cap, dtype=jnp.int32)
    wanted = jnp.arange(n_ep, dtype=jnp.int32)[:, None] * 8 + (at % cap)[None, :]
    member = (
        jnp.any(codes_all[None, None, :, :] == wanted[:, :, None, None], axis=-1)
        & ((jnp.arange(everyone, dtype=jnp.int32) // rows)[None, None, :] == (at // cap)[None, :, None])
    )
    outbound = dot(member.astype(BF).reshape(n_ep * n_ep * cap, everyone), resid).astype(BF)
    arrived = swap(outbound.reshape(n_ep, n_ep * cap, cols), "ep")
    summed = swap(gate_up.reshape(n_ep, rows, -1), "ep").astype(F32).sum(0)

    units = dense_gate.shape[1]
    ffn_scale = lax.rsqrt((summed[:, 2 * units] + summed[:, 2 * units + 1])[:, None] / width + EPS)
    branch_share = jax.nn.sigmoid((summed[:, 2 * units + 2] + summed[:, 2 * units + 3])[:, None] * ffn_scale)
    hidden = (jax.nn.silu(summed[:, :units] * ffn_scale) * (summed[:, units : 2 * units] * ffn_scale)).astype(BF)
    hidden_all = copies(hidden, "ep").reshape(everyone, units)

    rows_in = jnp.moveaxis(arrived, 0, 1).reshape(n_ep * cap, width).astype(F32)
    row_scale = lax.rsqrt(jnp.mean(rows_in * rows_in, axis=-1, keepdims=True) + EPS)
    rows_in = (rows_in * row_scale * ffn_gain).astype(BF)
    expert_hidden = (jax.nn.silu(dot(rows_in, expert_gate[0])) * dot(rows_in, expert_up[0])).astype(BF)
    expert_rows = dot(expert_hidden, expert_down[0]).astype(BF).reshape(n_ep, cap, width)
    returned = swap(expert_rows, "ep").reshape(n_ep * cap, width)

    dense_back = swap(dot(hidden_all, dense_down).astype(BF).reshape(n_ep, rows, cols), "ep")
    dense_back = jnp.moveaxis(dense_back, 0, 1).reshape(rows, width).astype(F32)

    shares = route_weight / jnp.sum(route_weight, axis=1, keepdims=True)
    place = (jnp.arange(n_ep, dtype=jnp.int32)[:, None] * 8 + jnp.arange(cap, dtype=jnp.int32)[None]).reshape(-1)
    mixing = jnp.sum(jnp.where(code[:, :, None] == place[None, None, :], shares[:, :, None], 0.0), axis=1)
    expert_sum = jnp.dot(mixing, returned.astype(F32), precision=lax.Precision.HIGHEST)
    total = (expert_sum + branch_share * dense_back).astype(BF)
    total = swap(jnp.moveaxis(total.reshape(rows, n_tp, width // n_tp), 1, 0), "tp").astype(F32).sum(0)
    out_block = (resid_turned.astype(F32) + total).astype(BF)
    layer_out = jnp.moveaxis(copies(out_block, "tp"), 0, 1).reshape(rows, width)
    return (layer_out, new_matrix[:, None], new_norm[:, None], new_max)


def solution(mesh):
    in_specs = (
        P("ep", None),
        P("ep", "tp", None, None),
        P("ep", "tp", None),
        P("ep", "tp"),
        P(),
        P("ep", "tp"),
        P("ep", "tp"),
        P("ep", "tp"),
        P("ep", "tp"),
        P(),
        P(),
        P(),
        P("tp", "ep"),
        P(),
        P(),
        P("ep", None),
        P("ep", None),
        P("ep", None, "tp"),
        P("ep", None, "tp"),
        P("ep", "tp", None),
        P("ep", "tp"),
        P("ep", "tp"),
        P("tp", "ep"),
    )
    out_specs = (P("ep", None), P("ep", "tp", None, None), P("ep", "tp", None), P("ep", "tp"))
    return jax.shard_map(
        on_device, mesh=mesh, in_specs=in_specs, out_specs=out_specs, check_vma=False
    )
```

time: 340 us -> 227 us (0.67)
  waiting for transfers between devices: 173 us -> 106 us
  blocking collectives: 53.1 us -> 0 us
  starting transfers between devices: 37.5 us -> 70.1 us
  between operations: 14.5 us -> 1.37 us
  local copies, waits for them, and re-layouts: 26 us -> 16.1 us
    all_gather x2 -> x0, waiting for transfers between devices: 113 us -> none  [the longest x1 56.4 us: total_of_pieces(): return lax.all_gather(shard, axis).sum(0)]
    all_to_all x4 -> x0, blocking collectives: 53.1 us -> none  [the longest x2 26 us: from_everyone(): lax.all_to_all(jnp.broadcast_to(shard[None], (devices, *shard.shape)), ax...]
    all_to_all x7 -> x12, waiting for transfers between devices: 60.3 us -> 106 us  [swap(): return lax.all_to_all(parts, axis, 0, 0, tiled=True)]
    all_to_all x7 -> x12, starting transfers between devices: 37.4 us -> 67.8 us  [swap(): return lax.all_to_all(parts, axis, 0, 0, tiled=True)]
    scatter x2 -> x0, local copies, waits for them, and re-layouts: 14.8 us -> none  [on_device(): outbound = jnp.zeros((experts_all, capacity, model_width), jnp.bfloat16)....]
    reduce_sum x7 -> x9, other arithmetic: 6.88 us -> 4.05 us  [the longest x1 1.45 us: on_device(): summed = swap(gate_up.reshape(n_ep, rows, -1), 'ep').astype(F32).sum(0)]
    dot_general x14 -> x15, matrix products: 20.7 us -> 18.6 us  [the longest x13 14.5 us: on_device(): dot = lambda a, b: jnp.dot(a, b, preferred_element_type=F32)]
  transfers between devices with their start and end apart: 9 -> 13, of which waited for: 8 -> 12; matrix products, arithmetic and copies ran while one was open for 11% -> 13% of each run, Pallas kernels for 0% -> 0%
where the time goes in v1:
time: 227 us; the launch traced here: 226 us
  waiting for transfers between devices  106 us (47%)
  starting transfers between devices  70.1 us (31%)
  matrix products  18.6 us (8%)
  local copies, waits for them, and re-layouts  16.1 us (7%)
  other arithmetic  14.1 us (6%)
    all_to_all x12, waiting for transfers between devices, swap(): return lax.all_to_all(parts, axis, 0, 0, tiled=True)  106 us
    all_to_all x12, starting transfers between devices, swap(): return lax.all_to_all(parts, axis, 0, 0, tiled=True)  67.8 us
    dot_general x13, matrix products, on_device(): dot = lambda a, b: jnp.dot(a, b, preferred_element_type=F32)  14.5 us
  transfers between devices with their start and end apart: 13, of which 12 were waited for; matrix products, arithmetic and copies ran while one was open for 13% of the time, Pallas kernels for 0%

profile of v1, /device:TPU:1, one launch (start us, length us, event | category | flops | bytes accessed | tf_op | source)
XLA Modules:
  0.0 225.8 jit_solution(8304466030562065241)
XLA Ops:
  2.7 7.7 %all-to-all-start = ((bf16[16,32,256]{2,1,0:T(8,128)(2,1)}), bf16[16,32,256]{2,1,0:T(8,128)(2,1)S(1)}, u32[]{:S(2)}, u32[]{:S(2)}) async-start(bf16[16,32,256]{2,1,0:T(8,128)(2,1)} %copy.68), calls=%async_computation | async-start | bytes 524288 | tf_op jit(solution)/shard_map/all_to_all | solution.py:12
  20.0 4.5 %all-to-all-start.1 = ((bf16[16,32,512]{2,1,0:T(8,128)(2,1)}), bf16[16,32,512]{2,1,0:T(8,128)(2,1)S(1)}, u32[]{:S(2)}, u32[]{:S(2)}) async-start(bf16[16,32,512]{2,1,0:T(8,128)(2,1)} %bitcast.3), calls=%async_computation.1 | async-start | bytes 1048576 | tf_op jit(solution)/shard_map/all_to_all | solution.py:12
  24.7 10.0 %all-to-all-done.1 = bf16[16,32,512]{2,1,0:T(8,128)(2,1)S(1)} async-done(((bf16[16,32,512]{2,1,0:T(8,128)(2,1)}), bf16[16,32,512]{2,1,0:T(8,128)(2,1)S(1)}, u32[]{:S(2)}, u32[]{:S(2)}) %all-to-all-start.1) | async-done | bytes 524320 | tf_op jit(solution)/shard_map/all_to_all | solution.py:12
  35.7 3.7 %fusion.7 = f32[32,1,128]{2,1,0:T(1,128)S(1)} fusion(f32[32,128,1]{1,2,0:T(1,128)S(1)} %bitcast.122, f32[32,1,128,128]{3,2,1,0:T(8,128)} %param.24, f32[32,128]{1,0:T(8,128)S(1)} %get-tuple-element.13, f32[32,128]{1,0:T(8,128)S(1)} %get-tuple-element.10, f32[32]{0:T(128)S(1)} %get-tuple-element.11), kind=kOutput, calls=%fused_computation.13 | convolution fusion | flops 7864320 | bytes 2162816 | tf_op jit(solution)/shard_map/bk,bkv->bv/dot_general | solution.py:96
  40.2 3.5 %all-to-all-start.2 = ((bf16[16,40,128]{2,1,0:T(8,128)(2,1)}), bf16[16,40,128]{2,1,0:T(8,128)(2,1)S(1)}, u32[]{:S(2)}, u32[]{:S(2)}) async-start(bf16[16,40,128]{2,1,0:T(8,128)(2,1)} %broadcast_in_dim.20), calls=%async_computation.2 | async-start | bytes 327680 | tf_op jit(solution)/shard_map/all_to_all | solution.py:12
  44.5 6.2 %all-to-all-done.2 = bf16[16,40,128]{2,1,0:T(8,128)(2,1)S(1)} async-done(((bf16[16,40,128]{2,1,0:T(8,128)(2,1)}), bf16[16,40,128]{2,1,0:T(8,128)(2,1)S(1)}, u32[]{:S(2)}, u32[]{:S(2)}) %all-to-all-start.2) | async-done | bytes 163872 | tf_op jit(solution)/shard_map/all_to_all | solution.py:12
  51.7 11.9 %all-to-all-start.3 = ((bf16[16,32,256]{2,1,0:T(8,128)(2,1)}), bf16[16,32,256]{2,1,0:T(8,128)(2,1)S(1)}, u32[]{:S(2)}, u32[]{:S(2)}) async-start(bf16[16,32,256]{2,1,0:T(8,128)(2,1)} %bitcast.14), calls=%async_computation.3 | async-start | bytes 524288 | tf_op jit(solution)/shard_map/all_to_all | solution.py:12
  64.2 11.0 %all-to-all-done.3 = bf16[16,32,256]{2,1,0:T(8,128)(2,1)S(1)} async-done(((bf16[16,32,256]{2,1,0:T(8,128)(2,1)}), bf16[16,32,256]{2,1,0:T(8,128)(2,1)S(1)}, u32[]{:S(2)}, u32[]{:S(2)}) %all-to-all-start.3) | async-done | bytes 262176 | tf_op jit(solution)/shard_map/all_to_all | solution.py:12
  76.0 3.4 %all-to-all-start.4 = ((bf16[16,32,256]{2,1,0:T(8,128)(2,1)}), bf16[16,32,256]{2,1,0:T(8,128)(2,1)S(1)}, u32[]{:S(2)}, u32[]{:S(2)}) async-start(bf16[16,32,256]{2,1,0:T(8,128)(2,1)} %broadcast_in_dim.24), calls=%async_computation.4 | async-start | bytes 524288 | tf_op jit(solution)/shard_map/all_to_all | solution.py:12
  80.5 10.0 %all-to-all-done.4 = bf16[16,32,256]{2,1,0:T(8,128)(2,1)S(1)} async-done(((bf16[16,32,256]{2,1,0:T(8,128)(2,1)}), bf16[16,32,256]{2,1,0:T(8,128)(2,1)S(1)}, u32[]{:S(2)}, u32[]{:S(2)}) %all-to-all-start.4) | async-done | bytes 262176 | tf_op jit(solution)/shard_map/all_to_all | solution.py:12
  92.4 3.6 %all-to-all-start.5 = ((bf16[16,96,256]{2,1,0:T(8,128)(2,1)}), bf16[16,96,256]{2,1,0:T(8,128)(2,1)S(1)}, u32[]{:S(2)}, u32[]{:S(2)}) async-start(bf16[16,96,256]{2,1,0:T(8,128)(2,1)} %bitcast.117), calls=%async_computation.5 | async-start | bytes 1572864 | tf_op jit(solution)/shard_map/all_to_all | solution.py:12
  101.2 9.8 %all-to-all-done.5 = bf16[16,96,256]{2,1,0:T(8,128)(2,1)S(1)} async-done(((bf16[16,96,256]{2,1,0:T(8,128)(2,1)}), bf16[16,96,256]{2,1,0:T(8,128)(2,1)S(1)}, u32[]{:S(2)}, u32[]{:S(2)}) %all-to-all-start.5) | async-done | bytes 786464 | tf_op jit(solution)/shard_map/all_to_all | solution.py:12
  111.0 4.4 %all-to-all-start.7 = ((bf16[16,32,1152]{2,1,0:T(8,128)(2,1)}), bf16[16,32,1152]{2,1,0:T(8,128)(2,1)}, u32[]{:S(2)}, u32[]{:S(2)}) async-start(bf16[16,32,1152]{2,1,0:T(8,128)(2,1)} %bitcast.106), calls=%async_computation.7 | async-start | bytes 2359296 | tf_op jit(solution)/shard_map/all_to_all | solution.py:12
  116.0 17.0 %all-to-all-done.7 = bf16[16,32,1152]{2,1,0:T(8,128)(2,1)} async-done(((bf16[16,32,1152]{2,1,0:T(8,128)(2,1)}), bf16[16,32,1152]{2,1,0:T(8,128)(2,1)}, u32[]{:S(2)}, u32[]{:S(2)}) %all-to-all-start.7) | async-done | bytes 1179680 | tf_op jit(solution)/shard_map/all_to_all | solution.py:12
  136.3 5.0 %all-to-all-start.8 = ((bf16[16,32,512]{2,1,0:T(8,128)(2,1)}), bf16[16,32,512]{2,1,0:T(8,128)(2,1)S(1)}, u32[]{:S(2)}, u32[]{:S(2)}) async-start(bf16[16,32,512]{2,1,0:T(8,128)(2,1)} %broadcast_in_dim.25), calls=%async_computation.8 | async-start | bytes 1048576 | tf_op jit(solution)/shard_map/all_to_all | solution.py:12
  143.3 3.8 %convolution_convert_fusion = bf16[96,4096]{1,0:T(8,128)(2,1)} fusion(bf16[1,256,4096]{2,1,0:T(8,128)(2,1)S(1)} %copy-done, bf16[96,4096]{1,0:T(8,128)(2,1)S(1)} %bitcast.105, bf16[1,4096,256]{2,1,0:T(8,128)(2,1)} %param.41, f32[96,256]{1,0:T(8,128)S(1)} %fusion.4), kind=kOutput, calls=%fused_computation.1 | convolution fusion | flops 403193856 | bytes 5865472 | tf_op jit(solution)/shard_map/dot_general | solution.py:63
  152.6 4.2 %all-to-all-start.6 = ((bf16[16,6,4096]{2,1,0:T(8,128)(2,1)}), bf16[16,6,4096]{2,1,0:T(8,128)(2,1)S(1)}, u32[]{:S(2)}, u32[]{:S(2)}) async-start(bf16[16,6,4096]{2,1,0:T(8,128)(2,1)} %reshape.382), calls=%async_computation.6 | async-start | bytes 2097152 | tf_op jit(solution)/shard_map/all_to_all | solution.py:12
  159.3 13.0 %all-to-all-done.6 = bf16[16,6,4096]{2,1,0:T(8,128)(2,1)S(1)} async-done(((bf16[16,6,4096]{2,1,0:T(8,128)(2,1)}), bf16[16,6,4096]{2,1,0:T(8,128)(2,1)S(1)}, u32[]{:S(2)}, u32[]{:S(2)}) %all-to-all-start.6) | async-done | bytes 786464 | tf_op jit(solution)/shard_map/all_to_all | solution.py:12
  172.2 4.8 %all-to-all-start.9 = ((bf16[16,32,256]{2,1,0:T(8,128)(2,1)}), bf16[16,32,256]{2,1,0:T(8,128)(2,1)S(1)}, u32[]{:S(2)}, u32[]{:S(2)}) async-start(bf16[16,32,256]{2,1,0:T(8,128)(2,1)} %bitcast.115), calls=%async_computation.9 | async-start | bytes 524288 | tf_op jit(solution)/shard_map/all_to_all | solution.py:12
  178.3 6.4 %all-to-all-done.9 = bf16[16,32,256]{2,1,0:T(8,128)(2,1)S(1)} async-done(((bf16[16,32,256]{2,1,0:T(8,128)(2,1)}), bf16[16,32,256]{2,1,0:T(8,128)(2,1)S(1)}, u32[]{:S(2)}, u32[]{:S(2)}) %all-to-all-start.9) | async-done | bytes 262176 | tf_op jit(solution)/shard_map/all_to_all | solution.py:12
  186.0 6.3 %all-to-all-start.10 = ((bf16[16,32,256]{2,1,0:T(8,128)(2,1)}), bf16[16,32,256]{2,1,0:T(8,128)(2,1)S(1)}, u32[]{:S(2)}, u32[]{:S(2)}) async-start(bf16[16,32,256]{2,1,0:T(8,128)(2,1)} %bitcast.103), calls=%async_computation.10 | async-start | bytes 524288 | tf_op jit(solution)/shard_map/all_to_all | solution.py:12
  195.3 9.0 %all-to-all-done.10 = bf16[16,32,256]{2,1,0:T(8,128)(2,1)S(1)} async-done(((bf16[16,32,256]{2,1,0:T(8,128)(2,1)}), bf16[16,32,256]{2,1,0:T(8,128)(2,1)S(1)}, u32[]{:S(2)}, u32[]{:S(2)}) %all-to-all-start.10) | async-done | bytes 262176 | tf_op jit(solution)/shard_map/all_to_all | solution.py:12
  205.1 8.4 %all-to-all-start.11 = ((bf16[16,32,256]{2,1,0:T(8,128)(2,1)}), bf16[16,32,256]{2,1,0:T(8,128)(2,1)S(1)}, u32[]{:S(2)}, u32[]{:S(2)}) async-start(bf16[16,32,256]{2,1,0:T(8,128)(2,1)} %broadcast_in_dim.26), calls=%async_computation.11 | async-start | bytes 524288 | tf_op jit(solution)/shard_map/all_to_all | solution.py:12
  216.5 8.6 %all-to-all-done.11 = bf16[16,32,256]{2,1,0:T(8,128)(2,1)S(1)} async-done(((bf16[16,32,256]{2,1,0:T(8,128)(2,1)}), bf16[16,32,256]{2,1,0:T(8,128)(2,1)S(1)}, u32[]{:S(2)}, u32[]{:S(2)}) %all-to-all-start.11) | async-done | bytes 262176 | tf_op jit(solution)/shard_map/all_to_all | solution.py:12
  (150 shorter events, 48.3 us)
Async XLA Ops:
  0.6 142.7 %copy-start = (bf16[1,256,4096]{2,1,0:T(8,128)(2,1)S(1)}, bf16[1,256,4096]{2,1,0:T(8,128)(2,1)}, u32[]{:S(2)}) copy-start(bf16[1,256,4096]{2,1,0:T(8,128)(2,1)} %param.42) | copy-start | bytes 6291460
  0.7 17.3 %copy-start.8 = (bf16[256,128]{1,0:T(8,128)(2,1)S(1)}, bf16[256,128]{1,0:T(8,128)(2,1)}, u32[]{:S(2)}) copy-start(bf16[256,128]{1,0:T(8,128)(2,1)} %param.31) | copy-start | bytes 196612
  0.7 17.5 %copy-start.9 = (bf16[256,128]{1,0:T(8,128)(2,1)S(1)}, bf16[256,128]{1,0:T(8,128)(2,1)}, u32[]{:S(2)}) copy-start(bf16[256,128]{1,0:T(8,128)(2,1)} %param.30) | copy-start | bytes 196612
  2.7 15.3 %all-to-all-start = ((bf16[16,32,256]{2,1,0:T(8,128)(2,1)}), bf16[16,32,256]{2,1,0:T(8,128)(2,1)S(1)}, u32[]{:S(2)}, u32[]{:S(2)}) async-start(bf16[16,32,256]{2,1,0:T(8,128)(2,1)} %copy.68), calls=%async_computation | async-start | bytes 524288 | tf_op jit(solution)/shard_map/all_to_all | solution.py:12
  14.9 20.7 %copy-start.16 = (f32[32]{0:T(128)}, f32[32]{0:T(128)S(1)}, u32[]{:S(2)}) copy-start(f32[32]{0:T(128)S(1)} %get-tuple-element.11) | copy-start | bytes 388
  14.9 28.7 %copy-start.20 = (s32[16]{0:T(128)}, s32[16]{0:T(128)S(1)}, u32[]{:S(2)}) copy-start(s32[16]{0:T(128)S(1)} %iota_multiply_fusion) | copy-start | bytes 196
  17.9 57.3 %copy-start.3 = (bf16[16,32,256]{2,1,0:T(8,128)(2,1)}, bf16[16,32,256]{2,1,0:T(8,128)(2,1)S(1)}, u32[]{:S(2)}) copy-start(bf16[16,32,256]{2,1,0:T(8,128)(2,1)S(1)} %all-to-all-done) | copy-start | bytes 786436
  20.0 14.6 %all-to-all-start.1 = ((bf16[16,32,512]{2,1,0:T(8,128)(2,1)}), bf16[16,32,512]{2,1,0:T(8,128)(2,1)S(1)}, u32[]{:S(2)}, u32[]{:S(2)}) async-start(bf16[16,32,512]{2,1,0:T(8,128)(2,1)} %bitcast.3), calls=%async_computation.1 | async-start | bytes 1048576 | tf_op jit(solution)/shard_map/all_to_all | solution.py:12
  24.5 26.2 %copy-start.12 = (bf16[128,256]{1,0:T(8,128)(2,1)S(1)}, bf16[128,256]{1,0:T(8,128)(2,1)}, u32[]{:S(2)}) copy-start(bf16[128,256]{1,0:T(8,128)(2,1)} %param.35) | copy-start | bytes 196612
  34.8 28.7 %copy-start.14 = (f32[4096]{0:T(1024)S(1)}, f32[4096]{0:T(1024)}, u32[]{:S(2)}) copy-start(f32[4096]{0:T(1024)} %param.36) | copy-start | bytes 49156
  35.6 28.4 %copy-start.6 = (f32[32,128]{1,0:T(8,128)}, f32[32,128]{1,0:T(8,128)S(1)}, u32[]{:S(2)}) copy-start(f32[32,128]{1,0:T(8,128)S(1)} %get-tuple-element.13) | copy-start | bytes 49156
  40.2 10.6 %all-to-all-start.2 = ((bf16[16,40,128]{2,1,0:T(8,128)(2,1)}), bf16[16,40,128]{2,1,0:T(8,128)(2,1)S(1)}, u32[]{:S(2)}, u32[]{:S(2)}) async-start(bf16[16,40,128]{2,1,0:T(8,128)(2,1)} %broadcast_in_dim.20), calls=%async_computation.2 | async-start | bytes 327680 | tf_op jit(solution)/shard_map/all_to_all | solution.py:12
  51.7 23.5 %all-to-all-start.3 = ((bf16[16,32,256]{2,1,0:T(8,128)(2,1)}), bf16[16,32,256]{2,1,0:T(8,128)(2,1)S(1)}, u32[]{:S(2)}, u32[]{:S(2)}) async-start(bf16[16,32,256]{2,1,0:T(8,128)(2,1)} %bitcast.14), calls=%async_computation.3 | async-start | bytes 524288 | tf_op jit(solution)/shard_map/all_to_all | solution.py:12
  76.0 14.6 %all-to-all-start.4 = ((bf16[16,32,256]{2,1,0:T(8,128)(2,1)}), bf16[16,32,256]{2,1,0:T(8,128)(2,1)S(1)}, u32[]{:S(2)}, u32[]{:S(2)}) async-start(bf16[16,32,256]{2,1,0:T(8,128)(2,1)} %broadcast_in_dim.24), calls=%async_computation.4 | async-start | bytes 524288 | tf_op jit(solution)/shard_map/all_to_all | solution.py:12
  92.4 18.6 %all-to-all-start.5 = ((bf16[16,96,256]{2,1,0:T(8,128)(2,1)}), bf16[16,96,256]{2,1,0:T(8,128)(2,1)S(1)}, u32[]{:S(2)}, u32[]{:S(2)}) async-start(bf16[16,96,256]{2,1,0:T(8,128)(2,1)} %bitcast.117), calls=%async_computation.5 | async-start | bytes 1572864 | tf_op jit(solution)/shard_map/all_to_all | solution.py:12
  111.0 22.0 %all-to-all-start.7 = ((bf16[16,32,1152]{2,1,0:T(8,128)(2,1)}), bf16[16,32,1152]{2,1,0:T(8,128)(2,1)}, u32[]{:S(2)}, u32[]{:S(2)}) async-start(bf16[16,32,1152]{2,1,0:T(8,128)(2,1)} %bitcast.106), calls=%async_computation.7 | async-start | bytes 2359296 | tf_op jit(solution)/shard_map/all_to_all | solution.py:12
  136.3 15.6 %all-to-all-start.8 = ((bf16[16,32,512]{2,1,0:T(8,128)(2,1)}), bf16[16,32,512]{2,1,0:T(8,128)(2,1)S(1)}, u32[]{:S(2)}, u32[]{:S(2)}) async-start(bf16[16,32,512]{2,1,0:T(8,128)(2,1)} %broadcast_in_dim.25), calls=%async_computation.8 | async-start | bytes 1048576 | tf_op jit(solution)/shard_map/all_to_all | solution.py:12
  152.6 19.6 %all-to-all-start.6 = ((bf16[16,6,4096]{2,1,0:T(8,128)(2,1)}), bf16[16,6,4096]{2,1,0:T(8,128)(2,1)S(1)}, u32[]{:S(2)}, u32[]{:S(2)}) async-start(bf16[16,6,4096]{2,1,0:T(8,128)(2,1)} %reshape.382), calls=%async_computation.6 | async-start | bytes 2097152 | tf_op jit(solution)/shard_map/all_to_all | solution.py:12
  172.2 12.5 %all-to-all-start.9 = ((bf16[16,32,256]{2,1,0:T(8,128)(2,1)}), bf16[16,32,256]{2,1,0:T(8,128)(2,1)S(1)}, u32[]{:S(2)}, u32[]{:S(2)}) async-start(bf16[16,32,256]{2,1,0:T(8,128)(2,1)} %bitcast.115), calls=%async_computation.9 | async-start | bytes 524288 | tf_op jit(solution)/shard_map/all_to_all | solution.py:12
  184.8 28.8 %copy-start.7 = (f32[32,128]{1,0:T(8,128)S(1)}, f32[32,128]{1,0:T(8,128)}, u32[]{:S(2)}) copy-start(f32[32,128]{1,0:T(8,128)} %copy-done.6) | copy-start | bytes 49156
  184.8 28.8 %copy-start.17 = (f32[32]{0:T(128)S(1)}, f32[32]{0:T(128)}, u32[]{:S(2)}) copy-start(f32[32]{0:T(128)} %copy-done.16) | copy-start | bytes 388
  186.0 18.3 %all-to-all-start.10 = ((bf16[16,32,256]{2,1,0:T(8,128)(2,1)}), bf16[16,32,256]{2,1,0:T(8,128)(2,1)S(1)}, u32[]{:S(2)}, u32[]{:S(2)}) async-start(bf16[16,32,256]{2,1,0:T(8,128)(2,1)} %bitcast.103), calls=%async_computation.10 | async-start | bytes 524288 | tf_op jit(solution)/shard_map/all_to_all | solution.py:12
  193.0 11.4 %collective-permute-start = (bf16[32,256]{1,0:T(8,128)(2,1)S(1)}, bf16[32,256]{1,0:T(8,128)(2,1)S(1)}, u32[]{:S(2)}, u32[]{:S(2)}) collective-permute-start(bf16[32,256]{1,0:T(8,128)(2,1)S(1)} %fusion.52), channel_id=1, source_target_pairs={{0,0},{1,16},{2,32},{3,48},{4,64},{5,80},{6,96},{7,112},{8,128},{9... | collective-permute-start | bytes 49160 | tf_op jit(solution)/shard_map/ppermute | solution.py:110
  205.1 20.0 %all-to-all-start.11 = ((bf16[16,32,256]{2,1,0:T(8,128)(2,1)}), bf16[16,32,256]{2,1,0:T(8,128)(2,1)S(1)}, u32[]{:S(2)}, u32[]{:S(2)}) async-start(bf16[16,32,256]{2,1,0:T(8,128)(2,1)} %broadcast_in_dim.26), calls=%async_computation.11 | async-start | bytes 524288 | tf_op jit(solution)/shard_map/all_to_all | solution.py:12
  (17 other events, 198.9 us)

commit v2 on v1

v2 whole, which is shorter than its diff:
```python
import jax
import jax.numpy as jnp
from jax import lax
from jax.experimental import pallas as pl
from jax.experimental.pallas import tpu as pltpu
from jax.sharding import PartitionSpec as P

EPS = 1e-06
BF = jnp.bfloat16
F32 = jnp.float32
I32 = jnp.int32
EP, TP = 16, 16
ROWS, WIDTH, COLS, HEAD, UNITS, CAP = 32, 4096, 256, 128, 512, 6
ALL = ROWS * EP
ROUTED = 2 * CAP * EP
SIDE = ROUTED + 8 * ROWS
PACKED = SIDE + 16
CHUNKS = WIDTH // 128
BACK = CAP * CHUNKS
RETURN = BACK + 2 * ROWS
def in_hbm(x):
    return pltpu.with_memory_space_constraint(x, pltpu.HBM)


def grant(mib):
    return pltpu.CompilerParams(vmem_limit_bytes=mib * 1024 * 1024)


VMEM = pl.BlockSpec(memory_space=pltpu.VMEM)
SMEM = pl.BlockSpec(memory_space=pltpu.SMEM)
HBM = pl.BlockSpec(memory_space=pltpu.HBM)


def swap(parts, axis):
    return lax.all_to_all(parts, axis, 0, 0, tiled=True)


def copies(shard, axis):
    return swap(jnp.broadcast_to(shard[None], (lax.axis_size(axis), *shard.shape)), axis)


def mm(a, b):
    return jnp.dot(a, b, preferred_element_type=F32)


def mm_nt(a, b):
    return lax.dot_general(a, b, (((1,), (1,)), ((), ())), preferred_element_type=F32)


def cut_kernel(x_ref, o_ref, done):
    moves = [
        pltpu.make_async_copy(x_ref.at[:, pl.ds(e * COLS, COLS)], o_ref.at[e], done.at[e]) for e in range(EP)
    ]
    for move in moves:
        move.start()
    for move in moves:
        move.wait()


def cut(tokens):
    return pl.pallas_call(
        cut_kernel,
        out_shape=jax.ShapeDtypeStruct((EP, ROWS, COLS), BF),
        in_specs=[HBM],
        out_specs=VMEM,
        scratch_shapes=[pltpu.SemaphoreType.DMA((EP,))],
        compiler_params=grant(1),
    )(in_hbm(tokens))


def prepare_kernel(
    me_ref, *refs,
):
    sources, outs, scratch = refs[:10], refs[10:17], refs[17:27]
    done = refs[27]
    moves = [pltpu.make_async_copy(a, b, done.at[i]) for i, (a, b) in enumerate(zip(sources, scratch))]
    for move in moves:
        move.start()
    x_ref, gain_ref, in_ref, forget_ref, bias_ref, max_ref, norm_ref, route_ref, weight_ref, state_ref = scratch
    scale_ref, write_ref, new_max_ref, extra_ref, table_ref, old_norm_ref, old_ref = outs
    for move in moves[:-1]:
        move.wait()
    wide = x_ref[...].astype(F32)
    scale = lax.rsqrt(jnp.sum(wide * wide, axis=1, keepdims=True) / WIDTH + EPS)
    scale_ref[...] = jnp.broadcast_to(scale, (ROWS, HEAD))
    normed = (wide * scale * gain_ref[...]).astype(BF)
    head = lax.broadcasted_iota(I32, (ROWS, TP), 1) == me_ref[1]
    pick = lambda x: jnp.sum(jnp.where(head, x, 0.0), axis=1, keepdims=True)
    row = lax.broadcasted_iota(I32, (ROWS, ROWS), 0)
    lane = lax.broadcasted_iota(I32, (ROWS, ROWS), 1)
    upright = lambda x: jnp.sum(jnp.where(lane == row, x, jnp.zeros_like(x)), axis=1, keepdims=True)
    flat = lambda x: jnp.sum(jnp.where(lane == row, x, jnp.zeros_like(x)), axis=0, keepdims=True)
    gate_in = pick(mm_nt(normed, in_ref[...]))
    gate_forget = pick(mm_nt(normed, forget_ref[...]) + bias_ref[...])
    old_max = upright(max_ref[...])
    log_keep = jnp.minimum(gate_forget, 0.0) - jnp.log1p(jnp.exp(-jnp.abs(gate_forget)))
    new_max = jnp.maximum(log_keep + old_max, gate_in)
    new_max_ref[...] = flat(new_max)
    keep = jnp.broadcast_to(jnp.exp(log_keep + old_max - new_max), (ROWS, HEAD))
    write_ref[...] = jnp.broadcast_to(jnp.exp(gate_in - new_max), (ROWS, HEAD))
    old_norm_ref[...] = keep * norm_ref[...].reshape(ROWS, HEAD)

    place = lax.broadcasted_iota(I32, (ROWS, 128), 1) == (me_ref[0] % 4) * ROWS + lax.broadcasted_iota(
        I32, (ROWS, 128), 0
    )
    across = [route_ref[k : k + 1, :] for k in range(2)]
    column = [upright(x) for x in across]
    lines = []
    for k in range(2):
        same = (across[0] == column[k]).astype(I32) + (across[1] == column[k]).astype(I32)
        slot = jnp.sum(jnp.where(lane < row, same, 0), axis=1, keepdims=True)
        code = column[k] * 8 + slot
        table_ref[k : k + 1, :] = flat(code).astype(F32)
        lines.append(jnp.sum(jnp.where(place, code, 0), axis=0, keepdims=True))
    lines.append(jnp.zeros((6, 128), I32))
    extra_ref[...] = jnp.concatenate(lines, axis=0).astype(F32).astype(BF)
    weight = weight_ref[...]
    table_ref[2:4, :] = weight / jnp.sum(weight, axis=0, keepdims=True)
    moves[-1].wait()
    for r in range(ROWS):
        old_ref[r] = keep[r : r + 1] * state_ref[r, 0]


def prepare(me, *sources):
    wide = jax.ShapeDtypeStruct((ROWS, HEAD), F32)
    return pl.pallas_call(
        prepare_kernel,
        out_shape=(
            wide, wide, jax.ShapeDtypeStruct((1, ROWS), F32), jax.ShapeDtypeStruct((8, HEAD), BF),
            jax.ShapeDtypeStruct((4, ROWS), F32), wide, jax.ShapeDtypeStruct((ROWS, HEAD, HEAD), F32),
        ),
        in_specs=[SMEM] + [HBM] * 10,
        out_specs=(VMEM,) * 7,
        scratch_shapes=[pltpu.VMEM(x.shape, x.dtype) for x in sources] + [pltpu.SemaphoreType.DMA((10,))],
        compiler_params=grant(12),
    )(me, *[in_hbm(x) for x in sources])


def my_columns(ref, me_ref):
    return ref[:, pl.ds(pl.multiple_of(me_ref[0] * COLS, COLS), COLS)]


def heads_kernel(me_ref, x_ref, gain_ref, q_ref, k_ref, v_ref, g_ref, o_ref, mine_ref):
    x = (x_ref[...].reshape(ALL, COLS).astype(F32) * my_columns(gain_ref, me_ref)).astype(BF)
    for i, w in enumerate((q_ref, k_ref, v_ref, g_ref)):
        o_ref[:, :, i * HEAD : (i + 1) * HEAD] = mm(x, w[...]).astype(BF).reshape(EP, ROWS, HEAD)
    mine_ref[...] = x_ref[me_ref[1]]


def heads(me, token_cols, gain, ws):
    return pl.pallas_call(
        heads_kernel,
        out_shape=(
            jax.ShapeDtypeStruct((EP, ROWS, 4 * HEAD), BF),
            jax.ShapeDtypeStruct((ROWS, COLS), BF),
        ),
        in_specs=[SMEM] + [VMEM] * 6,
        out_specs=(VMEM, VMEM),
        compiler_params=grant(6),
    )(me, token_cols, gain, *ws)


STEP = 8


def cell_kernel(
    p_ref, scale_ref, write_ref, extra_ref, norm_ref, old_ref,
    mixed_ref, new_norm_ref, new_ref, proj, numer, gated,
):
    step = pl.program_id(0)

    @pl.when(step == 0)
    def _():
        for i in range(4):
            lanes = slice(i * HEAD, (i + 1) * HEAD)
            total = p_ref[0, :, lanes].astype(F32)
            for e in range(1, EP):
                total = total + p_ref[e, :, lanes].astype(F32)
            proj[i] = total * scale_ref[...]

    here = pl.ds(pl.multiple_of(step * STEP, STEP), STEP)
    query, key, value, outgate = (proj[i, here, :] for i in range(4))
    write = write_ref[here, :]
    key = key * HEAD ** (-0.5)
    wkey = write * key
    new_norm = norm_ref[here, :] + wkey
    new_norm_ref[here, :] = new_norm
    query_t, wkey_t = query.T, wkey.T
    for j in range(STEP):
        row = slice(j, j + 1)
        new = old_ref[step * STEP + j] + wkey_t[:, row] * value[row]
        new_ref[j, 0] = new
        numer[row, :] = jnp.sum(query_t[:, row] * new, axis=0, keepdims=True)
    denom = jnp.sum(query * new_norm, axis=1, keepdims=True)
    out = numer[...] / jnp.maximum(jnp.abs(denom), 1.0)
    gated[here, :] = jax.nn.sigmoid(outgate) * out

    @pl.when(step == ROWS // STEP - 1)
    def _():
        mixed = gated[...].astype(BF)
        extra = extra_ref[...]
        for e in range(EP):
            mixed_ref[e, :ROWS] = mixed
            mixed_ref[e, ROWS:] = extra


def cell(parts, scale, write, extra, norm, old):
    whole = lambda *shape: pl.BlockSpec(shape, lambda i: (0,) * len(shape))
    return pl.pallas_call(
        cell_kernel,
        grid=(ROWS // STEP,),
        out_shape=(
            jax.ShapeDtypeStruct((EP, ROWS + 8, HEAD), BF),
            jax.ShapeDtypeStruct((ROWS, HEAD), F32),
            jax.ShapeDtypeStruct((ROWS, 1, HEAD, HEAD), F32),
        ),
        in_specs=[VMEM] * 6,
        out_specs=(
            whole(EP, ROWS + 8, HEAD), whole(ROWS, HEAD),
            pl.BlockSpec((STEP, 1, HEAD, HEAD), lambda i: (i, 0, 0, 0)),
        ),
        scratch_shapes=[
            pltpu.VMEM((4, ROWS, HEAD), F32),
            pltpu.VMEM((STEP, HEAD), F32),
            pltpu.VMEM((ROWS, HEAD), F32),
        ],
        compiler_params=grant(6),
    )(parts, scale, write, extra, norm, old)


def settle_kernel(p_ref, base_ref, o_ref):
    total = p_ref[0].astype(F32)
    for t in range(1, TP):
        total = total + p_ref[t].astype(F32)
    out = (base_ref[...].astype(F32) + total).astype(BF)
    for t in range(TP):
        o_ref[t] = out


def settle(parts, base):
    return pl.pallas_call(
        settle_kernel,
        out_shape=jax.ShapeDtypeStruct(parts.shape, BF),
        in_specs=[VMEM, VMEM],
        out_specs=VMEM,
        compiler_params=grant(4),
    )(parts, base)


def high_low(x):
    high = x.astype(BF).astype(F32)
    return high, x - high


def feed_kernel(t_ref, r_ref, gain_ref, branch_ref, mix_ref, gate_ref, up_ref, o_ref):
    resid = r_ref[...].reshape(ALL, COLS)
    wide = resid.astype(F32)
    gained = (wide * my_columns(gain_ref, t_ref)).astype(BF)
    for half, w in enumerate((gate_ref, up_ref)):
        for j in range(4):
            part = mm(gained, w[:, j * 128 : (j + 1) * 128]).astype(BF).reshape(EP, ROWS, 128)
            at = ROUTED + (half * 4 + j) * ROWS
            o_ref[:, at : at + ROWS, :] = part
    square_high, square_low = high_low(wide * wide)
    ones = jnp.ones((8, COLS), BF)
    squares = mm_nt(ones, square_high.astype(BF)) + mm_nt(ones, square_low.astype(BF))
    branch = mm_nt(jnp.broadcast_to(my_columns(branch_ref, t_ref), (8, COLS)), gained)
    sq_high, sq_low = high_low(squares)
    br_high, br_low = high_low(branch)
    line = lax.broadcasted_iota(I32, (8, ALL), 0)
    side = jnp.where(line == 0, sq_high, jnp.where(line == 1, sq_low, jnp.where(line == 2, br_high, br_low)))
    me = t_ref[1]
    at = lax.broadcasted_iota(I32, (8 * EP, ALL), 0)
    token = lax.broadcasted_iota(I32, (8 * EP, ALL), 1)
    quarter = at % 8
    mine = (token == (at // 8) * ROWS + 2 * me + quarter // 2) & (quarter < 4)
    own = mm((mine & (quarter % 2 == 0)).astype(F32).astype(BF), resid[:, :128])
    own = own + mm((mine & (quarter % 2 == 1)).astype(F32).astype(BF), resid[:, 128:])
    for g in range(EP):
        tile = g // 4
        block = jnp.concatenate(
            [side[:, tile * 128 : (tile + 1) * 128], own[g * 8 : (g + 1) * 8]], axis=0
        )
        o_ref[g, SIDE:PACKED, :] = block.astype(BF)
    half_rows = CAP * EP // 2
    line = lax.broadcasted_iota(I32, (half_rows, 2 * 128), 0)
    base = (line // CAP) * 128 + line % CAP
    group = lax.broadcasted_iota(I32, (1, 2 * 128), 1) // ROWS
    for half in range(2):
        tiles = []
        for tile in (2 * half, 2 * half + 1):
            tiles.append(sum(mix_ref[4 * tile + i, ROWS:, :].astype(F32) for i in range(4)))
        codes = jnp.concatenate(tiles, axis=1).astype(I32)
        first = codes[0:1] + group * 128 - base
        second = codes[1:2] + group * 128 - base
        source = resid[half * 256 : (half + 1) * 256]
        for x in range(EP):
            member = (first == x * 8) | (second == x * 8)
            picked = mm(jnp.where(member, 1.0, 0.0).astype(BF), source).astype(BF)
            for h in range(2):
                at = h * CAP * EP + half * half_rows
                o_ref[x, at : at + half_rows, :] = picked[:, h * 128 : (h + 1) * 128]


def feed(me, resid, gain, branch, mix, gate, up):
    return pl.pallas_call(
        feed_kernel,
        out_shape=jax.ShapeDtypeStruct((EP, PACKED, 128), BF),
        in_specs=[SMEM] + [VMEM] * 6,
        out_specs=VMEM,
        compiler_params=grant(14),
    )(me, resid, gain, branch, mix, gate, up)


def hidden_kernel(e_ref, p_ref, o_ref, b_ref, kept_ref, kept):
    def total(at, size):
        value = p_ref[0, at : at + size, :].astype(F32)
        for e in range(1, EP):
            value = value + p_ref[e, at : at + size, :].astype(F32)
        return value

    side = total(SIDE, 16)
    lane = lax.broadcasted_iota(I32, (ROWS, 128), 1)
    row = lax.broadcasted_iota(I32, (ROWS, 128), 0)
    mine = lane == (e_ref[0] % 4) * ROWS + row
    squares = jnp.sum(jnp.where(mine, side[0:1] + side[1:2], 0.0), axis=1, keepdims=True)
    branch = jnp.sum(jnp.where(mine, side[2:3] + side[3:4], 0.0), axis=1, keepdims=True)
    scale = lax.rsqrt(squares / WIDTH + EPS)
    for e in range(EP):
        rows = p_ref[e, SIDE:PACKED, :].astype(F32)
        for r in range(2):
            at = r * CHUNKS + 2 * e
            kept[at : at + 2, :] = rows[8 + 2 * r : 10 + 2 * r]
    kept_ref[...] = kept[...].astype(BF)
    b_ref[...] = jnp.broadcast_to(jax.nn.sigmoid(branch * scale), (ROWS, 128))
    for j in range(4):
        gate = total(ROUTED + j * ROWS, ROWS) * scale
        up = total(ROUTED + (4 + j) * ROWS, ROWS) * scale
        value = (gate * jax.nn.sigmoid(gate) * up).astype(BF)
        for e in range(EP):
            o_ref[e, :, j * 128 : (j + 1) * 128] = value


def hidden_units(me, packed):
    return pl.pallas_call(
        hidden_kernel,
        out_shape=(
            jax.ShapeDtypeStruct((EP, ROWS, UNITS), BF),
            jax.ShapeDtypeStruct((ROWS, 128), F32),
            jax.ShapeDtypeStruct((2 * CHUNKS, 128), BF),
        ),
        in_specs=[SMEM, VMEM],
        out_specs=(VMEM,) * 3,
        scratch_shapes=[pltpu.VMEM((2 * CHUNKS, 128), F32)],
        compiler_params=grant(8),
    )(me, packed)


K_STEPS, N_STEPS = 8, 8
PER_STEP = EP // K_STEPS
DEEP = WIDTH // K_STEPS
LANES = WIDTH // N_STEPS


def expert_kernel(
    x_ref, gain_ref, gate_hbm, up_hbm, down_hbm, dense_hbm, o_ref, dense_ref, gate_ref, up_ref, down_ref, turned, done,
):
    slots = CAP * EP
    gates, ups, downs = [], [], []
    for i in range(K_STEPS):
        part = pl.ds(i * DEEP, DEEP)
        gates.append(pltpu.make_async_copy(gate_hbm.at[0, part, :], gate_ref.at[part, :], done.at[0, i]))
        ups.append(pltpu.make_async_copy(up_hbm.at[0, part, :], up_ref.at[part, :], done.at[1, i]))
    for i in range(N_STEPS):
        part = pl.ds(i * LANES, LANES)
        downs.append(pltpu.make_async_copy(down_hbm.at[0, :, part], down_ref.at[:, part], done.at[2, i]))
    dense = pltpu.make_async_copy(dense_hbm, dense_ref, done.at[3, 0])
    for i in range(K_STEPS):
        gates[i].start()
        ups[i].start()
    for move in downs:
        move.start()
    dense.start()
    squares = jnp.zeros((slots, 128), F32)
    gate = jnp.zeros((slots, COLS), F32)
    up = jnp.zeros((slots, COLS), F32)
    for i in range(K_STEPS):
        pieces = []
        for e in range(i * PER_STEP, (i + 1) * PER_STEP):
            for h in range(2):
                x = x_ref[e, h * slots : (h + 1) * slots, :].astype(F32)
                squares += x * x
                at = (2 * e + h) * 128
                pieces.append((x * gain_ref[:, at : at + 128]).astype(BF))
        x = jnp.concatenate(pieces, axis=1)
        gates[i].wait()
        ups[i].wait()
        gate += mm(x, gate_ref[i * DEEP : (i + 1) * DEEP, :])
        up += mm(x, up_ref[i * DEEP : (i + 1) * DEEP, :])
    scale = lax.rsqrt(jnp.sum(squares, axis=1, keepdims=True) / WIDTH + EPS)
    gate = gate * scale
    hidden = (gate * jax.nn.sigmoid(gate) * (up * scale)).astype(BF)
    for i in range(N_STEPS):
        downs[i].wait()
        out = mm(hidden, down_ref[:, i * LANES : (i + 1) * LANES])
        for c in range(LANES // 128):
            turned[pl.ds(i * (LANES // 128) + c, slots, stride=CHUNKS), :] = out[:, c * 128 : (c + 1) * 128]
    for g in range(EP):
        o_ref[g, :BACK, :] = turned[g * BACK : (g + 1) * BACK, :].astype(BF)
    dense.wait()


def expert(packed, gain, gate, up, down_w, dense_w):
    return pl.pallas_call(
        expert_kernel,
        out_shape=(
            jax.ShapeDtypeStruct((EP, RETURN, 128), BF),
            jax.ShapeDtypeStruct(dense_w.shape, BF),
        ),
        in_specs=[VMEM, VMEM, HBM, HBM, HBM, HBM],
        out_specs=(VMEM, VMEM),
        scratch_shapes=[
            pltpu.VMEM((WIDTH, COLS), BF),
            pltpu.VMEM((WIDTH, COLS), BF),
            pltpu.VMEM((COLS, WIDTH), BF),
            pltpu.VMEM((CAP * EP * CHUNKS, 128), F32),
            pltpu.SemaphoreType.DMA((4, 8)),
        ],
        compiler_params=grant(14),
    )(packed, gain, in_hbm(gate), in_hbm(up), in_hbm(down_w), in_hbm(dense_w))


def down_kernel(h_ref, w_ref, _, o_ref):
    out = mm(h_ref[...].reshape(ALL, UNITS), w_ref[...]).astype(BF)
    for h in range(2):
        o_ref[:, h * ROWS : (h + 1) * ROWS, :] = out[:, h * 128 : (h + 1) * 128].reshape(EP, ROWS, 128)


def down(hidden, w, buffer):
    whole = lambda *shape: pl.BlockSpec(shape, lambda i: (0,) * len(shape))
    return pl.pallas_call(
        down_kernel,
        grid=(1,),
        out_shape=jax.ShapeDtypeStruct((EP, RETURN, 128), BF),
        in_specs=[whole(EP, ROWS, UNITS), whole(UNITS, COLS), pl.BlockSpec(memory_space=pl.ANY)],
        out_specs=pl.BlockSpec((EP, 2 * ROWS, 128), lambda i: (0, BACK // (2 * ROWS), 0)),
        input_output_aliases={2: 0},
        compiler_params=grant(6),
    )(hidden, w, buffer)


def gather_kernel(table_ref, branch_ref, r_ref, o_ref, dense):
    for c in range(CHUNKS):
        at = BACK + (c % 2) * ROWS
        dense[c * ROWS : (c + 1) * ROWS, :] = r_ref[c // 2, at : at + ROWS, :].astype(F32)
    for r in range(ROWS):
        total = branch_ref[r : r + 1, :] * dense[pl.ds(r, CHUNKS, stride=ROWS), :]
        for k in range(2):
            code = table_ref[k, r].astype(I32)
            at = pl.multiple_of((code % 8) * CHUNKS, CHUNKS)
            total = total + table_ref[2 + k, r] * r_ref[code // 8, pl.ds(at, CHUNKS), :].astype(F32)
        o_ref[r // 2, (r % 2) * CHUNKS : (r % 2 + 1) * CHUNKS, :] = total.astype(BF)


def gather(table, branch, returned):
    return pl.pallas_call(
        gather_kernel,
        out_shape=jax.ShapeDtypeStruct((TP, 2 * CHUNKS, 128), BF),
        in_specs=[SMEM, VMEM, VMEM],
        out_specs=VMEM,
        scratch_shapes=[pltpu.VMEM((CHUNKS * ROWS, 128), F32)],
        compiler_params=grant(6),
    )(table, branch, returned)


def on_device(
    tokens,
    state_matrix,
    state_norm,
    state_max,
    mixer_gain,
    w_query,
    w_key,
    w_value,
    w_outgate,
    w_ingate,
    w_forget,
    forget_bias,
    w_proj,
    ffn_gain,
    w_branch,
    routes,
    route_weight,
    expert_gate,
    expert_up,
    expert_down,
    dense_gate,
    dense_up,
    dense_down,
):
    me = jnp.stack([lax.axis_index("ep"), lax.axis_index("tp")]).astype(I32)
    token_cols = swap(cut(tokens), "ep")
    own = prepare(
        me, tokens, mixer_gain[None], w_ingate.T, w_forget.T, forget_bias[None], state_max.T, state_norm,
        routes.T, route_weight.T, state_matrix,
    )
    gains = (mixer_gain[None], ffn_gain[None], w_branch[None])
    scale, write, new_max, extra, table, norm, old = own
    (token_cols, scale, write, extra, norm, old, gains, me) = lax.optimization_barrier(
        (token_cols, scale, write, extra, norm, old, gains, me)
    )
    partial, token_block = heads(me, token_cols, gains[0], (w_query, w_key, w_value, w_outgate))
    parts = swap(partial, "ep")
    mixed, new_norm, new_matrix = cell(parts, scale, write, extra, norm, old)
    mixed_all = swap(mixed, "ep")

    spread_out = mm(mixed_all[:, :ROWS].reshape(ALL, HEAD), w_proj).astype(BF).reshape(TP, ROWS, COLS)
    resid = swap(settle(swap(spread_out, "tp"), token_block), "tp")

    arrived = swap(feed(me, resid, gains[1], gains[2], mixed_all, dense_gate, dense_up), "ep")
    hidden, branch, kept = hidden_units(me, arrived)
    hidden_all = swap(hidden, "ep")

    _, arrived = lax.optimization_barrier((hidden, arrived))
    buffer, down_w = expert(arrived, gains[1], expert_gate, expert_up, expert_down, dense_down)
    hidden_all, buffer, down_w, branch, kept, new_max, new_norm, table = lax.optimization_barrier(
        (hidden_all, buffer, down_w, branch, kept, new_max, new_norm, table)
    )

    returned = swap(down(hidden_all, down_w, buffer), "ep")
    parts = swap(gather(table, branch, returned), "tp")
    layer_out = swap(settle(parts, kept), "tp").reshape(ROWS, WIDTH)
    new_max = new_max.T
    return (layer_out, new_matrix, new_norm[:, None], new_max)


def solution(mesh):
    in_specs = (
        P("ep", None),
        P("ep", "tp", None, None),
        P("ep", "tp", None),
        P("ep", "tp"),
        P(),
        P("ep", "tp"),
        P("ep", "tp"),
        P("ep", "tp"),
        P("ep", "tp"),
        P(),
        P(),
        P(),
        P("tp", "ep"),
        P(),
        P(),
        P("ep", None),
        P("ep", None),
        P("ep", None, "tp"),
        P("ep", None, "tp"),
        P("ep", "tp", None),
        P("ep", "tp"),
        P("ep", "tp"),
        P("tp", "ep"),
    )
    out_specs = (P("ep", None), P("ep", "tp", None, None), P("ep", "tp", None), P("ep", "tp"))
    return jax.shard_map(
        on_device, mesh=mesh, in_specs=in_specs, out_specs=out_specs, check_vma=False
    )
```

time: 227 us -> 185 us (0.81)
  blocking collectives: 0 us -> 140 us
  waiting for transfers between devices: 106 us -> 8.6 us
  starting transfers between devices: 70.1 us -> 11.2 us
  Pallas kernels: 0 us -> 19.4 us
  matrix products: 18.6 us -> 0.21 us
  other arithmetic: 14.1 us -> 0.08 us
  local copies, waits for them, and re-layouts: 16.1 us -> 3.84 us
    all_to_all x0 -> x8, blocking collectives: none -> 140 us  [swap(): return lax.all_to_all(parts, axis, 0, 0, tiled=True)]
    all_to_all x12 -> x2, waiting for transfers between devices: 106 us -> 8.6 us  [swap(): return lax.all_to_all(parts, axis, 0, 0, tiled=True)]
    all_to_all x12 -> x2, starting transfers between devices: 67.8 us -> 11.2 us  [swap(): return lax.all_to_all(parts, axis, 0, 0, tiled=True)]
    pallas_call x0 -> x11, Pallas kernels: none -> 19.4 us  [the longest x1 4.91 us: expert(): pl.pallas_call(expert_kernel, out_shape=(jax.ShapeDtypeStruct((EP, RETURN...]
    dot_general x15 -> x1, matrix products: 18.6 us -> 0.21 us  [mm(): return jnp.dot(a, b, preferred_element_type=F32)]
    reduce_sum x11 -> x0, other arithmetic: 4.25 us -> none  [the longest x1 1.45 us: on_device(): summed = swap(gate_up.reshape(n_ep, rows, -1), 'ep').astype(F32).sum(0)]
    reshape x4 -> x1, local copies, waits for them, and re-layouts: 4.85 us -> 0.82 us  [on_device(): layer_out = swap(settle(parts, kept), 'tp').reshape(ROWS, WIDTH)]
    concatenate x2 -> x0, local copies, waits for them, and re-layouts: 3.38 us -> none  [the longest x1 2.38 us: on_device(): jnp.concatenate([dot(gained, dense_gate).astype(BF), dot(gained, dense_up...]
  transfers between devices with their start and end apart: 13 -> 2, of which waited for: 12 -> 2; matrix products, arithmetic and copies ran while one was open for 13% -> 0% of each run, Pallas kernels for 0% -> 4%
where the time goes in v2:
time: 185 us; the launch traced here: 184 us
  blocking collectives  140 us (76%)
  Pallas kernels  19.4 us (10%)
  starting transfers between devices  11.2 us (6%)
  waiting for transfers between devices  8.6 us (5%)
  local copies, waits for them, and re-layouts  3.84 us (2%)
    all_to_all x8, blocking collectives, swap(): return lax.all_to_all(parts, axis, 0, 0, tiled=True)  140 us
    all_to_all x2, starting transfers between devices, swap(): return lax.all_to_all(parts, axis, 0, 0, tiled=True)  11.2 us
    all_to_all x2, waiting for transfers between devices, swap(): return lax.all_to_all(parts, axis, 0, 0, tiled=True)  8.6 us
    pallas_call x1, Pallas kernels, expert(): pl.pallas_call(expert_kernel, out_shape=(jax.ShapeDtypeStruct((EP, RETURN...  4.91 us
  transfers between devices with their start and end apart: 2, of which 2 were waited for; matrix products, arithmetic and copies ran while one was open for 0% of the time, Pallas kernels for 4%

profile of v2, /device:TPU:1, one launch (start us, length us, event | category | flops | bytes accessed | tf_op | source)
XLA Modules:
  0.0 183.9 jit_solution(1780347854966037765)
XLA Ops:
  0.7 1.8 shard_map.246
  2.5 7.6 %all-to-all-start = ((bf16[16,32,256]{2,1,0:T(8,128)(2,1)}), bf16[16,32,256]{2,1,0:T(8,128)(2,1)S(1)}, u32[]{:S(2)}, u32[]{:S(2)}) async-start(bf16[16,32,256]{2,1,0:T(8,128)(2,1)} %shard_map.246), calls=%async_computation | async-start | bytes 524288 | tf_op jit(solution)/shard_map/all_to_all | solution.py:35
  10.1 0.7 broadcast_in_dim.19.branch_ref
  10.9 3.0 %shard_map.247 = (f32[32,128]{1,0:T(8,128)S(1)}, f32[32,128]{1,0:T(8,128)S(1)}, f32[1,32]{1,0:T(1,128)}, bf16[8,128]{1,0:T(8,128)(2,1)S(1)}, f32[4,32]{1,0:T(4,1...) custom-call(s32[2]{0:T(128)S(1)} %pad_add_fusion.me_ref.t_ref.e_ref, bf16[32,4096]{1,0:T(8,128)(2,1)} %refs_0_.1, ...), custom_call_target="tpu_custom_call" | custom-call | tf_op jit(solution)/shard_map/pallas_call | solution.py:126
  13.9 3.7 %all-to-all-done.x_ref = bf16[16,32,256]{2,1,0:T(8,128)(2,1)S(1)} async-done(((bf16[16,32,256]{2,1,0:T(8,128)(2,1)}), bf16[16,32,256]{2,1,0:T(8,128)(2,1)S(1)}, u32[]{:S(2)}, u32[]{:S(2)}) %all-to-all-start) | async-done | bytes 262176 | tf_op jit(solution)/shard_map/all_to_all | solution.py:35
  17.7 1.0 shard_map.248
  18.6 13.4 %all_to_all.50.p_ref = bf16[16,32,512]{2,1,0:T(8,128)(2,1)S(1)} all-to-all(bf16[16,32,512]{2,1,0:T(8,128)(2,1)S(1)} %get-tuple-element.48), channel_id=1, replica_groups=mesh['ep'=16,'tp'=16] {'ep'}, dimensions={0} | all-to-all | bytes 1048576 | tf_op jit(solution)/shard_map/all_to_all | solution.py:35
  32.1 3.3 %shard_map.249 = (bf16[16,40,128]{2,1,0:T(8,128)(2,1)S(1)}, f32[32,128]{1,0:T(8,128)}, f32[32,1,128,128]{3,2,1,0:T(8,128)}) custom-call(bf16[16,32,512]{2,1,0:T(8,128)(2,1)S(1)} %all_to_all.50.p_ref, f32[32,128]{1,0:T(8,128)S(1)} %get-tuple-element.49.scale_ref, f32[32,128]{1,0:T(8,128)S(1)} %get-tuple-element.50.write_ref, ...), custom_call_target="tpu_custom_call" | custom-call | tf_op jit(solution)/shard_map/pallas_call | solution.py:209
  35.4 10.2 %all_to_all.51.mix_ref = bf16[16,40,128]{2,1,0:T(8,128)(2,1)S(1)} all-to-all(bf16[16,40,128]{2,1,0:T(8,128)(2,1)S(1)} %get-tuple-element.54), channel_id=1, replica_groups=mesh['ep'=16,'tp'=16] {'ep'}, dimensions={0} | all-to-all | bytes 327680 | tf_op jit(solution)/shard_map/all_to_all | solution.py:35
  45.8 23.2 %all_to_all.52.p_ref = bf16[16,32,256]{2,1,0:T(8,128)(2,1)S(1)} all-to-all(bf16[16,32,256]{2,1,0:T(8,128)(2,1)S(1)} %bitcast.22), channel_id=1, replica_groups=mesh['ep'=16,'tp'=16] {'tp'}, dimensions={0} | all-to-all | bytes 524288 | tf_op jit(solution)/shard_map/all_to_all | solution.py:35
  69.0 14.4 %all_to_all.53.r_ref = bf16[16,32,256]{2,1,0:T(8,128)(2,1)S(1)} all-to-all(bf16[16,32,256]{2,1,0:T(8,128)(2,1)S(1)} %shard_map.250), channel_id=1, replica_groups=mesh['ep'=16,'tp'=16] {'tp'}, dimensions={0} | all-to-all | bytes 524288 | tf_op jit(solution)/shard_map/all_to_all | solution.py:35
  83.4 2.2 %shard_map.251 = bf16[16,464,128]{2,1,0:T(8,128)(2,1)S(1)} custom-call(s32[2]{0:T(128)S(1)} %pad_add_fusion.me_ref.t_ref.e_ref, bf16[16,32,256]{2,1,0:T(8,128)(2,1)S(1)} %all_to_all.53.r_ref, f32[1,4096]{1,0:T(1,128)S(1)} %bitcast.18, bf16[1,4096]{1,0:T(2,128)(2,1)S(1)} %broadcast_in_dim.19.branch_ref, bf16[16,40,128]{2,1,0:T(8,128)(2,1)S(1)} %all_to_all.51.mix_ref, ...), custom_call_target="tpu_custom_call" | custom-call | tf_op jit(solution)/shard_map/pallas_call | solution.py:306
  85.6 29.0 %all_to_all.54.p_ref.x_ref = bf16[16,464,128]{2,1,0:T(8,128)(2,1)S(1)} all-to-all(bf16[16,464,128]{2,1,0:T(8,128)(2,1)S(1)} %shard_map.251), channel_id=1, replica_groups=mesh['ep'=16,'tp'=16] {'ep'}, dimensions={0} | all-to-all | bytes 3801088 | tf_op jit(solution)/shard_map/all_to_all | solution.py:35
  114.6 1.6 shard_map.252
  116.8 3.6 %all-to-all-start.6 = ((bf16[16,32,512]{2,1,0:T(8,128)(2,1)}), bf16[16,32,512]{2,1,0:T(8,128)(2,1)S(1)}, u32[]{:S(2)}, u32[]{:S(2)}) async-start(bf16[16,32,512]{2,1,0:T(8,128)(2,1)} %get-tuple-element.58), calls=%async_computation.6 | async-start | bytes 1048576 | tf_op jit(solution)/shard_map/all_to_all | solution.py:35
  120.4 4.9 %shard_map.253 = (bf16[16,256,128]{2,1,0:T(8,128)(2,1)S(1)}, bf16[512,256]{1,0:T(8,128)(2,1)S(1)}) custom-call(bf16[16,464,128]{2,1,0:T(8,128)(2,1)S(1)} %all_to_all.54.p_ref.x_ref, f32[1,4096]{1,0:T(1,128)S(1)} %bitcast.19, bf16[1,4096,256]{2,1,0:T(8,128)(2,1)} %gate_hbm.1, bf16[1,4096,256]{2,1,0:T(8,128)(2,1)} %up_hbm.1, bf16[1,256,4096]{2,1,0:T(8,128)(2,1)} %down_hbm.1, ...), custom_call_target="tpu_custom_call" | custom-call | tf_op jit(solution)/shard_map/pallas_call | solution.py:414
  125.4 0.7 copy-done.3
  126.1 4.9 %all-to-all-done.6.h_ref = bf16[16,32,512]{2,1,0:T(8,128)(2,1)S(1)} async-done(((bf16[16,32,512]{2,1,0:T(8,128)(2,1)}), bf16[16,32,512]{2,1,0:T(8,128)(2,1)S(1)}, u32[]{:S(2)}, u32[]{:S(2)}) %all-to-all-start.6) | async-done | bytes 524320 | tf_op jit(solution)/shard_map/all_to_all | solution.py:35
  131.0 0.9 copy-done.4
  132.3 18.4 %all_to_all.55.r_ref = bf16[16,256,128]{2,1,0:T(8,128)(2,1)S(1)} all-to-all(bf16[16,256,128]{2,1,0:T(8,128)(2,1)S(1)} %shard_map.254), channel_id=1, replica_groups=mesh['ep'=16,'tp'=16] {'ep'}, dimensions={0} | all-to-all | bytes 2097152 | tf_op jit(solution)/shard_map/all_to_all | solution.py:35
  150.7 1.1 shard_map.255
  151.9 16.9 %all_to_all.56.p_ref = bf16[16,64,128]{2,1,0:T(8,128)(2,1)S(1)} all-to-all(bf16[16,64,128]{2,1,0:T(8,128)(2,1)S(1)} %shard_map.255), channel_id=1, replica_groups=mesh['ep'=16,'tp'=16] {'tp'}, dimensions={0} | all-to-all | bytes 524288 | tf_op jit(solution)/shard_map/all_to_all | solution.py:35
  168.8 14.2 %all_to_all.57 = bf16[16,64,128]{2,1,0:T(8,128)(2,1)S(1)} all-to-all(bf16[16,64,128]{2,1,0:T(8,128)(2,1)S(1)} %shard_map.256), channel_id=1, replica_groups=mesh['ep'=16,'tp'=16] {'tp'}, dimensions={0} | all-to-all | bytes 524288 | tf_op jit(solution)/shard_map/all_to_all | solution.py:35
  183.1 0.8 reshape.19
  (38 shorter events, 1.4 us)
Async XLA Ops:
  0.6 44.9 %copy-start = (bf16[128,256]{1,0:T(8,128)(2,1)S(1)}, bf16[128,256]{1,0:T(8,128)(2,1)}, u32[]{:S(2)}) copy-start(bf16[128,256]{1,0:T(8,128)(2,1)} %param.35) | copy-start | bytes 196612
  0.6 17.0 %copy-start.6 = (f32[4096]{0:T(1024)S(1)}, f32[4096]{0:T(1024)}, u32[]{:S(2)}) copy-start(f32[4096]{0:T(1024)} %param.27) | copy-start | bytes 49156
  0.7 17.0 %copy-start.10 = (bf16[256,128]{1,0:T(8,128)(2,1)S(1)}, bf16[256,128]{1,0:T(8,128)(2,1)}, u32[]{:S(2)}) copy-start(bf16[256,128]{1,0:T(8,128)(2,1)} %g_ref.1) | copy-start | bytes 196612
  0.7 17.0 %copy-start.9 = (bf16[256,128]{1,0:T(8,128)(2,1)S(1)}, bf16[256,128]{1,0:T(8,128)(2,1)}, u32[]{:S(2)}) copy-start(bf16[256,128]{1,0:T(8,128)(2,1)} %v_ref.1) | copy-start | bytes 196612
  0.7 17.0 %copy-start.8 = (bf16[256,128]{1,0:T(8,128)(2,1)S(1)}, bf16[256,128]{1,0:T(8,128)(2,1)}, u32[]{:S(2)}) copy-start(bf16[256,128]{1,0:T(8,128)(2,1)} %k_ref.1) | copy-start | bytes 196612
  0.7 17.0 %copy-start.7 = (bf16[256,128]{1,0:T(8,128)(2,1)S(1)}, bf16[256,128]{1,0:T(8,128)(2,1)}, u32[]{:S(2)}) copy-start(bf16[256,128]{1,0:T(8,128)(2,1)} %q_ref.1) | copy-start | bytes 196612
  2.5 15.1 %all-to-all-start = ((bf16[16,32,256]{2,1,0:T(8,128)(2,1)}), bf16[16,32,256]{2,1,0:T(8,128)(2,1)S(1)}, u32[]{:S(2)}, u32[]{:S(2)}) async-start(bf16[16,32,256]{2,1,0:T(8,128)(2,1)} %shard_map.246), calls=%async_computation | async-start | bytes 524288 | tf_op jit(solution)/shard_map/all_to_all | solution.py:35
  13.9 3.7 %copy-start.15 = (f32[4,32]{1,0:T(4,128)}, f32[4,32]{1,0:T(4,128)S(1)}, u32[]{:S(2)}) copy-start(f32[4,32]{1,0:T(4,128)S(1)} %get-tuple-element.67.table_ref) | copy-start | bytes 1540
  32.1 51.3 %copy-start.1 = (bf16[256,512]{1,0:T(8,128)(2,1)S(1)}, bf16[256,512]{1,0:T(8,128)(2,1)}, u32[]{:S(2)}) copy-start(bf16[256,512]{1,0:T(8,128)(2,1)} %gate_ref.1) | copy-start | bytes 786436
  32.1 51.4 %copy-start.2 = (bf16[256,512]{1,0:T(8,128)(2,1)S(1)}, bf16[256,512]{1,0:T(8,128)(2,1)}, u32[]{:S(2)}) copy-start(bf16[256,512]{1,0:T(8,128)(2,1)} %up_ref.1) | copy-start | bytes 786436
  32.1 51.4 %copy-start.5 = (f32[4096]{0:T(1024)S(1)}, f32[4096]{0:T(1024)}, u32[]{:S(2)}) copy-start(f32[4096]{0:T(1024)} %param.36) | copy-start | bytes 49156
  116.2 0.6 copy-start.11
  116.2 0.6 copy-start.13
  116.8 14.1 %all-to-all-start.6 = ((bf16[16,32,512]{2,1,0:T(8,128)(2,1)}), bf16[16,32,512]{2,1,0:T(8,128)(2,1)S(1)}, u32[]{:S(2)}, u32[]{:S(2)}) async-start(bf16[16,32,512]{2,1,0:T(8,128)(2,1)} %get-tuple-element.58), calls=%async_computation.6 | async-start | bytes 1048576 | tf_op jit(solution)/shard_map/all_to_all | solution.py:35
  125.3 0.7 copy-start.3
  131.0 1.0 copy-start.4
  131.9 18.8 %copy-start.14 = (f32[32,128]{1,0:T(8,128)S(1)}, f32[32,128]{1,0:T(8,128)}, u32[]{:S(2)}) copy-start(f32[32,128]{1,0:T(8,128)} %copy-done.13) | copy-start | bytes 49156
  131.9 18.8 %copy-start.16 = (f32[4,32]{1,0:T(4,128)S(1)}, f32[4,32]{1,0:T(4,128)}, u32[]{:S(2)}) copy-start(f32[4,32]{1,0:T(4,128)} %copy-done.15) | copy-start | bytes 1540
  132.3 36.5 %copy-start.12 = (bf16[64,128]{1,0:T(8,128)(2,1)S(1)}, bf16[64,128]{1,0:T(8,128)(2,1)}, u32[]{:S(2)}) copy-start(bf16[64,128]{1,0:T(8,128)(2,1)} %copy-done.11) | copy-start | bytes 49156

commit v3 on v2

--- a/solution.py
+++ b/solution.py
@@ -12,11 +12,11 @@
 EP, TP = 16, 16
 ROWS, WIDTH, COLS, HEAD, UNITS, CAP = 32, 4096, 256, 128, 512, 6
 ALL = ROWS * EP
-ROUTED = 2 * CAP * EP
+ROUTED = CAP * EP
 SIDE = ROUTED + 8 * ROWS
 PACKED = SIDE + 16
 CHUNKS = WIDTH // 128
-BACK = CAP * CHUNKS
+BACK = CAP * EP
 RETURN = BACK + 2 * ROWS
 def in_hbm(x):
     return pltpu.with_memory_space_constraint(x, pltpu.HBM)
@@ -47,13 +47,19 @@
     return lax.dot_general(a, b, (((1,), (1,)), ((), ())), preferred_element_type=F32)
 
 
-def cut_kernel(x_ref, o_ref, done):
-    moves = [
-        pltpu.make_async_copy(x_ref.at[:, pl.ds(e * COLS, COLS)], o_ref.at[e], done.at[e]) for e in range(EP)
-    ]
-    for move in moves:
+def cut_kernel(x_hbm, o_hbm, x_ref, o_ref, done):
+    half = ROWS // 2
+    rows = [pl.ds(i * half, half) for i in range(2)]
+    into = [pltpu.make_async_copy(x_hbm.at[r], x_ref.at[r], done.at[0, i]) for i, r in enumerate(rows)]
+    back = [pltpu.make_async_copy(o_ref.at[:, r], o_hbm.at[:, r], done.at[1, i]) for i, r in enumerate(rows)]
+    for move in into:
         move.start()
-    for move in moves:
+    for i in range(2):
+        into[i].wait()
+        for e in range(EP):
+            o_ref[e, i * half : (i + 1) * half] = x_ref[i * half : (i + 1) * half, e * COLS : (e + 1) * COLS]
+        back[i].start()
+    for move in back:
         move.wait()
 
 
@@ -62,9 +68,11 @@
         cut_kernel,
         out_shape=jax.ShapeDtypeStruct((EP, ROWS, COLS), BF),
         in_specs=[HBM],
-        out_specs=VMEM,
-        scratch_shapes=[pltpu.SemaphoreType.DMA((EP,))],
-        compiler_params=grant(1),
+        out_specs=HBM,
+        scratch_shapes=[
+            pltpu.VMEM((ROWS, WIDTH), BF), pltpu.VMEM((EP, ROWS, COLS), BF), pltpu.SemaphoreType.DMA((2, 2)),
+        ],
+        compiler_params=grant(2),
     )(in_hbm(tokens))
 
 
@@ -163,68 +171,56 @@
 STEP = 8
 
 
-def cell_kernel(
-    p_ref, scale_ref, write_ref, extra_ref, norm_ref, old_ref,
-    mixed_ref, new_norm_ref, new_ref, proj, numer, gated,
-):
-    step = pl.program_id(0)
-
-    @pl.when(step == 0)
-    def _():
-        for i in range(4):
-            lanes = slice(i * HEAD, (i + 1) * HEAD)
-            total = p_ref[0, :, lanes].astype(F32)
-            for e in range(1, EP):
-                total = total + p_ref[e, :, lanes].astype(F32)
-            proj[i] = total * scale_ref[...]
-
-    here = pl.ds(pl.multiple_of(step * STEP, STEP), STEP)
-    query, key, value, outgate = (proj[i, here, :] for i in range(4))
-    write = write_ref[here, :]
-    key = key * HEAD ** (-0.5)
-    wkey = write * key
-    new_norm = norm_ref[here, :] + wkey
-    new_norm_ref[here, :] = new_norm
-    query_t, wkey_t = query.T, wkey.T
-    for j in range(STEP):
-        row = slice(j, j + 1)
-        new = old_ref[step * STEP + j] + wkey_t[:, row] * value[row]
-        new_ref[j, 0] = new
-        numer[row, :] = jnp.sum(query_t[:, row] * new, axis=0, keepdims=True)
+def cell_kernel(p_ref, scale_ref, write_ref, extra_ref, norm_ref, old_ref, mixed_ref, new_norm_ref, new_hbm, numer, new_ref, done):
+    proj = []
+    for i in range(4):
+        lanes = slice(i * HEAD, (i + 1) * HEAD)
+        total = p_ref[0, :, lanes].astype(F32)
+        for e in range(1, EP):
+            total = total + p_ref[e, :, lanes].astype(F32)
+        proj.append(total * scale_ref[...])
+    query, key, value, outgate = proj
+    wkey = write_ref[...] * (key * HEAD ** (-0.5))
+    new_norm = norm_ref[...] + wkey
+    new_norm_ref[...] = new_norm
+    moves = []
+    for step in range(ROWS // STEP):
+        here = slice(step * STEP, (step + 1) * STEP)
+        query_t, wkey_t = query[here].T, wkey[here].T
+        for j in range(STEP):
+            row = step * STEP + j
+            new = old_ref[row] + wkey_t[:, j : j + 1] * value[row : row + 1]
+            new_ref[row, 0] = new
+            numer[row : row + 1, :] = jnp.sum(query_t[:, j : j + 1] * new, axis=0, keepdims=True)
+        moves.append(pltpu.make_async_copy(new_ref.at[pl.ds(step * STEP, STEP)], new_hbm.at[pl.ds(step * STEP, STEP)], done.at[step]))
+        moves[-1].start()
     denom = jnp.sum(query * new_norm, axis=1, keepdims=True)
     out = numer[...] / jnp.maximum(jnp.abs(denom), 1.0)
-    gated[here, :] = jax.nn.sigmoid(outgate) * out
-
-    @pl.when(step == ROWS // STEP - 1)
-    def _():
-        mixed = gated[...].astype(BF)
-        extra = extra_ref[...]
-        for e in range(EP):
-            mixed_ref[e, :ROWS] = mixed
-            mixed_ref[e, ROWS:] = extra
+    mixed = (jax.nn.sigmoid(outgate) * out).astype(BF)
+    extra = extra_ref[...]
+    for e in range(EP):
+        mixed_ref[e, :ROWS] = mixed
+        mixed_ref[e, ROWS:] = extra
+    for move in moves:
+        move.wait()
 
 
 def cell(parts, scale, write, extra, norm, old):
-    whole = lambda *shape: pl.BlockSpec(shape, lambda i: (0,) * len(shape))
     return pl.pallas_call(
         cell_kernel,
-        grid=(ROWS // STEP,),
         out_shape=(
             jax.ShapeDtypeStruct((EP, ROWS + 8, HEAD), BF),
             jax.ShapeDtypeStruct((ROWS, HEAD), F32),
             jax.ShapeDtypeStruct((ROWS, 1, HEAD, HEAD), F32),
         ),
         in_specs=[VMEM] * 6,
-        out_specs=(
-            whole(EP, ROWS + 8, HEAD), whole(ROWS, HEAD),
-            pl.BlockSpec((STEP, 1, HEAD, HEAD), lambda i: (i, 0, 0, 0)),
-        ),
+        out_specs=(VMEM, VMEM, HBM),
         scratch_shapes=[
-            pltpu.VMEM((4, ROWS, HEAD), F32),
-            pltpu.VMEM((STEP, HEAD), F32),
             pltpu.VMEM((ROWS, HEAD), F32),
+            pltpu.VMEM((ROWS, 1, HEAD, HEAD), F32),
+            pltpu.SemaphoreType.DMA((ROWS // STEP,)),
         ],
-        compiler_params=grant(6),
+        compiler_params=grant(8),
     )(parts, scale, write, extra, norm, old)
 
 
@@ -264,16 +260,18 @@
     square_high, square_low = high_low(wide * wide)
     ones = jnp.ones((8, COLS), BF)
     squares = mm_nt(ones, square_high.astype(BF)) + mm_nt(ones, square_low.astype(BF))
-    branch = mm_nt(jnp.broadcast_to(my_columns(branch_ref, t_ref), (8, COLS)), gained)
+    line = lax.broadcasted_iota(I32, (2 * EP, 128), 0)
+    pick = lambda h: jnp.sum(jnp.where(line == 2 * t_ref[0] + h, branch_ref[...].astype(F32), 0.0), axis=0, keepdims=True)
+    weights = jnp.concatenate([pick(0), pick(1)], axis=1).astype(BF)
+    branch = mm_nt(jnp.broadcast_to(weights, (8, COLS)), gained)
     sq_high, sq_low = high_low(squares)
     br_high, br_low = high_low(branch)
     line = lax.broadcasted_iota(I32, (8, ALL), 0)
     side = jnp.where(line == 0, sq_high, jnp.where(line == 1, sq_low, jnp.where(line == 2, br_high, br_low)))
-    me = t_ref[1]
     at = lax.broadcasted_iota(I32, (8 * EP, ALL), 0)
     token = lax.broadcasted_iota(I32, (8 * EP, ALL), 1)
     quarter = at % 8
-    mine = (token == (at // 8) * ROWS + 2 * me + quarter // 2) & (quarter < 4)
+    mine = (token == (at // 8) * ROWS + 2 * t_ref[1] + quarter // 2) & (quarter < 4)
     own = mm((mine & (quarter % 2 == 0)).astype(F32).astype(BF), resid[:, :128])
     own = own + mm((mine & (quarter % 2 == 1)).astype(F32).astype(BF), resid[:, 128:])
     for g in range(EP):
@@ -293,13 +291,11 @@
         codes = jnp.concatenate(tiles, axis=1).astype(I32)
         first = codes[0:1] + group * 128 - base
         second = codes[1:2] + group * 128 - base
-        source = resid[half * 256 : (half + 1) * 256]
+        source = jnp.where(t_ref[1] % 2 == 0, wide[:, :128], wide[:, 128:])[half * 256 : (half + 1) * 256].astype(BF)
         for x in range(EP):
             member = (first == x * 8) | (second == x * 8)
             picked = mm(jnp.where(member, 1.0, 0.0).astype(BF), source).astype(BF)
-            for h in range(2):
-                at = h * CAP * EP + half * half_rows
-                o_ref[x, at : at + half_rows, :] = picked[:, h * 128 : (h + 1) * 128]
+            o_ref[x, half * half_rows : (half + 1) * half_rows, :] = picked
 
 
 def feed(me, resid, gain, branch, mix, gate, up):
@@ -312,30 +308,27 @@
     )(me, resid, gain, branch, mix, gate, up)
 
 
-def hidden_kernel(e_ref, p_ref, o_ref, b_ref, kept_ref, kept):
-    def total(at, size):
-        value = p_ref[0, at : at + size, :].astype(F32)
-        for e in range(1, EP):
-            value = value + p_ref[e, at : at + size, :].astype(F32)
-        return value
-
-    side = total(SIDE, 16)
+def over_peers(ref, at, size):
+    value = ref[0, at : at + size, :].astype(F32)
+    for e in range(1, EP):
+        value = value + ref[e, at : at + size, :].astype(F32)
+    return value
+
+
+def token_sums(me_ref, side):
     lane = lax.broadcasted_iota(I32, (ROWS, 128), 1)
     row = lax.broadcasted_iota(I32, (ROWS, 128), 0)
-    mine = lane == (e_ref[0] % 4) * ROWS + row
+    mine = lane == (me_ref[0] % 4) * ROWS + row
     squares = jnp.sum(jnp.where(mine, side[0:1] + side[1:2], 0.0), axis=1, keepdims=True)
     branch = jnp.sum(jnp.where(mine, side[2:3] + side[3:4], 0.0), axis=1, keepdims=True)
-    scale = lax.rsqrt(squares / WIDTH + EPS)
-    for e in range(EP):
-        rows = p_ref[e, SIDE:PACKED, :].astype(F32)
-        for r in range(2):
-            at = r * CHUNKS + 2 * e
-            kept[at : at + 2, :] = rows[8 + 2 * r : 10 + 2 * r]
-    kept_ref[...] = kept[...].astype(BF)
-    b_ref[...] = jnp.broadcast_to(jax.nn.sigmoid(branch * scale), (ROWS, 128))
+    return lax.rsqrt(squares / WIDTH + EPS), branch
+
+
+def hidden_kernel(me_ref, p_ref, o_ref):
+    scale, _ = token_sums(me_ref, over_peers(p_ref, SIDE, 16))
     for j in range(4):
-        gate = total(ROUTED + j * ROWS, ROWS) * scale
-        up = total(ROUTED + (4 + j) * ROWS, ROWS) * scale
+        gate = over_peers(p_ref, ROUTED + j * ROWS, ROWS) * scale
+        up = over_peers(p_ref, ROUTED + (4 + j) * ROWS, ROWS) * scale
         value = (gate * jax.nn.sigmoid(gate) * up).astype(BF)
         for e in range(EP):
             o_ref[e, :, j * 128 : (j + 1) * 128] = value
@@ -344,15 +337,34 @@
 def hidden_units(me, packed):
     return pl.pallas_call(
         hidden_kernel,
+        out_shape=jax.ShapeDtypeStruct((EP, ROWS, UNITS), BF),
+        in_specs=[SMEM, VMEM],
+        out_specs=VMEM,
+        compiler_params=grant(8),
+    )(me, packed)
+
+
+def sides_kernel(me_ref, p_ref, b_ref, kept_ref, kept):
+    scale, branch = token_sums(me_ref, over_peers(p_ref, SIDE, 16))
+    b_ref[...] = jnp.broadcast_to(jax.nn.sigmoid(branch * scale), (ROWS, 128))
+    for e in range(EP):
+        rows = p_ref[e, SIDE:PACKED, :].astype(F32)
+        for q in range(4):
+            kept[q * EP + e : q * EP + e + 1, :] = rows[8 + q : 9 + q]
+    kept_ref[...] = kept[...].astype(BF)
+
+
+def sides(me, packed):
+    return pl.pallas_call(
+        sides_kernel,
         out_shape=(
-            jax.ShapeDtypeStruct((EP, ROWS, UNITS), BF),
             jax.ShapeDtypeStruct((ROWS, 128), F32),
             jax.ShapeDtypeStruct((2 * CHUNKS, 128), BF),
         ),
         in_specs=[SMEM, VMEM],
-        out_specs=(VMEM,) * 3,
+        out_specs=(VMEM, VMEM),
         scratch_shapes=[pltpu.VMEM((2 * CHUNKS, 128), F32)],
-        compiler_params=grant(8),
+        compiler_params=grant(4),
     )(me, packed)
 
 
@@ -363,9 +375,10 @@
 
 
 def expert_kernel(
-    x_ref, gain_ref, gate_hbm, up_hbm, down_hbm, dense_hbm, o_ref, dense_ref, gate_ref, up_ref, down_ref, turned, done,
+    me_ref, x_ref, y_ref, gain_ref, gate_hbm, up_hbm, down_hbm, o_ref, send_ref, gate_ref, up_ref, down_ref, turned, done,
 ):
     slots = CAP * EP
+    core = me_ref[1] % 2
     gates, ups, downs = [], [], []
     for i in range(K_STEPS):
         part = pl.ds(i * DEEP, DEEP)
@@ -374,13 +387,11 @@
     for i in range(N_STEPS):
         part = pl.ds(i * LANES, LANES)
         downs.append(pltpu.make_async_copy(down_hbm.at[0, :, part], down_ref.at[:, part], done.at[2, i]))
-    dense = pltpu.make_async_copy(dense_hbm, dense_ref, done.at[3, 0])
     for i in range(K_STEPS):
         gates[i].start()
         ups[i].start()
     for move in downs:
         move.start()
-    dense.start()
     squares = jnp.zeros((slots, 128), F32)
     gate = jnp.zeros((slots, COLS), F32)
     up = jnp.zeros((slots, COLS), F32)
@@ -388,7 +399,7 @@
         pieces = []
         for e in range(i * PER_STEP, (i + 1) * PER_STEP):
             for h in range(2):
-                x = x_ref[e, h * slots : (h + 1) * slots, :].astype(F32)
+                x = jnp.where(core == h, x_ref[e, :ROUTED, :].astype(F32), y_ref[e].astype(F32))
                 squares += x * x
                 at = (2 * e + h) * 128
                 pieces.append((x * gain_ref[:, at : at + 128]).astype(BF))
@@ -404,73 +415,104 @@
         downs[i].wait()
         out = mm(hidden, down_ref[:, i * LANES : (i + 1) * LANES])
         for c in range(LANES // 128):
-            turned[pl.ds(i * (LANES // 128) + c, slots, stride=CHUNKS), :] = out[:, c * 128 : (c + 1) * 128]
+            chunk = i * (LANES // 128) + c
+            at = (chunk % 2) * slots * EP + chunk // 2
+            turned[pl.ds(at, slots, stride=EP), :] = out[:, c * 128 : (c + 1) * 128]
     for g in range(EP):
-        o_ref[g, :BACK, :] = turned[g * BACK : (g + 1) * BACK, :].astype(BF)
-    dense.wait()
-
-
-def expert(packed, gain, gate, up, down_w, dense_w):
+        mine = pl.multiple_of(core * slots * EP + g * BACK, BACK)
+        other = pl.multiple_of((1 - core) * slots * EP + g * BACK, BACK)
+        o_ref[g] = turned[pl.ds(mine, BACK), :].astype(BF)
+        send_ref[g] = turned[pl.ds(other, BACK), :].astype(BF)
+
+
+def expert(me, packed, other, gain, gate, up, down_w):
+    rows = jax.ShapeDtypeStruct((EP, BACK, 128), BF)
     return pl.pallas_call(
         expert_kernel,
-        out_shape=(
-            jax.ShapeDtypeStruct((EP, RETURN, 128), BF),
-            jax.ShapeDtypeStruct(dense_w.shape, BF),
-        ),
-        in_specs=[VMEM, VMEM, HBM, HBM, HBM, HBM],
+        out_shape=(rows, rows),
+        in_specs=[SMEM, VMEM, VMEM, VMEM, HBM, HBM, HBM],
         out_specs=(VMEM, VMEM),
         scratch_shapes=[
             pltpu.VMEM((WIDTH, COLS), BF),
             pltpu.VMEM((WIDTH, COLS), BF),
             pltpu.VMEM((COLS, WIDTH), BF),
             pltpu.VMEM((CAP * EP * CHUNKS, 128), F32),
-            pltpu.SemaphoreType.DMA((4, 8)),
+            pltpu.SemaphoreType.DMA((3, 8)),
         ],
-        compiler_params=grant(14),
-    )(packed, gain, in_hbm(gate), in_hbm(up), in_hbm(down_w), in_hbm(dense_w))
-
-
-def down_kernel(h_ref, w_ref, _, o_ref):
+        compiler_params=grant(16),
+    )(me, packed, other, gain, in_hbm(gate), in_hbm(up), in_hbm(down_w))
+
+
+def down_kernel(h_ref, w_ref, x_ref, y_ref, o_ref):
+    for g in range(EP):
+        o_ref[g, :BACK, :] = (x_ref[g].astype(F32) + y_ref[g].astype(F32)).astype(BF)
     out = mm(h_ref[...].reshape(ALL, UNITS), w_ref[...]).astype(BF)
     for h in range(2):
-        o_ref[:, h * ROWS : (h + 1) * ROWS, :] = out[:, h * 128 : (h + 1) * 128].reshape(EP, ROWS, 128)
-
-
-def down(hidden, w, buffer):
-    whole = lambda *shape: pl.BlockSpec(shape, lambda i: (0,) * len(shape))
+        at = BACK + h * ROWS
+        o_ref[:, at : at + ROWS, :] = out[:, h * 128 : (h + 1) * 128].reshape(EP, ROWS, 128)
+
+
+def down(hidden, w, rows, more):
     return pl.pallas_call(
         down_kernel,
-        grid=(1,),
         out_shape=jax.ShapeDtypeStruct((EP, RETURN, 128), BF),
-        in_specs=[whole(EP, ROWS, UNITS), whole(UNITS, COLS), pl.BlockSpec(memory_space=pl.ANY)],
-        out_specs=pl.BlockSpec((EP, 2 * ROWS, 128), lambda i: (0, BACK // (2 * ROWS), 0)),
-        input_output_aliases={2: 0},
+        in_specs=[VMEM] * 4,
+        out_specs=VMEM,
         compiler_params=grant(6),
-    )(hidden, w, buffer)
-
-
-def gather_kernel(table_ref, branch_ref, r_ref, o_ref, dense):
-    for c in range(CHUNKS):
-        at = BACK + (c % 2) * ROWS
-        dense[c * ROWS : (c + 1) * ROWS, :] = r_ref[c // 2, at : at + ROWS, :].astype(F32)
+    )(hidden, w, rows, more)
+
+
+def gather_kernel(me_ref, table_ref, branch_ref, r_ref, o_ref, dense):
+    for h in range(2):
+        for e in range(EP):
+            at = (h * EP + e) * ROWS
+            dense[at : at + ROWS, :] = r_ref[e, BACK + h * ROWS : BACK + (h + 1) * ROWS, :].astype(F32)
+    mine = lax.broadcasted_iota(I32, (CHUNKS, 128), 0) // EP == me_ref[1] % 2
     for r in range(ROWS):
-        total = branch_ref[r : r + 1, :] * dense[pl.ds(r, CHUNKS, stride=ROWS), :]
+        total = jnp.zeros((EP, 128), F32)
         for k in range(2):
             code = table_ref[k, r].astype(I32)
-            at = pl.multiple_of((code % 8) * CHUNKS, CHUNKS)
-            total = total + table_ref[2 + k, r] * r_ref[code // 8, pl.ds(at, CHUNKS), :].astype(F32)
+            at = pl.multiple_of((code % 8) * EP, EP)
+            total = total + table_ref[2 + k, r] * r_ref[code // 8, pl.ds(at, EP), :].astype(F32)
+        total = jnp.where(mine, jnp.concatenate([total, total], axis=0), 0.0)
+        total = total + branch_ref[r : r + 1, :] * dense[pl.ds(r, CHUNKS, stride=ROWS), :]
         o_ref[r // 2, (r % 2) * CHUNKS : (r % 2 + 1) * CHUNKS, :] = total.astype(BF)
 
 
-def gather(table, branch, returned):
+def gather(me, table, branch, returned):
     return pl.pallas_call(
         gather_kernel,
         out_shape=jax.ShapeDtypeStruct((TP, 2 * CHUNKS, 128), BF),
-        in_specs=[SMEM, VMEM, VMEM],
+        in_specs=[SMEM, SMEM, VMEM, VMEM],
         out_specs=VMEM,
         scratch_shapes=[pltpu.VMEM((CHUNKS * ROWS, 128), F32)],
         compiler_params=grant(6),
-    )(table, branch, returned)
+    )(me, table, branch, returned)
+
+
+def finish_kernel(p_ref, kept_ref, o_ref, turned):
+    total = p_ref[0].astype(F32)
+    for t in range(1, TP):
+        total = total + p_ref[t].astype(F32)
+    total = total + kept_ref[...].astype(F32)
+    for r in range(2):
+        for h in range(2):
+            at = r * CHUNKS + h * EP
+            turned[pl.ds(r * CHUNKS + h, EP, stride=2), :] = total[at : at + EP]
+    out = turned[...].astype(BF)
+    for t in range(TP):
+        o_ref[t] = out
+
+
+def finish(parts, kept):
+    return pl.pallas_call(
+        finish_kernel,
+        out_shape=jax.ShapeDtypeStruct(parts.shape, BF),
+        in_specs=[VMEM, VMEM],
+        out_specs=VMEM,
+        scratch_shapes=[pltpu.VMEM((2 * CHUNKS, 128), F32)],
+        compiler_params=grant(4),
+    )(parts, kept)
 
 
 def on_device(
@@ -504,7 +546,7 @@
         me, tokens, mixer_gain[None], w_ingate.T, w_forget.T, forget_bias[None], state_max.T, state_norm,
         routes.T, route_weight.T, state_matrix,
     )
-    gains = (mixer_gain[None], ffn_gain[None], w_branch[None])
+    gains = (mixer_gain[None], ffn_gain[None], w_branch.reshape(2 * EP, 128))
     scale, write, new_max, extra, table, norm, old = own
     (token_cols, scale, write, extra, norm, old, gains, me) = lax.optimization_barrier(
         (token_cols, scale, write, extra, norm, old, gains, me)
@@ -517,19 +559,23 @@
     spread_out = mm(mixed_all[:, :ROWS].reshape(ALL, HEAD), w_proj).astype(BF).reshape(TP, ROWS, COLS)
     resid = swap(settle(swap(spread_out, "tp"), token_block), "tp")
 
-    arrived = swap(feed(me, resid, gains[1], gains[2], mixed_all, dense_gate, dense_up), "ep")
-    hidden, branch, kept = hidden_units(me, arrived)
+    packed = swap(feed(me, resid, gains[1], gains[2], mixed_all, dense_gate, dense_up), "ep")
+    cores = [(t, t ^ 1) for t in range(TP)]
+    other = lax.ppermute(packed[:, :ROUTED], "tp", cores)
+    hidden = hidden_units(me, packed)
     hidden_all = swap(hidden, "ep")
 
-    _, arrived = lax.optimization_barrier((hidden, arrived))
-    buffer, down_w = expert(arrived, gains[1], expert_gate, expert_up, expert_down, dense_down)
-    hidden_all, buffer, down_w, branch, kept, new_max, new_norm, table = lax.optimization_barrier(
-        (hidden_all, buffer, down_w, branch, kept, new_max, new_norm, table)
+    _, packed, other = lax.optimization_barrier((hidden, packed, other))
+    branch, kept = sides(me, packed)
+    rows_out, rows_sent = expert(me, packed, other, gains[1], expert_gate, expert_up, expert_down)
+    more = lax.ppermute(rows_sent, "tp", cores)
+    hidden_all, rows_out, more, branch, kept, new_max, new_norm, table = lax.optimization_barrier(
+        (hidden_all, rows_out, more, branch, kept, new_max, new_norm, table)
     )
 
-    returned = swap(down(hidden_all, down_w, buffer), "ep")
-    parts = swap(gather(table, branch, returned), "tp")
-    layer_out = swap(settle(parts, kept), "tp").reshape(ROWS, WIDTH)
+    returned = swap(down(hidden_all, dense_down, rows_out, more), "ep")
+    parts = swap(gather(me, table, branch, returned), "tp")
+    layer_out = swap(finish(parts, kept), "tp").reshape(ROWS, WIDTH)
     new_max = new_max.T
     return (layer_out, new_matrix, new_norm[:, None], new_max)
 

time: 185 us -> 176 us (0.951)
  blocking collectives: 140 us -> 131 us
  local copies, waits for them, and re-layouts: 3.84 us -> 0.91 us
    all_to_all x8, blocking collectives: 140 us -> 131 us  [swap(): return lax.all_to_all(parts, axis, 0, 0, tiled=True)]
    unnamed x34 -> x22, local copies, waits for them, and re-layouts: 2.31 us -> 0.05 us
    pallas_call x4 -> x6, Pallas kernels: 10.2 us -> 11.5 us  [the longest x1 5.71 us: expert(): pl.pallas_call(expert_kernel, out_shape=(rows, rows), in_specs=[SMEM, VME...]
  transfers between devices with their start and end apart: 2 -> 4, of which waited for: 2 -> 2; matrix products, arithmetic and copies ran while one was open for 0% -> 0% of each run, Pallas kernels for 4% -> 6%
where the time goes in v3:
time: 176 us; the launch traced here: 175 us
  blocking collectives  131 us (74%)
  Pallas kernels  20.3 us (12%)
  starting transfers between devices  12.4 us (7%)
  waiting for transfers between devices  9.2 us (5%)
    all_to_all x8, blocking collectives, swap(): return lax.all_to_all(parts, axis, 0, 0, tiled=True)  131 us
    all_to_all x2, starting transfers between devices, swap(): return lax.all_to_all(parts, axis, 0, 0, tiled=True)  11.2 us
    all_to_all x2, waiting for transfers between devices, swap(): return lax.all_to_all(parts, axis, 0, 0, tiled=True)  9.19 us
    pallas_call x1, Pallas kernels, expert(): pl.pallas_call(expert_kernel, out_shape=(rows, rows), in_specs=[SMEM, VME...  5.71 us
  transfers between devices with their start and end apart: 4, of which 2 were waited for; matrix products, arithmetic and copies ran while one was open for 0% of the time, Pallas kernels for 6%

profile of v3, /device:TPU:1, one launch (start us, length us, event | category | flops | bytes accessed | tf_op | source)
XLA Modules:
  0.0 174.9 jit_solution(9401843472455771379)
XLA Ops:
  0.7 1.8 %shard_map.246 = bf16[16,32,256]{2,1,0:T(8,128)(2,1)} custom-call(bf16[32,4096]{1,0:T(8,128)(2,1)} %refs_0_.1), custom_call_target="tpu_custom_call" | custom-call | tf_op jit(solution)/shard_map/pallas_call | solution.py:67
  2.5 7.6 %all-to-all-start = ((bf16[16,32,256]{2,1,0:T(8,128)(2,1)}), bf16[16,32,256]{2,1,0:T(8,128)(2,1)S(1)}, u32[]{:S(2)}, u32[]{:S(2)}) async-start(bf16[16,32,256]{2,1,0:T(8,128)(2,1)} %shard_map.246), calls=%async_computation | async-start | bytes 524288 | tf_op jit(solution)/shard_map/all_to_all | solution.py:35
  10.1 3.0 %shard_map.247 = (f32[32,128]{1,0:T(8,128)S(1)}, f32[32,128]{1,0:T(8,128)S(1)}, f32[1,32]{1,0:T(1,128)}, bf16[8,128]{1,0:T(8,128)(2,1)S(1)}, f32[4,32]{1,0:T(4,1...) custom-call(s32[2]{0:T(128)S(1)} %pad_add_fusion.me_ref.t_ref, bf16[32,4096]{1,0:T(8,128)(2,1)} %refs_0_.1, ...), custom_call_target="tpu_custom_call" | custom-call | tf_op jit(solution)/shard_map/pallas_call | solution.py:134
  13.2 4.4 %all-to-all-done.x_ref = bf16[16,32,256]{2,1,0:T(8,128)(2,1)S(1)} async-done(((bf16[16,32,256]{2,1,0:T(8,128)(2,1)}), bf16[16,32,256]{2,1,0:T(8,128)(2,1)S(1)}, u32[]{:S(2)}, u32[]{:S(2)}) %all-to-all-start) | async-done | bytes 262176 | tf_op jit(solution)/shard_map/all_to_all | solution.py:35
  17.6 1.0 shard_map.248
  18.6 12.5 %all_to_all.50.p_ref = bf16[16,32,512]{2,1,0:T(8,128)(2,1)S(1)} all-to-all(bf16[16,32,512]{2,1,0:T(8,128)(2,1)S(1)} %get-tuple-element.48), channel_id=1, replica_groups=mesh['ep'=16,'tp'=16] {'ep'}, dimensions={0} | all-to-all | bytes 1048576 | tf_op jit(solution)/shard_map/all_to_all | solution.py:35
  31.2 3.2 %shard_map.249 = (bf16[16,40,128]{2,1,0:T(8,128)(2,1)S(1)}, f32[32,128]{1,0:T(8,128)}, f32[32,1,128,128]{3,2,1,0:T(8,128)}) custom-call(bf16[16,32,512]{2,1,0:T(8,128)(2,1)S(1)} %all_to_all.50.p_ref, f32[32,128]{1,0:T(8,128)S(1)} %get-tuple-element.49.scale_ref, f32[32,128]{1,0:T(8,128)S(1)} %get-tuple-element.50.write_ref, ...), custom_call_target="tpu_custom_call" | custom-call | tf_op jit(solution)/shard_map/pallas_call | solution.py:209
  34.3 9.6 %all_to_all.51.mix_ref = bf16[16,40,128]{2,1,0:T(8,128)(2,1)S(1)} all-to-all(bf16[16,40,128]{2,1,0:T(8,128)(2,1)S(1)} %get-tuple-element.54), channel_id=1, replica_groups=mesh['ep'=16,'tp'=16] {'ep'}, dimensions={0} | all-to-all | bytes 327680 | tf_op jit(solution)/shard_map/all_to_all | solution.py:35
  44.2 24.2 %all_to_all.52.p_ref = bf16[16,32,256]{2,1,0:T(8,128)(2,1)S(1)} all-to-all(bf16[16,32,256]{2,1,0:T(8,128)(2,1)S(1)} %bitcast.24), channel_id=1, replica_groups=mesh['ep'=16,'tp'=16] {'tp'}, dimensions={0} | all-to-all | bytes 524288 | tf_op jit(solution)/shard_map/all_to_all | solution.py:35
  68.5 14.4 %all_to_all.53.r_ref = bf16[16,32,256]{2,1,0:T(8,128)(2,1)S(1)} all-to-all(bf16[16,32,256]{2,1,0:T(8,128)(2,1)S(1)} %shard_map.250), channel_id=1, replica_groups=mesh['ep'=16,'tp'=16] {'tp'}, dimensions={0} | all-to-all | bytes 524288 | tf_op jit(solution)/shard_map/all_to_all | solution.py:35
  82.9 1.8 %shard_map.251 = bf16[16,368,128]{2,1,0:T(8,128)(2,1)S(1)} custom-call(s32[2]{0:T(128)S(1)} %pad_add_fusion.me_ref.t_ref, bf16[16,32,256]{2,1,0:T(8,128)(2,1)S(1)} %all_to_all.53.r_ref, f32[1,4096]{1,0:T(1,128)S(1)} %bitcast.19, bf16[32,128]{1,0:T(8,128)(2,1)S(1)} %bitcast.23, bf16[16,40,128]{2,1,0:T(8,128)(2,1)S(1)} %all_to_all.51.mix_ref, ...), custom_call_target="tpu_custom_call" | custom-call | tf_op jit(solution)/shard_map/pallas_call | solution.py:302
  84.7 24.8 %all_to_all.54.p_ref.x_ref = bf16[16,368,128]{2,1,0:T(8,128)(2,1)S(1)} all-to-all(bf16[16,368,128]{2,1,0:T(8,128)(2,1)S(1)} %shard_map.251), channel_id=1, replica_groups=mesh['ep'=16,'tp'=16] {'ep'}, dimensions={0} | all-to-all | bytes 3014656 | tf_op jit(solution)/shard_map/all_to_all | solution.py:35
  109.5 1.2 collective-permute-start
  110.7 1.6 shard_map.252
  112.3 3.6 %all-to-all-start.6 = ((bf16[16,32,512]{2,1,0:T(8,128)(2,1)}), bf16[16,32,512]{2,1,0:T(8,128)(2,1)S(1)}, u32[]{:S(2)}, u32[]{:S(2)}) async-start(bf16[16,32,512]{2,1,0:T(8,128)(2,1)} %shard_map.252), calls=%async_computation.6 | async-start | bytes 1048576 | tf_op jit(solution)/shard_map/all_to_all | solution.py:35
  115.9 5.7 %shard_map.253 = (bf16[16,96,128]{2,1,0:T(8,128)(2,1)S(1)}, bf16[16,96,128]{2,1,0:T(8,128)(2,1)}) custom-call(s32[2]{0:T(128)S(1)} %pad_add_fusion.me_ref.t_ref, bf16[16,368,128]{2,1,0:T(8,128)(2,1)S(1)} %all_to_all.54.p_ref.x_ref, bf16[16,96,128]{2,1,0:T(8,128)(2,1)S(1)} %collective-permute-done.y_ref, f32[1,4096]{1,0:T(1,128)S(1)} %bitcast.20, ...), custom_call_target="tpu_custom_call" | custom-call | tf_op jit(solution)/shard_map/pallas_call | solution.py:430
  121.7 0.7 shard_map.254
  122.4 4.8 %all-to-all-done.6.h_ref = bf16[16,32,512]{2,1,0:T(8,128)(2,1)S(1)} async-done(((bf16[16,32,512]{2,1,0:T(8,128)(2,1)}), bf16[16,32,512]{2,1,0:T(8,128)(2,1)S(1)}, u32[]{:S(2)}, u32[]{:S(2)}) %all-to-all-start.6) | async-done | bytes 524320 | tf_op jit(solution)/shard_map/all_to_all | solution.py:35
  127.2 0.3 shard_map.255
  127.5 14.9 %all_to_all.55.r_ref = bf16[16,160,128]{2,1,0:T(8,128)(2,1)S(1)} all-to-all(bf16[16,160,128]{2,1,0:T(8,128)(2,1)S(1)} %shard_map.255), channel_id=1, replica_groups=mesh['ep'=16,'tp'=16] {'ep'}, dimensions={0} | all-to-all | bytes 1310720 | tf_op jit(solution)/shard_map/all_to_all | solution.py:35
  142.4 1.1 shard_map.256
  143.5 16.3 %all_to_all.56.p_ref = bf16[16,64,128]{2,1,0:T(8,128)(2,1)S(1)} all-to-all(bf16[16,64,128]{2,1,0:T(8,128)(2,1)S(1)} %shard_map.256), channel_id=1, replica_groups=mesh['ep'=16,'tp'=16] {'tp'}, dimensions={0} | all-to-all | bytes 524288 | tf_op jit(solution)/shard_map/all_to_all | solution.py:35
  159.9 14.2 %all_to_all.57 = bf16[16,64,128]{2,1,0:T(8,128)(2,1)S(1)} all-to-all(bf16[16,64,128]{2,1,0:T(8,128)(2,1)S(1)} %shard_map.257), channel_id=1, replica_groups=mesh['ep'=16,'tp'=16] {'tp'}, dimensions={0} | all-to-all | bytes 524288 | tf_op jit(solution)/shard_map/all_to_all | solution.py:35
  174.1 0.8 reshape.23
  (31 shorter events, 0.6 us)
Async XLA Ops:
  0.6 43.3 %copy-start = (bf16[128,256]{1,0:T(8,128)(2,1)S(1)}, bf16[128,256]{1,0:T(8,128)(2,1)}, u32[]{:S(2)}) copy-start(bf16[128,256]{1,0:T(8,128)(2,1)} %param.35) | copy-start | bytes 196612
  0.6 17.0 %copy-start.5 = (f32[4096]{0:T(1024)S(1)}, f32[4096]{0:T(1024)}, u32[]{:S(2)}) copy-start(f32[4096]{0:T(1024)} %param.27) | copy-start | bytes 49156
  0.7 17.0 %copy-start.9 = (bf16[256,128]{1,0:T(8,128)(2,1)S(1)}, bf16[256,128]{1,0:T(8,128)(2,1)}, u32[]{:S(2)}) copy-start(bf16[256,128]{1,0:T(8,128)(2,1)} %g_ref.1) | copy-start | bytes 196612
  0.7 16.9 %copy-start.8 = (bf16[256,128]{1,0:T(8,128)(2,1)S(1)}, bf16[256,128]{1,0:T(8,128)(2,1)}, u32[]{:S(2)}) copy-start(bf16[256,128]{1,0:T(8,128)(2,1)} %v_ref.1) | copy-start | bytes 196612
  0.7 16.9 %copy-start.7 = (bf16[256,128]{1,0:T(8,128)(2,1)S(1)}, bf16[256,128]{1,0:T(8,128)(2,1)}, u32[]{:S(2)}) copy-start(bf16[256,128]{1,0:T(8,128)(2,1)} %k_ref.1) | copy-start | bytes 196612
  0.7 16.9 %copy-start.6 = (bf16[256,128]{1,0:T(8,128)(2,1)S(1)}, bf16[256,128]{1,0:T(8,128)(2,1)}, u32[]{:S(2)}) copy-start(bf16[256,128]{1,0:T(8,128)(2,1)} %q_ref.1) | copy-start | bytes 196612
  2.5 15.1 %all-to-all-start = ((bf16[16,32,256]{2,1,0:T(8,128)(2,1)}), bf16[16,32,256]{2,1,0:T(8,128)(2,1)S(1)}, u32[]{:S(2)}, u32[]{:S(2)}) async-start(bf16[16,32,256]{2,1,0:T(8,128)(2,1)} %shard_map.246), calls=%async_computation | async-start | bytes 524288 | tf_op jit(solution)/shard_map/all_to_all | solution.py:35
  31.1 51.7 %copy-start.2 = (bf16[256,512]{1,0:T(8,128)(2,1)S(1)}, bf16[256,512]{1,0:T(8,128)(2,1)}, u32[]{:S(2)}) copy-start(bf16[256,512]{1,0:T(8,128)(2,1)} %gate_ref.1) | copy-start | bytes 786436
  31.1 51.7 %copy-start.3 = (bf16[256,512]{1,0:T(8,128)(2,1)S(1)}, bf16[256,512]{1,0:T(8,128)(2,1)}, u32[]{:S(2)}) copy-start(bf16[256,512]{1,0:T(8,128)(2,1)} %up_ref.1) | copy-start | bytes 786436
  31.1 51.7 %copy-start.4 = (f32[4096]{0:T(1024)S(1)}, f32[4096]{0:T(1024)}, u32[]{:S(2)}) copy-start(f32[4096]{0:T(1024)} %param.36) | copy-start | bytes 49156
  31.1 51.7 %copy-start.10 = (bf16[4096]{0:T(1024)(128)(2,1)S(1)}, bf16[4096]{0:T(1024)(128)(2,1)}, u32[]{:S(2)}) copy-start(bf16[4096]{0:T(1024)(128)(2,1)} %param.37) | copy-start | bytes 24580
  109.5 6.4 %collective-permute-start = (bf16[16,96,128]{2,1,0:T(8,128)(2,1)S(1)}, bf16[16,96,128]{2,1,0:T(8,128)(2,1)S(1)}, u32[]{:S(2)}, u32[]{:S(2)}) collective-permute-start(bf16[16,96,128]{2,1,0:T(8,128)(2,1)S(1)} %slice.9), channel_id=1, source_target_pairs={{0,1},{1,0},{2,3},{3,2},{4,5},{5,4},{6,7},{7,6},{8,9},{9,8},{10,11... | collective-permute-start | bytes 1179656 | tf_op jit(solution)/shard_map/ppermute | solution.py:564
  112.3 14.9 %all-to-all-start.6 = ((bf16[16,32,512]{2,1,0:T(8,128)(2,1)}), bf16[16,32,512]{2,1,0:T(8,128)(2,1)S(1)}, u32[]{:S(2)}, u32[]{:S(2)}) async-start(bf16[16,32,512]{2,1,0:T(8,128)(2,1)} %shard_map.252), calls=%async_computation.6 | async-start | bytes 1048576 | tf_op jit(solution)/shard_map/all_to_all | solution.py:35
  115.9 11.3 %copy-start.1 = (bf16[512,256]{1,0:T(8,128)(2,1)S(1)}, bf16[512,256]{1,0:T(8,128)(2,1)}, u32[]{:S(2)}) copy-start(bf16[512,256]{1,0:T(8,128)(2,1)} %w_ref.1) | copy-start | bytes 786436
  121.6 5.6 %collective-permute-start.1 = (bf16[16,96,128]{2,1,0:T(8,128)(2,1)}, bf16[16,96,128]{2,1,0:T(8,128)(2,1)S(1)}, u32[]{:S(2)}, u32[]{:S(2)}) collective-permute-start(bf16[16,96,128]{2,1,0:T(8,128)(2,1)} %get-tuple-element.61), channel_id=1, source_target_pairs={{0,1},{1,0},{2,3},{3,2},{4,5},{5,4},{6,7},{7,6},{8,9},{9,8},{10,11... | collective-permute-start | bytes 1179656 | tf_op jit(solution)/shard_map/ppermute | solution.py:571

commit v4 on v3

--- a/solution.py
+++ b/solution.py
@@ -22,6 +22,10 @@
     return pltpu.with_memory_space_constraint(x, pltpu.HBM)
 
 
+def in_vmem(x):
+    return pltpu.with_memory_space_constraint(x, pltpu.VMEM)
+
+
 def grant(mib):
     return pltpu.CompilerParams(vmem_limit_bytes=mib * 1024 * 1024)
 
@@ -35,8 +39,17 @@
     return lax.all_to_all(parts, axis, 0, 0, tiled=True)
 
 
-def copies(shard, axis):
-    return swap(jnp.broadcast_to(shard[None], (lax.axis_size(axis), *shard.shape)), axis)
+CHIPS = TP // 2
+ALONG_Z = [[2 * z + core for z in range(CHIPS)] for core in range(2)]
+CORES = [(t, t ^ 1) for t in range(TP)]
+
+
+def swap_z(parts):
+    return lax.all_to_all(parts, "tp", 0, 0, tiled=True, axis_index_groups=ALONG_Z)
+
+
+def from_core(x):
+    return lax.ppermute(x, "tp", CORES)
 
 
 def mm(a, b):
@@ -171,7 +184,7 @@
 STEP = 8
 
 
-def cell_kernel(p_ref, scale_ref, write_ref, extra_ref, norm_ref, old_ref, mixed_ref, new_norm_ref, new_hbm, numer, new_ref, done):
+def cell_kernel(p_ref, scale_ref, write_ref, extra_ref, norm_ref, old_ref, mixed_ref, new_norm_ref, new_ref, numer):
     proj = []
     for i in range(4):
         lanes = slice(i * HEAD, (i + 1) * HEAD)
@@ -183,7 +196,6 @@
     wkey = write_ref[...] * (key * HEAD ** (-0.5))
     new_norm = norm_ref[...] + wkey
     new_norm_ref[...] = new_norm
-    moves = []
     for step in range(ROWS // STEP):
         here = slice(step * STEP, (step + 1) * STEP)
         query_t, wkey_t = query[here].T, wkey[here].T
@@ -192,8 +204,6 @@
             new = old_ref[row] + wkey_t[:, j : j + 1] * value[row : row + 1]
             new_ref[row, 0] = new
             numer[row : row + 1, :] = jnp.sum(query_t[:, j : j + 1] * new, axis=0, keepdims=True)
-        moves.append(pltpu.make_async_copy(new_ref.at[pl.ds(step * STEP, STEP)], new_hbm.at[pl.ds(step * STEP, STEP)], done.at[step]))
-        moves[-1].start()
     denom = jnp.sum(query * new_norm, axis=1, keepdims=True)
     out = numer[...] / jnp.maximum(jnp.abs(denom), 1.0)
     mixed = (jax.nn.sigmoid(outgate) * out).astype(BF)
@@ -201,8 +211,6 @@
     for e in range(EP):
         mixed_ref[e, :ROWS] = mixed
         mixed_ref[e, ROWS:] = extra
-    for move in moves:
-        move.wait()
 
 
 def cell(parts, scale, write, extra, norm, old):
@@ -210,27 +218,57 @@
         cell_kernel,
         out_shape=(
             jax.ShapeDtypeStruct((EP, ROWS + 8, HEAD), BF),
-            jax.ShapeDtypeStruct((ROWS, HEAD), F32),
-            jax.ShapeDtypeStruct((ROWS, 1, HEAD, HEAD), F32),
+            pltpu.VMEM((ROWS, HEAD), F32),
+            pltpu.VMEM((ROWS, 1, HEAD, HEAD), F32),
         ),
         in_specs=[VMEM] * 6,
-        out_specs=(VMEM, VMEM, HBM),
-        scratch_shapes=[
-            pltpu.VMEM((ROWS, HEAD), F32),
-            pltpu.VMEM((ROWS, 1, HEAD, HEAD), F32),
-            pltpu.SemaphoreType.DMA((ROWS // STEP,)),
-        ],
+        out_specs=(VMEM,) * 3,
+        scratch_shapes=[pltpu.VMEM((ROWS, HEAD), F32)],
         compiler_params=grant(8),
     )(parts, scale, write, extra, norm, old)
 
 
+def proj_kernel(me_ref, x_ref, w_ref, mine_ref, sent_ref, out):
+    core = me_ref[1] % 2
+    out[...] = mm(x_ref[:, :ROWS, :].reshape(ALL, HEAD), w_ref[...])
+    for z in range(CHIPS):
+        mine_ref[z] = out[pl.ds(pl.multiple_of((2 * z + core) * ROWS, ROWS), ROWS), :].astype(BF)
+        sent_ref[z] = out[pl.ds(pl.multiple_of((2 * z + 1 - core) * ROWS, ROWS), ROWS), :].astype(BF)
+
+
+def proj(me, mixed, w):
+    part = jax.ShapeDtypeStruct((CHIPS, ROWS, COLS), BF)
+    return pl.pallas_call(
+        proj_kernel,
+        out_shape=(part, part),
+        in_specs=[SMEM, VMEM, VMEM],
+        out_specs=(VMEM, VMEM),
+        scratch_shapes=[pltpu.VMEM((ALL, COLS), F32)],
+        compiler_params=grant(4),
+    )(me, mixed, w)
+
+
+def join_kernel(x_ref, y_ref, o_ref):
+    o_ref[...] = (x_ref[...].astype(F32) + y_ref[...].astype(F32)).astype(BF)
+
+
+def join(x, y):
+    return pl.pallas_call(
+        join_kernel,
+        out_shape=jax.ShapeDtypeStruct(x.shape, BF),
+        in_specs=[VMEM, VMEM],
+        out_specs=VMEM,
+        compiler_params=grant(2),
+    )(x, y)
+
+
 def settle_kernel(p_ref, base_ref, o_ref):
     total = p_ref[0].astype(F32)
-    for t in range(1, TP):
-        total = total + p_ref[t].astype(F32)
+    for z in range(1, CHIPS):
+        total = total + p_ref[z].astype(F32)
     out = (base_ref[...].astype(F32) + total).astype(BF)
-    for t in range(TP):
-        o_ref[t] = out
+    for z in range(CHIPS):
+        o_ref[z] = out
 
 
 def settle(parts, base):
@@ -239,7 +277,7 @@
         out_shape=jax.ShapeDtypeStruct(parts.shape, BF),
         in_specs=[VMEM, VMEM],
         out_specs=VMEM,
-        compiler_params=grant(4),
+        compiler_params=grant(2),
     )(parts, base)
 
 
@@ -248,8 +286,19 @@
     return high, x - high
 
 
-def feed_kernel(t_ref, r_ref, gain_ref, branch_ref, mix_ref, gate_ref, up_ref, o_ref):
-    resid = r_ref[...].reshape(ALL, COLS)
+def feed_kernel(
+    t_ref, r_ref, s_ref, gain_ref, branch_ref, mix_ref, gate_ref, up_ref, new_ref, norm_ref, o_ref, new_hbm, norm_hbm, whole, done,
+):
+    stores = [
+        pltpu.make_async_copy(new_ref, new_hbm, done.at[0]), pltpu.make_async_copy(norm_ref, norm_hbm, done.at[1])
+    ]
+    for store in stores:
+        store.start()
+    core = t_ref[1] % 2
+    for z in range(CHIPS):
+        whole[2 * z + core] = r_ref[z]
+        whole[2 * z + 1 - core] = s_ref[z]
+    resid = whole[...].reshape(ALL, COLS)
     wide = resid.astype(F32)
     gained = (wide * my_columns(gain_ref, t_ref)).astype(BF)
     for half, w in enumerate((gate_ref, up_ref)):
@@ -296,16 +345,23 @@
             member = (first == x * 8) | (second == x * 8)
             picked = mm(jnp.where(member, 1.0, 0.0).astype(BF), source).astype(BF)
             o_ref[x, half * half_rows : (half + 1) * half_rows, :] = picked
-
-
-def feed(me, resid, gain, branch, mix, gate, up):
+    for store in stores:
+        store.wait()
+
+
+def feed(me, resid, more, gain, branch, mix, gate, up, new_matrix, new_norm):
     return pl.pallas_call(
         feed_kernel,
-        out_shape=jax.ShapeDtypeStruct((EP, PACKED, 128), BF),
-        in_specs=[SMEM] + [VMEM] * 6,
-        out_specs=VMEM,
+        out_shape=(
+            jax.ShapeDtypeStruct((EP, PACKED, 128), BF),
+            jax.ShapeDtypeStruct(new_matrix.shape, F32),
+            jax.ShapeDtypeStruct(new_norm.shape, F32),
+        ),
+        in_specs=[SMEM] + [VMEM] * 9,
+        out_specs=(VMEM, HBM, HBM),
+        scratch_shapes=[pltpu.VMEM((EP, ROWS, COLS), BF), pltpu.SemaphoreType.DMA((2,))],
         compiler_params=grant(14),
-    )(me, resid, gain, branch, mix, gate, up)
+    )(me, resid, more, gain, branch, mix, gate, up, in_vmem(new_matrix), in_vmem(new_norm))
 
 
 def over_peers(ref, at, size):
@@ -462,7 +518,7 @@
     )(hidden, w, rows, more)
 
 
-def gather_kernel(me_ref, table_ref, branch_ref, r_ref, o_ref, dense):
+def gather_kernel(me_ref, table_ref, branch_ref, r_ref, mine_ref, sent_ref, dense, out):
     for h in range(2):
         for e in range(EP):
             at = (h * EP + e) * ROWS
@@ -476,23 +532,28 @@
             total = total + table_ref[2 + k, r] * r_ref[code // 8, pl.ds(at, EP), :].astype(F32)
         total = jnp.where(mine, jnp.concatenate([total, total], axis=0), 0.0)
         total = total + branch_ref[r : r + 1, :] * dense[pl.ds(r, CHUNKS, stride=ROWS), :]
-        o_ref[r // 2, (r % 2) * CHUNKS : (r % 2 + 1) * CHUNKS, :] = total.astype(BF)
+        out[r // 2, (r % 2) * CHUNKS : (r % 2 + 1) * CHUNKS, :] = total
+    core = me_ref[1] % 2
+    for z in range(CHIPS):
+        mine_ref[z] = out[2 * z + core].astype(BF)
+        sent_ref[z] = out[2 * z + 1 - core].astype(BF)
 
 
 def gather(me, table, branch, returned):
+    part = jax.ShapeDtypeStruct((CHIPS, 2 * CHUNKS, 128), BF)
     return pl.pallas_call(
         gather_kernel,
-        out_shape=jax.ShapeDtypeStruct((TP, 2 * CHUNKS, 128), BF),
+        out_shape=(part, part),
         in_specs=[SMEM, SMEM, VMEM, VMEM],
-        out_specs=VMEM,
-        scratch_shapes=[pltpu.VMEM((CHUNKS * ROWS, 128), F32)],
+        out_specs=(VMEM, VMEM),
+        scratch_shapes=[pltpu.VMEM((CHUNKS * ROWS, 128), F32), pltpu.VMEM((TP, 2 * CHUNKS, 128), F32)],
         compiler_params=grant(6),
     )(me, table, branch, returned)
 
 
 def finish_kernel(p_ref, kept_ref, o_ref, turned):
     total = p_ref[0].astype(F32)
-    for t in range(1, TP):
+    for t in range(1, CHIPS):
         total = total + p_ref[t].astype(F32)
     total = total + kept_ref[...].astype(F32)
     for r in range(2):
@@ -500,7 +561,7 @@
             at = r * CHUNKS + h * EP
             turned[pl.ds(r * CHUNKS + h, EP, stride=2), :] = total[at : at + EP]
     out = turned[...].astype(BF)
-    for t in range(TP):
+    for t in range(CHIPS):
         o_ref[t] = out
 
 
@@ -513,6 +574,27 @@
         scratch_shapes=[pltpu.VMEM((2 * CHUNKS, 128), F32)],
         compiler_params=grant(4),
     )(parts, kept)
+
+
+def place_kernel(me_ref, x_ref, y_ref, o_ref, rows):
+    core = me_ref[1] % 2
+    size = 2 * CHUNKS
+    for z in range(CHIPS):
+        rows[pl.ds(pl.multiple_of((2 * z + core) * size, size), size), :] = x_ref[z].astype(F32)
+        rows[pl.ds(pl.multiple_of((2 * z + 1 - core) * size, size), size), :] = y_ref[z].astype(F32)
+    for c in range(CHUNKS):
+        o_ref[:, c * 128 : (c + 1) * 128] = rows[pl.ds(c, ROWS, stride=CHUNKS), :].astype(BF)
+
+
+def place(me, mine, other):
+    return pl.pallas_call(
+        place_kernel,
+        out_shape=jax.ShapeDtypeStruct((ROWS, WIDTH), BF),
+        in_specs=[SMEM, VMEM, VMEM],
+        out_specs=VMEM,
+        scratch_shapes=[pltpu.VMEM((ROWS * CHUNKS, 128), F32)],
+        compiler_params=grant(4),
+    )(me, mine, other)
 
 
 def on_device(
@@ -556,26 +638,32 @@
     mixed, new_norm, new_matrix = cell(parts, scale, write, extra, norm, old)
     mixed_all = swap(mixed, "ep")
 
-    spread_out = mm(mixed_all[:, :ROWS].reshape(ALL, HEAD), w_proj).astype(BF).reshape(TP, ROWS, COLS)
-    resid = swap(settle(swap(spread_out, "tp"), token_block), "tp")
-
-    packed = swap(feed(me, resid, gains[1], gains[2], mixed_all, dense_gate, dense_up), "ep")
-    cores = [(t, t ^ 1) for t in range(TP)]
-    other = lax.ppermute(packed[:, :ROUTED], "tp", cores)
+    mine, sent = proj(me, mixed_all, w_proj)
+    parts = swap_z(join(mine, from_core(sent)))
+    resid = swap_z(settle(parts, token_block))
+    more = from_core(resid)
+
+    packed, new_matrix, new_norm = feed(
+        me, resid, more, gains[1], gains[2], mixed_all, dense_gate, dense_up, new_matrix, new_norm
+    )
+    packed = swap(packed, "ep")
+    other = from_core(packed[:, :ROUTED])
     hidden = hidden_units(me, packed)
     hidden_all = swap(hidden, "ep")
 
     _, packed, other = lax.optimization_barrier((hidden, packed, other))
     branch, kept = sides(me, packed)
     rows_out, rows_sent = expert(me, packed, other, gains[1], expert_gate, expert_up, expert_down)
-    more = lax.ppermute(rows_sent, "tp", cores)
+    more = from_core(rows_sent)
     hidden_all, rows_out, more, branch, kept, new_max, new_norm, table = lax.optimization_barrier(
         (hidden_all, rows_out, more, branch, kept, new_max, new_norm, table)
     )
 
     returned = swap(down(hidden_all, dense_down, rows_out, more), "ep")
-    parts = swap(gather(me, table, branch, returned), "tp")
-    layer_out = swap(finish(parts, kept), "tp").reshape(ROWS, WIDTH)
+    mine, sent = gather(me, table, branch, returned)
+    parts = swap_z(join(mine, from_core(sent)))
+    done = swap_z(finish(parts, kept))
+    layer_out = place(me, done, from_core(done))
     new_max = new_max.T
     return (layer_out, new_matrix, new_norm[:, None], new_max)
 

time: 176 us -> 170 us (0.966)
  blocking collectives: 131 us -> 109 us
  starting transfers between devices: 12.4 us -> 25.8 us
  waiting for transfers between devices: 9.2 us -> 13.9 us
    all_to_all x8 -> x4, blocking collectives: 131 us -> 61.1 us  [swap(): return lax.all_to_all(parts, axis, 0, 0, tiled=True)]
    all_to_all x0 -> x4, blocking collectives: none -> 47.4 us  [swap_z(): lax.all_to_all(parts, 'tp', 0, 0, tiled=True, axis_index_groups=ALONG_Z)]
    ppermute x2 -> x6, starting transfers between devices: 1.28 us -> 14.6 us  [from_core(): return lax.ppermute(x, 'tp', CORES)]
    ppermute x2 -> x6, waiting for transfers between devices: 0.01 us -> 3.95 us  [from_core(): return lax.ppermute(x, 'tp', CORES)]
    pallas_call x2 -> x6, Pallas kernels: 2.97 us -> 5.53 us  [the longest x1 1.9 us: feed(): pl.pallas_call(feed_kernel, out_shape=(jax.ShapeDtypeStruct((EP, PACKED,...]
  transfers between devices with their start and end apart: 4 -> 8, of which waited for: 2 -> 6; matrix products, arithmetic and copies ran while one was open for 0% -> 0% of each run, Pallas kernels for 6% -> 6%
where the time goes in v4:
time: 170 us
  blocking collectives  109 us (64%)
  starting transfers between devices  25.8 us (15%)
  Pallas kernels  20.4 us (12%)
  waiting for transfers between devices  13.9 us (8%)
    all_to_all x4, blocking collectives, swap(): return lax.all_to_all(parts, axis, 0, 0, tiled=True)  61.1 us
    all_to_all x4, blocking collectives, swap_z(): lax.all_to_all(parts, 'tp', 0, 0, tiled=True, axis_index_groups=ALONG_Z)  47.4 us
    ppermute x6, starting transfers between devices, from_core(): return lax.ppermute(x, 'tp', CORES)  14.6 us
    all_to_all x2, starting transfers between devices, swap(): return lax.all_to_all(parts, axis, 0, 0, tiled=True)  11.2 us
    all_to_all x2, waiting for transfers between devices, swap(): return lax.all_to_all(parts, axis, 0, 0, tiled=True)  9.94 us
    pallas_call x1, Pallas kernels, expert(): pl.pallas_call(expert_kernel, out_shape=(rows, rows), in_specs=[SMEM, VME...  4.96 us
    ppermute x6, waiting for transfers between devices, from_core(): return lax.ppermute(x, 'tp', CORES)  3.95 us
  transfers between devices with their start and end apart: 8, of which 6 were waited for; matrix products, arithmetic and copies ran while one was open for 0% of the time, Pallas kernels for 6%

profile of v4, /device:TPU:1, one launch (start us, length us, event | category | flops | bytes accessed | tf_op | source)
XLA Modules:
  0.0 169.5 jit_solution(8421656422651370809)
XLA Ops:
  0.7 1.7 %shard_map.246 = bf16[16,32,256]{2,1,0:T(8,128)(2,1)} custom-call(bf16[32,4096]{1,0:T(8,128)(2,1)} %refs_0_.1), custom_call_target="tpu_custom_call" | custom-call | tf_op jit(solution)/shard_map/pallas_call | solution.py:80
  2.4 7.6 %all-to-all-start = ((bf16[16,32,256]{2,1,0:T(8,128)(2,1)}), bf16[16,32,256]{2,1,0:T(8,128)(2,1)S(1)}, u32[]{:S(2)}, u32[]{:S(2)}) async-start(bf16[16,32,256]{2,1,0:T(8,128)(2,1)} %shard_map.246), calls=%async_computation | async-start | bytes 524288 | tf_op jit(solution)/shard_map/all_to_all | solution.py:39
  10.1 3.0 %shard_map.247 = (f32[32,128]{1,0:T(8,128)S(1)}, f32[32,128]{1,0:T(8,128)S(1)}, f32[1,32]{1,0:T(1,128)}, bf16[8,128]{1,0:T(8,128)(2,1)S(1)}, f32[4,32]{1,0:T(4,1...) custom-call(s32[2]{0:T(128)S(1)} %pad_add_fusion.me_ref.t_ref, bf16[32,4096]{1,0:T(8,128)(2,1)} %refs_0_.1, ...), custom_call_target="tpu_custom_call" | custom-call | tf_op jit(solution)/shard_map/pallas_call | solution.py:147
  13.2 4.4 %all-to-all-done.x_ref = bf16[16,32,256]{2,1,0:T(8,128)(2,1)S(1)} async-done(((bf16[16,32,256]{2,1,0:T(8,128)(2,1)}), bf16[16,32,256]{2,1,0:T(8,128)(2,1)S(1)}, u32[]{:S(2)}, u32[]{:S(2)}) %all-to-all-start) | async-done | bytes 262176 | tf_op jit(solution)/shard_map/all_to_all | solution.py:39
  18.6 12.7 %all_to_all.50.p_ref = bf16[16,32,512]{2,1,0:T(8,128)(2,1)S(1)} all-to-all(bf16[16,32,512]{2,1,0:T(8,128)(2,1)S(1)} %get-tuple-element.55), channel_id=1, replica_groups=mesh['ep'=16,'tp'=16] {'ep'}, dimensions={0} | all-to-all | bytes 1048576 | tf_op jit(solution)/shard_map/all_to_all | solution.py:39
  31.2 1.5 shard_map.249
  32.8 9.6 %all_to_all.51.x_ref.mix_ref = bf16[16,40,128]{2,1,0:T(8,128)(2,1)S(1)} all-to-all(bf16[16,40,128]{2,1,0:T(8,128)(2,1)S(1)} %get-tuple-element.61), channel_id=1, replica_groups=mesh['ep'=16,'tp'=16] {'ep'}, dimensions={0} | all-to-all | bytes 327680 | tf_op jit(solution)/shard_map/all_to_all | solution.py:39
  43.2 4.5 %collective-permute-start = (bf16[8,32,256]{2,1,0:T(8,128)(2,1)S(1)}, bf16[8,32,256]{2,1,0:T(8,128)(2,1)S(1)}, u32[]{:S(2)}, u32[]{:S(2)}) collective-permute-start(bf16[8,32,256]{2,1,0:T(8,128)(2,1)S(1)} %get-tuple-element.63), channel_id=1, source_target_pairs={{0,1},{1,0},{2,3},{3,2},{4,5},{5,4},{6,7},{7,6},{8,9},{9,8},{10,11... | collective-permute-start | bytes 393224 | tf_op jit(solution)/shard_map/ppermute | solution.py:52
  48.7 15.9 %all_to_all.52.p_ref = bf16[8,32,256]{2,1,0:T(8,128)(2,1)S(1)} all-to-all(bf16[8,32,256]{2,1,0:T(8,128)(2,1)S(1)} %shard_map.251), channel_id=1, replica_groups={{0,2,4,6,8,10,12,14},{1,3,5,7,9,11,13,15},{16,18,20,22,24,26,28,30},{17..., dimensions={0} | all-to-all | bytes 262144 | tf_op jit(solution)/shard_map/all_to_all | solution.py:48
  64.6 10.4 %all_to_all.53.r_ref = bf16[8,32,256]{2,1,0:T(8,128)(2,1)S(1)} all-to-all(bf16[8,32,256]{2,1,0:T(8,128)(2,1)S(1)} %shard_map.252), channel_id=1, replica_groups={{0,2,4,6,8,10,12,14},{1,3,5,7,9,11,13,15},{16,18,20,22,24,26,28,30},{17..., dimensions={0} | all-to-all | bytes 262144 | tf_op jit(solution)/shard_map/all_to_all | solution.py:48
  75.0 3.2 %collective-permute-start.1 = (bf16[8,32,256]{2,1,0:T(8,128)(2,1)S(1)}, bf16[8,32,256]{2,1,0:T(8,128)(2,1)S(1)}, u32[]{:S(2)}, u32[]{:S(2)}) collective-permute-start(bf16[8,32,256]{2,1,0:T(8,128)(2,1)S(1)} %all_to_all.53.r_ref), channel_id=1, source_target_pairs={{0,1},{1,0},{2,3},{3,2},{4,5},{5,4},{6,7},{7,6},{8,9},{9,8},{10,11... | collective-permute-start | bytes 393224 | tf_op jit(solution)/shard_map/ppermute | solution.py:52
  79.2 1.9 %shard_map.253 = (bf16[16,368,128]{2,1,0:T(8,128)(2,1)S(1)}, f32[32,1,128,128]{3,2,1,0:T(8,128)}, f32[32,128]{1,0:T(8,128)}) custom-call(s32[2]{0:T(128)S(1)} %pad_add_fusion.me_ref.t_ref, bf16[8,32,256]{2,1,0:T(8,128)(2,1)S(1)} %all_to_all.53.r_ref, bf16[8,32,256]{2,1,0:T(8,128)(2,1)S(1)} %collective-permute-done.1.s_ref, f32[1,4096]{1,0:T(1,128)S(1)} %bitcast.15, ...), custom_call_target="tpu_custom_call" | custom-call | tf_op jit(solution)/shard_map/pallas_call | solution.py:353
  81.1 24.0 %all_to_all.54.p_ref.x_ref = bf16[16,368,128]{2,1,0:T(8,128)(2,1)S(1)} all-to-all(bf16[16,368,128]{2,1,0:T(8,128)(2,1)S(1)} %get-tuple-element.69), channel_id=1, replica_groups=mesh['ep'=16,'tp'=16] {'ep'}, dimensions={0} | all-to-all | bytes 3014656 | tf_op jit(solution)/shard_map/all_to_all | solution.py:39
  105.1 1.8 %collective-permute-start.2 = (bf16[16,96,128]{2,1,0:T(8,128)(2,1)S(1)}, bf16[16,96,128]{2,1,0:T(8,128)(2,1)S(1)}, u32[]{:S(2)}, u32[]{:S(2)}) collective-permute-start(bf16[16,96,128]{2,1,0:T(8,128)(2,1)S(1)} %slice.4), channel_id=1, source_target_pairs={{0,1},{1,0},{2,3},{3,2},{4,5},{5,4},{6,7},{7,6},{8,9},{9,8},{10,11... | collective-permute-start | bytes 1179656 | tf_op jit(solution)/shard_map/ppermute | solution.py:52
  107.0 1.6 shard_map.254
  108.6 3.6 %all-to-all-start.6 = ((bf16[16,32,512]{2,1,0:T(8,128)(2,1)}), bf16[16,32,512]{2,1,0:T(8,128)(2,1)S(1)}, u32[]{:S(2)}, u32[]{:S(2)}) async-start(bf16[16,32,512]{2,1,0:T(8,128)(2,1)} %shard_map.254), calls=%async_computation.6 | async-start | bytes 1048576 | tf_op jit(solution)/shard_map/all_to_all | solution.py:39
  112.2 5.0 %shard_map.255 = (bf16[16,96,128]{2,1,0:T(8,128)(2,1)S(1)}, bf16[16,96,128]{2,1,0:T(8,128)(2,1)S(1)}) custom-call(s32[2]{0:T(128)S(1)} %pad_add_fusion.me_ref.t_ref, bf16[16,368,128]{2,1,0:T(8,128)(2,1)S(1)} %all_to_all.54.p_ref.x_ref, bf16[16,96,128]{2,1,0:T(8,128)(2,1)S(1)} %collective-permute-done.2.y_ref, f32[1,4096]{1,0:T(1,128)S(1)} %bitcast.16, ...), custom_call_target="tpu_custom_call" | custom-call | tf_op jit(solution)/shard_map/pallas_call | solution.py:486
  117.9 5.5 %all-to-all-done.6.h_ref = bf16[16,32,512]{2,1,0:T(8,128)(2,1)S(1)} async-done(((bf16[16,32,512]{2,1,0:T(8,128)(2,1)}), bf16[16,32,512]{2,1,0:T(8,128)(2,1)S(1)}, u32[]{:S(2)}, u32[]{:S(2)}) %all-to-all-start.6) | async-done | bytes 524320 | tf_op jit(solution)/shard_map/all_to_all | solution.py:39
  123.8 14.8 %all_to_all.55.r_ref = bf16[16,160,128]{2,1,0:T(8,128)(2,1)S(1)} all-to-all(bf16[16,160,128]{2,1,0:T(8,128)(2,1)S(1)} %shard_map.257), channel_id=1, replica_groups=mesh['ep'=16,'tp'=16] {'ep'}, dimensions={0} | all-to-all | bytes 1310720 | tf_op jit(solution)/shard_map/all_to_all | solution.py:39
  139.8 2.2 %collective-permute-start.4 = (bf16[8,64,128]{2,1,0:T(8,128)(2,1)S(1)}, bf16[8,64,128]{2,1,0:T(8,128)(2,1)S(1)}, u32[]{:S(2)}, u32[]{:S(2)}) collective-permute-start(bf16[8,64,128]{2,1,0:T(8,128)(2,1)S(1)} %get-tuple-element.85), channel_id=1, source_target_pairs={{0,1},{1,0},{2,3},{3,2},{4,5},{5,4},{6,7},{7,6},{8,9},{9,8},{10,11... | collective-permute-start | bytes 393224 | tf_op jit(solution)/shard_map/ppermute | solution.py:52
  143.0 10.8 %all_to_all.56.p_ref = bf16[8,64,128]{2,1,0:T(8,128)(2,1)S(1)} all-to-all(bf16[8,64,128]{2,1,0:T(8,128)(2,1)S(1)} %shard_map.259), channel_id=1, replica_groups={{0,2,4,6,8,10,12,14},{1,3,5,7,9,11,13,15},{16,18,20,22,24,26,28,30},{17..., dimensions={0} | all-to-all | bytes 262144 | tf_op jit(solution)/shard_map/all_to_all | solution.py:48
  153.9 10.3 %all_to_all.57.x_ref = bf16[8,64,128]{2,1,0:T(8,128)(2,1)S(1)} all-to-all(bf16[8,64,128]{2,1,0:T(8,128)(2,1)S(1)} %shard_map.260), channel_id=1, replica_groups={{0,2,4,6,8,10,12,14},{1,3,5,7,9,11,13,15},{16,18,20,22,24,26,28,30},{17..., dimensions={0} | all-to-all | bytes 262144 | tf_op jit(solution)/shard_map/all_to_all | solution.py:48
  164.2 2.8 %collective-permute-start.5 = (bf16[8,64,128]{2,1,0:T(8,128)(2,1)S(1)}, bf16[8,64,128]{2,1,0:T(8,128)(2,1)S(1)}, u32[]{:S(2)}, u32[]{:S(2)}) collective-permute-start(bf16[8,64,128]{2,1,0:T(8,128)(2,1)S(1)} %all_to_all.57.x_ref), channel_id=1, source_target_pairs={{0,1},{1,0},{2,3},{3,2},{4,5},{5,4},{6,7},{7,6},{8,9},{9,8},{10,11... | collective-permute-start | bytes 393224 | tf_op jit(solution)/shard_map/ppermute | solution.py:52
  167.9 1.6 shard_map.261
  (40 shorter events, 8.3 us)
Async XLA Ops:
  0.6 16.9 %copy-start.4 = (f32[4096]{0:T(1024)S(1)}, f32[4096]{0:T(1024)}, u32[]{:S(2)}) copy-start(f32[4096]{0:T(1024)} %param.27) | copy-start | bytes 49156
  0.6 16.9 %copy-start.8 = (bf16[256,128]{1,0:T(8,128)(2,1)S(1)}, bf16[256,128]{1,0:T(8,128)(2,1)}, u32[]{:S(2)}) copy-start(bf16[256,128]{1,0:T(8,128)(2,1)} %g_ref.1) | copy-start | bytes 196612
  0.7 16.9 %copy-start.7 = (bf16[256,128]{1,0:T(8,128)(2,1)S(1)}, bf16[256,128]{1,0:T(8,128)(2,1)}, u32[]{:S(2)}) copy-start(bf16[256,128]{1,0:T(8,128)(2,1)} %v_ref.1) | copy-start | bytes 196612
  0.7 16.9 %copy-start.6 = (bf16[256,128]{1,0:T(8,128)(2,1)S(1)}, bf16[256,128]{1,0:T(8,128)(2,1)}, u32[]{:S(2)}) copy-start(bf16[256,128]{1,0:T(8,128)(2,1)} %k_ref.1) | copy-start | bytes 196612
  0.7 16.9 %copy-start.5 = (bf16[256,128]{1,0:T(8,128)(2,1)S(1)}, bf16[256,128]{1,0:T(8,128)(2,1)}, u32[]{:S(2)}) copy-start(bf16[256,128]{1,0:T(8,128)(2,1)} %q_ref.1) | copy-start | bytes 196612
  2.4 15.1 %all-to-all-start = ((bf16[16,32,256]{2,1,0:T(8,128)(2,1)}), bf16[16,32,256]{2,1,0:T(8,128)(2,1)S(1)}, u32[]{:S(2)}, u32[]{:S(2)}) async-start(bf16[16,32,256]{2,1,0:T(8,128)(2,1)} %shard_map.246), calls=%async_computation | async-start | bytes 524288 | tf_op jit(solution)/shard_map/all_to_all | solution.py:39
  18.6 23.8 %copy-start.9 = (bf16[128,256]{1,0:T(8,128)(2,1)S(1)}, bf16[128,256]{1,0:T(8,128)(2,1)}, u32[]{:S(2)}) copy-start(bf16[128,256]{1,0:T(8,128)(2,1)} %w_ref.2) | copy-start | bytes 196612
  31.2 47.9 %copy-start = (bf16[256,512]{1,0:T(8,128)(2,1)S(1)}, bf16[256,512]{1,0:T(8,128)(2,1)}, u32[]{:S(2)}) copy-start(bf16[256,512]{1,0:T(8,128)(2,1)} %gate_ref.1) | copy-start | bytes 786436
  31.2 47.9 %copy-start.1 = (bf16[256,512]{1,0:T(8,128)(2,1)S(1)}, bf16[256,512]{1,0:T(8,128)(2,1)}, u32[]{:S(2)}) copy-start(bf16[256,512]{1,0:T(8,128)(2,1)} %up_ref.1) | copy-start | bytes 786436
  31.2 47.9 %copy-start.3 = (f32[4096]{0:T(1024)S(1)}, f32[4096]{0:T(1024)}, u32[]{:S(2)}) copy-start(f32[4096]{0:T(1024)} %param.36) | copy-start | bytes 49156
  31.2 47.9 %copy-start.10 = (bf16[4096]{0:T(1024)(128)(2,1)S(1)}, bf16[4096]{0:T(1024)(128)(2,1)}, u32[]{:S(2)}) copy-start(bf16[4096]{0:T(1024)(128)(2,1)} %param.37) | copy-start | bytes 24580
  43.2 5.5 %collective-permute-start = (bf16[8,32,256]{2,1,0:T(8,128)(2,1)S(1)}, bf16[8,32,256]{2,1,0:T(8,128)(2,1)S(1)}, u32[]{:S(2)}, u32[]{:S(2)}) collective-permute-start(bf16[8,32,256]{2,1,0:T(8,128)(2,1)S(1)} %get-tuple-element.63), channel_id=1, source_target_pairs={{0,1},{1,0},{2,3},{3,2},{4,5},{5,4},{6,7},{7,6},{8,9},{9,8},{10,11... | collective-permute-start | bytes 393224 | tf_op jit(solution)/shard_map/ppermute | solution.py:52
  75.0 4.1 %collective-permute-start.1 = (bf16[8,32,256]{2,1,0:T(8,128)(2,1)S(1)}, bf16[8,32,256]{2,1,0:T(8,128)(2,1)S(1)}, u32[]{:S(2)}, u32[]{:S(2)}) collective-permute-start(bf16[8,32,256]{2,1,0:T(8,128)(2,1)S(1)} %all_to_all.53.r_ref), channel_id=1, source_target_pairs={{0,1},{1,0},{2,3},{3,2},{4,5},{5,4},{6,7},{7,6},{8,9},{9,8},{10,11... | collective-permute-start | bytes 393224 | tf_op jit(solution)/shard_map/ppermute | solution.py:52
  105.1 7.0 %collective-permute-start.2 = (bf16[16,96,128]{2,1,0:T(8,128)(2,1)S(1)}, bf16[16,96,128]{2,1,0:T(8,128)(2,1)S(1)}, u32[]{:S(2)}, u32[]{:S(2)}) collective-permute-start(bf16[16,96,128]{2,1,0:T(8,128)(2,1)S(1)} %slice.4), channel_id=1, source_target_pairs={{0,1},{1,0},{2,3},{3,2},{4,5},{5,4},{6,7},{7,6},{8,9},{9,8},{10,11... | collective-permute-start | bytes 1179656 | tf_op jit(solution)/shard_map/ppermute | solution.py:52
  108.6 14.9 %all-to-all-start.6 = ((bf16[16,32,512]{2,1,0:T(8,128)(2,1)}), bf16[16,32,512]{2,1,0:T(8,128)(2,1)S(1)}, u32[]{:S(2)}, u32[]{:S(2)}) async-start(bf16[16,32,512]{2,1,0:T(8,128)(2,1)} %shard_map.254), calls=%async_computation.6 | async-start | bytes 1048576 | tf_op jit(solution)/shard_map/all_to_all | solution.py:39
  112.1 11.3 %copy-start.2 = (bf16[512,256]{1,0:T(8,128)(2,1)S(1)}, bf16[512,256]{1,0:T(8,128)(2,1)}, u32[]{:S(2)}) copy-start(bf16[512,256]{1,0:T(8,128)(2,1)} %w_ref.3) | copy-start | bytes 786436
  117.1 6.3 %collective-permute-start.3 = (bf16[16,96,128]{2,1,0:T(8,128)(2,1)S(1)}, bf16[16,96,128]{2,1,0:T(8,128)(2,1)S(1)}, u32[]{:S(2)}, u32[]{:S(2)}) collective-permute-start(bf16[16,96,128]{2,1,0:T(8,128)(2,1)S(1)} %get-tuple-element.73), channel_id=1, source_target_pairs={{0,1},{1,0},{2,3},{3,2},{4,5},{5,4},{6,7},{7,6},{8,9},{9,8},{10,11... | collective-permute-start | bytes 1179656 | tf_op jit(solution)/shard_map/ppermute | solution.py:52
  139.8 3.2 %collective-permute-start.4 = (bf16[8,64,128]{2,1,0:T(8,128)(2,1)S(1)}, bf16[8,64,128]{2,1,0:T(8,128)(2,1)S(1)}, u32[]{:S(2)}, u32[]{:S(2)}) collective-permute-start(bf16[8,64,128]{2,1,0:T(8,128)(2,1)S(1)} %get-tuple-element.85), channel_id=1, source_target_pairs={{0,1},{1,0},{2,3},{3,2},{4,5},{5,4},{6,7},{7,6},{8,9},{9,8},{10,11... | collective-permute-start | bytes 393224 | tf_op jit(solution)/shard_map/ppermute | solution.py:52
  164.2 3.8 %collective-permute-start.5 = (bf16[8,64,128]{2,1,0:T(8,128)(2,1)S(1)}, bf16[8,64,128]{2,1,0:T(8,128)(2,1)S(1)}, u32[]{:S(2)}, u32[]{:S(2)}) collective-permute-start(bf16[8,64,128]{2,1,0:T(8,128)(2,1)S(1)} %all_to_all.57.x_ref), channel_id=1, source_target_pairs={{0,1},{1,0},{2,3},{3,2},{4,5},{5,4},{6,7},{7,6},{8,9},{9,8},{10,11... | collective-permute-start | bytes 393224 | tf_op jit(solution)/shard_map/ppermute | solution.py:52

commit v5 on v4

--- a/solution.py
+++ b/solution.py
@@ -12,12 +12,14 @@
 EP, TP = 16, 16
 ROWS, WIDTH, COLS, HEAD, UNITS, CAP = 32, 4096, 256, 128, 512, 6
 ALL = ROWS * EP
-ROUTED = CAP * EP
+ROUTED = CAP * EP // 2
 SIDE = ROUTED + 8 * ROWS
 PACKED = SIDE + 16
 CHUNKS = WIDTH // 128
 BACK = CAP * EP
 RETURN = BACK + 2 * ROWS
+
+
 def in_hbm(x):
     return pltpu.with_memory_space_constraint(x, pltpu.HBM)
 
@@ -329,22 +331,21 @@
             [side[:, tile * 128 : (tile + 1) * 128], own[g * 8 : (g + 1) * 8]], axis=0
         )
         o_ref[g, SIDE:PACKED, :] = block.astype(BF)
-    half_rows = CAP * EP // 2
-    line = lax.broadcasted_iota(I32, (half_rows, 2 * 128), 0)
+    line = lax.broadcasted_iota(I32, (ROUTED, 2 * 128), 0)
     base = (line // CAP) * 128 + line % CAP
     group = lax.broadcasted_iota(I32, (1, 2 * 128), 1) // ROWS
-    for half in range(2):
-        tiles = []
-        for tile in (2 * half, 2 * half + 1):
-            tiles.append(sum(mix_ref[4 * tile + i, ROWS:, :].astype(F32) for i in range(4)))
-        codes = jnp.concatenate(tiles, axis=1).astype(I32)
-        first = codes[0:1] + group * 128 - base
-        second = codes[1:2] + group * 128 - base
-        source = jnp.where(t_ref[1] % 2 == 0, wide[:, :128], wide[:, 128:])[half * 256 : (half + 1) * 256].astype(BF)
-        for x in range(EP):
-            member = (first == x * 8) | (second == x * 8)
-            picked = mm(jnp.where(member, 1.0, 0.0).astype(BF), source).astype(BF)
-            o_ref[x, half * half_rows : (half + 1) * half_rows, :] = picked
+    start = 8 * ((t_ref[1] // 2) % 2)
+    tiles = []
+    for tile in range(2):
+        tiles.append(sum(mix_ref[start + 4 * tile + i, ROWS:, :].astype(F32) for i in range(4)))
+    codes = jnp.concatenate(tiles, axis=1).astype(I32)
+    first = codes[0:1] + group * 128 - base
+    second = codes[1:2] + group * 128 - base
+    source = jnp.where(core == 0, wide[:, :128], wide[:, 128:])
+    source = jnp.where(start == 0, source[:256], source[256:]).astype(BF)
+    for x in range(EP):
+        member = (first == x * 8) | (second == x * 8)
+        o_ref[x, :ROUTED, :] = mm(jnp.where(member, 1.0, 0.0).astype(BF), source).astype(BF)
     for store in stores:
         store.wait()
 
@@ -455,7 +456,7 @@
         pieces = []
         for e in range(i * PER_STEP, (i + 1) * PER_STEP):
             for h in range(2):
-                x = jnp.where(core == h, x_ref[e, :ROUTED, :].astype(F32), y_ref[e].astype(F32))
+                x = jnp.where(core == h, x_ref[e].astype(F32), y_ref[e].astype(F32))
                 squares += x * x
                 at = (2 * e + h) * 128
                 pieces.append((x * gain_ref[:, at : at + 128]).astype(BF))
@@ -474,11 +475,13 @@
             chunk = i * (LANES // 128) + c
             at = (chunk % 2) * slots * EP + chunk // 2
             turned[pl.ds(at, slots, stride=EP), :] = out[:, c * 128 : (c + 1) * 128]
+    start = 8 * ((me_ref[1] // 2) % 2)
     for g in range(EP):
         mine = pl.multiple_of(core * slots * EP + g * BACK, BACK)
         other = pl.multiple_of((1 - core) * slots * EP + g * BACK, BACK)
-        o_ref[g] = turned[pl.ds(mine, BACK), :].astype(BF)
-        send_ref[g] = turned[pl.ds(other, BACK), :].astype(BF)
+        to = start + g if g < 8 else g - start
+        o_ref[to] = turned[pl.ds(mine, BACK), :].astype(BF)
+        send_ref[to] = turned[pl.ds(other, BACK), :].astype(BF)
 
 
 def expert(me, packed, other, gain, gate, up, down_w):
@@ -647,13 +650,16 @@
         me, resid, more, gains[1], gains[2], mixed_all, dense_gate, dense_up, new_matrix, new_norm
     )
     packed = swap(packed, "ep")
-    other = from_core(packed[:, :ROUTED])
+    quarter = packed[:, :ROUTED]
+    beside = lax.ppermute(quarter, "tp", [(t, t ^ 2) for t in range(TP)])
     hidden = hidden_units(me, packed)
     hidden_all = swap(hidden, "ep")
-
-    _, packed, other = lax.optimization_barrier((hidden, packed, other))
+    _, packed = lax.optimization_barrier((hidden, packed))
     branch, kept = sides(me, packed)
-    rows_out, rows_sent = expert(me, packed, other, gains[1], expert_gate, expert_up, expert_down)
+    pair = jnp.concatenate([quarter, beside], axis=1)
+    other = from_core(pair)
+
+    rows_out, rows_sent = expert(me, pair, other, gains[1], expert_gate, expert_up, expert_down)
     more = from_core(rows_sent)
     hidden_all, rows_out, more, branch, kept, new_max, new_norm, table = lax.optimization_barrier(
         (hidden_all, rows_out, more, branch, kept, new_max, new_norm, table)

time: 170 us -> 174 us (1.024)
  waiting for transfers between devices: 13.9 us -> 17.8 us
  blocking collectives: 109 us -> 107 us
    ppermute x0 -> x1, waiting for transfers between devices: none -> 4.71 us  [on_device(): beside = lax.ppermute(quarter, 'tp', [(t, t ^ 2) for t in range(TP)])]
    all_to_all x4, blocking collectives: 61.1 us -> 59.3 us  [swap(): return lax.all_to_all(parts, axis, 0, 0, tiled=True)]
  transfers between devices with their start and end apart: 8 -> 9, of which waited for: 6 -> 7; matrix products, arithmetic and copies ran while one was open for 0% -> 0% of each run, Pallas kernels for 6% -> 6%
where the time goes in v5:
time: 174 us; the launch traced here: 173 us
  blocking collectives  107 us (61%)
  starting transfers between devices  26.8 us (15%)
  Pallas kernels  21.2 us (12%)
  waiting for transfers between devices  17.8 us (10%)
    all_to_all x4, blocking collectives, swap(): return lax.all_to_all(parts, axis, 0, 0, tiled=True)  59.3 us
    all_to_all x4, blocking collectives, swap_z(): lax.all_to_all(parts, 'tp', 0, 0, tiled=True, axis_index_groups=ALONG_Z)  47.4 us
    ppermute x6, starting transfers between devices, from_core(): return lax.ppermute(x, 'tp', CORES)  15.2 us
    all_to_all x2, starting transfers between devices, swap(): return lax.all_to_all(parts, axis, 0, 0, tiled=True)  11.2 us
    all_to_all x2, waiting for transfers between devices, swap(): return lax.all_to_all(parts, axis, 0, 0, tiled=True)  9.11 us
    pallas_call x1, Pallas kernels, expert(): pl.pallas_call(expert_kernel, out_shape=(rows, rows), in_specs=[SMEM, VME...  5.7 us
    ppermute x1, waiting for transfers between devices, on_device(): beside = lax.ppermute(quarter, 'tp', [(t, t ^ 2) for t in range(TP)])  4.71 us
    ppermute x6, waiting for transfers between devices, from_core(): return lax.ppermute(x, 'tp', CORES)  3.95 us
  transfers between devices with their start and end apart: 9, of which 7 were waited for; matrix products, arithmetic and copies ran while one was open for 0% of the time, Pallas kernels for 6%

profile of v5, /device:TPU:1, one launch (start us, length us, event | category | flops | bytes accessed | tf_op | source)
XLA Modules:
  0.0 173.4 jit_solution(6678419706267348817)
XLA Ops:
  0.7 1.7 shard_map.246
  2.4 7.6 %all-to-all-start = ((bf16[16,32,256]{2,1,0:T(8,128)(2,1)}), bf16[16,32,256]{2,1,0:T(8,128)(2,1)S(1)}, u32[]{:S(2)}, u32[]{:S(2)}) async-start(bf16[16,32,256]{2,1,0:T(8,128)(2,1)} %shard_map.246), calls=%async_computation | async-start | bytes 524288 | tf_op jit(solution)/shard_map/all_to_all | solution.py:41
  10.1 3.0 %shard_map.247 = (f32[32,128]{1,0:T(8,128)S(1)}, f32[32,128]{1,0:T(8,128)S(1)}, f32[1,32]{1,0:T(1,128)}, bf16[8,128]{1,0:T(8,128)(2,1)S(1)}, f32[4,32]{1,0:T(4,1...) custom-call(s32[2]{0:T(128)S(1)} %pad_add_fusion.me_ref.t_ref, bf16[32,4096]{1,0:T(8,128)(2,1)} %refs_0_.1, ...), custom_call_target="tpu_custom_call" | custom-call | tf_op jit(solution)/shard_map/pallas_call | solution.py:149
  13.2 4.4 %all-to-all-done.x_ref = bf16[16,32,256]{2,1,0:T(8,128)(2,1)S(1)} async-done(((bf16[16,32,256]{2,1,0:T(8,128)(2,1)}), bf16[16,32,256]{2,1,0:T(8,128)(2,1)S(1)}, u32[]{:S(2)}, u32[]{:S(2)}) %all-to-all-start) | async-done | bytes 262176 | tf_op jit(solution)/shard_map/all_to_all | solution.py:41
  18.6 12.7 %all_to_all.50.p_ref = bf16[16,32,512]{2,1,0:T(8,128)(2,1)S(1)} all-to-all(bf16[16,32,512]{2,1,0:T(8,128)(2,1)S(1)} %get-tuple-element.54), channel_id=1, replica_groups=mesh['ep'=16,'tp'=16] {'ep'}, dimensions={0} | all-to-all | bytes 1048576 | tf_op jit(solution)/shard_map/all_to_all | solution.py:41
  32.8 9.6 %all_to_all.51.x_ref.mix_ref = bf16[16,40,128]{2,1,0:T(8,128)(2,1)S(1)} all-to-all(bf16[16,40,128]{2,1,0:T(8,128)(2,1)S(1)} %get-tuple-element.60), channel_id=1, replica_groups=mesh['ep'=16,'tp'=16] {'ep'}, dimensions={0} | all-to-all | bytes 327680 | tf_op jit(solution)/shard_map/all_to_all | solution.py:41
  43.2 4.5 %collective-permute-start = (bf16[8,32,256]{2,1,0:T(8,128)(2,1)S(1)}, bf16[8,32,256]{2,1,0:T(8,128)(2,1)S(1)}, u32[]{:S(2)}, u32[]{:S(2)}) collective-permute-start(bf16[8,32,256]{2,1,0:T(8,128)(2,1)S(1)} %get-tuple-element.62), channel_id=1, source_target_pairs={{0,1},{1,0},{2,3},{3,2},{4,5},{5,4},{6,7},{7,6},{8,9},{9,8},{10,11... | collective-permute-start | bytes 393224 | tf_op jit(solution)/shard_map/ppermute | solution.py:54
  48.7 15.9 %all_to_all.52.p_ref = bf16[8,32,256]{2,1,0:T(8,128)(2,1)S(1)} all-to-all(bf16[8,32,256]{2,1,0:T(8,128)(2,1)S(1)} %shard_map.251), channel_id=1, replica_groups={{0,2,4,6,8,10,12,14},{1,3,5,7,9,11,13,15},{16,18,20,22,24,26,28,30},{17..., dimensions={0} | all-to-all | bytes 262144 | tf_op jit(solution)/shard_map/all_to_all | solution.py:50
  64.6 10.4 %all_to_all.53.r_ref = bf16[8,32,256]{2,1,0:T(8,128)(2,1)S(1)} all-to-all(bf16[8,32,256]{2,1,0:T(8,128)(2,1)S(1)} %shard_map.252), channel_id=1, replica_groups={{0,2,4,6,8,10,12,14},{1,3,5,7,9,11,13,15},{16,18,20,22,24,26,28,30},{17..., dimensions={0} | all-to-all | bytes 262144 | tf_op jit(solution)/shard_map/all_to_all | solution.py:50
  75.0 3.2 %collective-permute-start.1 = (bf16[8,32,256]{2,1,0:T(8,128)(2,1)S(1)}, bf16[8,32,256]{2,1,0:T(8,128)(2,1)S(1)}, u32[]{:S(2)}, u32[]{:S(2)}) collective-permute-start(bf16[8,32,256]{2,1,0:T(8,128)(2,1)S(1)} %all_to_all.53.r_ref), channel_id=1, source_target_pairs={{0,1},{1,0},{2,3},{3,2},{4,5},{5,4},{6,7},{7,6},{8,9},{9,8},{10,11... | collective-permute-start | bytes 393224 | tf_op jit(solution)/shard_map/ppermute | solution.py:54
  79.2 2.0 %shard_map.253 = (bf16[16,320,128]{2,1,0:T(8,128)(2,1)S(1)}, f32[32,1,128,128]{3,2,1,0:T(8,128)}, f32[32,128]{1,0:T(8,128)}) custom-call(s32[2]{0:T(128)S(1)} %pad_add_fusion.me_ref.t_ref, bf16[8,32,256]{2,1,0:T(8,128)(2,1)S(1)} %all_to_all.53.r_ref, bf16[8,32,256]{2,1,0:T(8,128)(2,1)S(1)} %collective-permute-done.1.s_ref, f32[1,4096]{1,0:T(1,128)S(1)} %bitcast.15, ...), custom_call_target="tpu_custom_call" | custom-call | tf_op jit(solution)/shard_map/pallas_call | solution.py:354
  81.2 22.2 %all_to_all.54.p_ref = bf16[16,320,128]{2,1,0:T(8,128)(2,1)S(1)} all-to-all(bf16[16,320,128]{2,1,0:T(8,128)(2,1)S(1)} %get-tuple-element.68), channel_id=1, replica_groups=mesh['ep'=16,'tp'=16] {'ep'}, dimensions={0} | all-to-all | bytes 2621440 | tf_op jit(solution)/shard_map/all_to_all | solution.py:41
  103.7 4.7 %collective-permute-done.2 = bf16[16,48,128]{2,1,0:T(8,128)(2,1)S(1)} collective-permute-done((bf16[16,48,128]{2,1,0:T(8,128)(2,1)S(1)}, bf16[16,48,128]{2,1,0:T(8,128)(2,1)S(1)}, u32[]{:S(2)}, u32[]{:S(2)}) %collective-permute-start.2) | collective-permute-done | bytes 196640 | tf_op jit(solution)/shard_map/ppermute | solution.py:654
  108.5 2.4 %collective-permute-start.3 = (bf16[16,96,128]{2,1,0:T(8,128)(2,1)S(1)}, bf16[16,96,128]{2,1,0:T(8,128)(2,1)S(1)}, u32[]{:S(2)}, u32[]{:S(2)}) collective-permute-start(bf16[16,96,128]{2,1,0:T(8,128)(2,1)S(1)} %pad_maximum_fusion.x_ref), channel_id=1, source_target_pairs={{0,1},{1,0},{2,3},{3,2},{4,5},{5,4},{6,7},{7,6},{8,9},{9,8},{10,11... | collective-permute-start | bytes 1179656 | tf_op jit(solution)/shard_map/ppermute | solution.py:54
  110.9 1.6 shard_map.254
  112.5 3.6 %all-to-all-start.6 = ((bf16[16,32,512]{2,1,0:T(8,128)(2,1)}), bf16[16,32,512]{2,1,0:T(8,128)(2,1)S(1)}, u32[]{:S(2)}, u32[]{:S(2)}) async-start(bf16[16,32,512]{2,1,0:T(8,128)(2,1)} %shard_map.254), calls=%async_computation.6 | async-start | bytes 1048576 | tf_op jit(solution)/shard_map/all_to_all | solution.py:41
  116.1 5.7 %shard_map.255 = (bf16[16,96,128]{2,1,0:T(8,128)(2,1)S(1)}, bf16[16,96,128]{2,1,0:T(8,128)(2,1)}) custom-call(s32[2]{0:T(128)S(1)} %pad_add_fusion.me_ref.t_ref, bf16[16,96,128]{2,1,0:T(8,128)(2,1)S(1)} %pad_maximum_fusion.x_ref, bf16[16,96,128]{2,1,0:T(8,128)(2,1)S(1)} %collective-permute-done.3.y_ref, f32[1,4096]{1,0:T(1,128)S(1)} %bitcast.16, ...), custom_call_target="tpu_custom_call" | custom-call | tf_op jit(solution)/shard_map/pallas_call | solution.py:489
  122.6 4.7 %all-to-all-done.6.h_ref = bf16[16,32,512]{2,1,0:T(8,128)(2,1)S(1)} async-done(((bf16[16,32,512]{2,1,0:T(8,128)(2,1)}), bf16[16,32,512]{2,1,0:T(8,128)(2,1)S(1)}, u32[]{:S(2)}, u32[]{:S(2)}) %all-to-all-start.6) | async-done | bytes 524320 | tf_op jit(solution)/shard_map/all_to_all | solution.py:41
  127.6 14.8 %all_to_all.55.r_ref = bf16[16,160,128]{2,1,0:T(8,128)(2,1)S(1)} all-to-all(bf16[16,160,128]{2,1,0:T(8,128)(2,1)S(1)} %shard_map.257), channel_id=1, replica_groups=mesh['ep'=16,'tp'=16] {'ep'}, dimensions={0} | all-to-all | bytes 1310720 | tf_op jit(solution)/shard_map/all_to_all | solution.py:41
  143.6 2.3 %collective-permute-start.5 = (bf16[8,64,128]{2,1,0:T(8,128)(2,1)S(1)}, bf16[8,64,128]{2,1,0:T(8,128)(2,1)S(1)}, u32[]{:S(2)}, u32[]{:S(2)}) collective-permute-start(bf16[8,64,128]{2,1,0:T(8,128)(2,1)S(1)} %get-tuple-element.83), channel_id=1, source_target_pairs={{0,1},{1,0},{2,3},{3,2},{4,5},{5,4},{6,7},{7,6},{8,9},{9,8},{10,11... | collective-permute-start | bytes 393224 | tf_op jit(solution)/shard_map/ppermute | solution.py:54
  146.9 10.8 %all_to_all.56.p_ref = bf16[8,64,128]{2,1,0:T(8,128)(2,1)S(1)} all-to-all(bf16[8,64,128]{2,1,0:T(8,128)(2,1)S(1)} %shard_map.259), channel_id=1, replica_groups={{0,2,4,6,8,10,12,14},{1,3,5,7,9,11,13,15},{16,18,20,22,24,26,28,30},{17..., dimensions={0} | all-to-all | bytes 262144 | tf_op jit(solution)/shard_map/all_to_all | solution.py:50
  157.7 10.3 %all_to_all.57.x_ref = bf16[8,64,128]{2,1,0:T(8,128)(2,1)S(1)} all-to-all(bf16[8,64,128]{2,1,0:T(8,128)(2,1)S(1)} %shard_map.260), channel_id=1, replica_groups={{0,2,4,6,8,10,12,14},{1,3,5,7,9,11,13,15},{16,18,20,22,24,26,28,30},{17..., dimensions={0} | all-to-all | bytes 262144 | tf_op jit(solution)/shard_map/all_to_all | solution.py:50
  168.1 2.8 %collective-permute-start.6 = (bf16[8,64,128]{2,1,0:T(8,128)(2,1)S(1)}, bf16[8,64,128]{2,1,0:T(8,128)(2,1)S(1)}, u32[]{:S(2)}, u32[]{:S(2)}) collective-permute-start(bf16[8,64,128]{2,1,0:T(8,128)(2,1)S(1)} %all_to_all.57.x_ref), channel_id=1, source_target_pairs={{0,1},{1,0},{2,3},{3,2},{4,5},{5,4},{6,7},{7,6},{8,9},{9,8},{10,11... | collective-permute-start | bytes 393224 | tf_op jit(solution)/shard_map/ppermute | solution.py:54
  171.8 1.6 shard_map.261
  (43 shorter events, 10.2 us)
Async XLA Ops:
  0.6 16.9 %copy-start.4 = (f32[4096]{0:T(1024)S(1)}, f32[4096]{0:T(1024)}, u32[]{:S(2)}) copy-start(f32[4096]{0:T(1024)} %param.27) | copy-start | bytes 49156
  0.6 16.9 %copy-start.8 = (bf16[256,128]{1,0:T(8,128)(2,1)S(1)}, bf16[256,128]{1,0:T(8,128)(2,1)}, u32[]{:S(2)}) copy-start(bf16[256,128]{1,0:T(8,128)(2,1)} %g_ref.1) | copy-start | bytes 196612
  0.7 16.9 %copy-start.7 = (bf16[256,128]{1,0:T(8,128)(2,1)S(1)}, bf16[256,128]{1,0:T(8,128)(2,1)}, u32[]{:S(2)}) copy-start(bf16[256,128]{1,0:T(8,128)(2,1)} %v_ref.1) | copy-start | bytes 196612
  0.7 16.9 %copy-start.6 = (bf16[256,128]{1,0:T(8,128)(2,1)S(1)}, bf16[256,128]{1,0:T(8,128)(2,1)}, u32[]{:S(2)}) copy-start(bf16[256,128]{1,0:T(8,128)(2,1)} %k_ref.1) | copy-start | bytes 196612
  0.7 16.9 %copy-start.5 = (bf16[256,128]{1,0:T(8,128)(2,1)S(1)}, bf16[256,128]{1,0:T(8,128)(2,1)}, u32[]{:S(2)}) copy-start(bf16[256,128]{1,0:T(8,128)(2,1)} %q_ref.1) | copy-start | bytes 196612
  2.4 15.1 %all-to-all-start = ((bf16[16,32,256]{2,1,0:T(8,128)(2,1)}), bf16[16,32,256]{2,1,0:T(8,128)(2,1)S(1)}, u32[]{:S(2)}, u32[]{:S(2)}) async-start(bf16[16,32,256]{2,1,0:T(8,128)(2,1)} %shard_map.246), calls=%async_computation | async-start | bytes 524288 | tf_op jit(solution)/shard_map/all_to_all | solution.py:41
  18.6 23.8 %copy-start.9 = (bf16[128,256]{1,0:T(8,128)(2,1)S(1)}, bf16[128,256]{1,0:T(8,128)(2,1)}, u32[]{:S(2)}) copy-start(bf16[128,256]{1,0:T(8,128)(2,1)} %w_ref.2) | copy-start | bytes 196612
  31.2 47.9 %copy-start = (bf16[256,512]{1,0:T(8,128)(2,1)S(1)}, bf16[256,512]{1,0:T(8,128)(2,1)}, u32[]{:S(2)}) copy-start(bf16[256,512]{1,0:T(8,128)(2,1)} %gate_ref.1) | copy-start | bytes 786436
  31.2 47.9 %copy-start.1 = (bf16[256,512]{1,0:T(8,128)(2,1)S(1)}, bf16[256,512]{1,0:T(8,128)(2,1)}, u32[]{:S(2)}) copy-start(bf16[256,512]{1,0:T(8,128)(2,1)} %up_ref.1) | copy-start | bytes 786436
  31.2 47.9 %copy-start.3 = (f32[4096]{0:T(1024)S(1)}, f32[4096]{0:T(1024)}, u32[]{:S(2)}) copy-start(f32[4096]{0:T(1024)} %param.36) | copy-start | bytes 49156
  31.2 47.9 %copy-start.10 = (bf16[4096]{0:T(1024)(128)(2,1)S(1)}, bf16[4096]{0:T(1024)(128)(2,1)}, u32[]{:S(2)}) copy-start(bf16[4096]{0:T(1024)(128)(2,1)} %param.37) | copy-start | bytes 24580
  43.2 5.5 %collective-permute-start = (bf16[8,32,256]{2,1,0:T(8,128)(2,1)S(1)}, bf16[8,32,256]{2,1,0:T(8,128)(2,1)S(1)}, u32[]{:S(2)}, u32[]{:S(2)}) collective-permute-start(bf16[8,32,256]{2,1,0:T(8,128)(2,1)S(1)} %get-tuple-element.62), channel_id=1, source_target_pairs={{0,1},{1,0},{2,3},{3,2},{4,5},{5,4},{6,7},{7,6},{8,9},{9,8},{10,11... | collective-permute-start | bytes 393224 | tf_op jit(solution)/shard_map/ppermute | solution.py:54
  75.0 4.1 %collective-permute-start.1 = (bf16[8,32,256]{2,1,0:T(8,128)(2,1)S(1)}, bf16[8,32,256]{2,1,0:T(8,128)(2,1)S(1)}, u32[]{:S(2)}, u32[]{:S(2)}) collective-permute-start(bf16[8,32,256]{2,1,0:T(8,128)(2,1)S(1)} %all_to_all.53.r_ref), channel_id=1, source_target_pairs={{0,1},{1,0},{2,3},{3,2},{4,5},{5,4},{6,7},{7,6},{8,9},{9,8},{10,11... | collective-permute-start | bytes 393224 | tf_op jit(solution)/shard_map/ppermute | solution.py:54
  103.4 5.1 %collective-permute-start.2 = (bf16[16,48,128]{2,1,0:T(8,128)(2,1)S(1)}, bf16[16,48,128]{2,1,0:T(8,128)(2,1)S(1)}, u32[]{:S(2)}, u32[]{:S(2)}) collective-permute-start(bf16[16,48,128]{2,1,0:T(8,128)(2,1)S(1)} %slice.4), channel_id=1, source_target_pairs={{0,2},{1,3},{2,0},{3,1},{4,6},{5,7},{6,4},{7,5},{8,10},{9,11},{10,... | collective-permute-start | bytes 589832 | tf_op jit(solution)/shard_map/ppermute | solution.py:654
  108.5 7.6 %collective-permute-start.3 = (bf16[16,96,128]{2,1,0:T(8,128)(2,1)S(1)}, bf16[16,96,128]{2,1,0:T(8,128)(2,1)S(1)}, u32[]{:S(2)}, u32[]{:S(2)}) collective-permute-start(bf16[16,96,128]{2,1,0:T(8,128)(2,1)S(1)} %pad_maximum_fusion.x_ref), channel_id=1, source_target_pairs={{0,1},{1,0},{2,3},{3,2},{4,5},{5,4},{6,7},{7,6},{8,9},{9,8},{10,11... | collective-permute-start | bytes 1179656 | tf_op jit(solution)/shard_map/ppermute | solution.py:54
  112.5 14.8 %all-to-all-start.6 = ((bf16[16,32,512]{2,1,0:T(8,128)(2,1)}), bf16[16,32,512]{2,1,0:T(8,128)(2,1)S(1)}, u32[]{:S(2)}, u32[]{:S(2)}) async-start(bf16[16,32,512]{2,1,0:T(8,128)(2,1)} %shard_map.254), calls=%async_computation.6 | async-start | bytes 1048576 | tf_op jit(solution)/shard_map/all_to_all | solution.py:41
  116.1 11.2 %copy-start.2 = (bf16[512,256]{1,0:T(8,128)(2,1)S(1)}, bf16[512,256]{1,0:T(8,128)(2,1)}, u32[]{:S(2)}) copy-start(bf16[512,256]{1,0:T(8,128)(2,1)} %w_ref.3) | copy-start | bytes 786436
  121.8 5.5 %collective-permute-start.4 = (bf16[16,96,128]{2,1,0:T(8,128)(2,1)}, bf16[16,96,128]{2,1,0:T(8,128)(2,1)S(1)}, u32[]{:S(2)}, u32[]{:S(2)}) collective-permute-start(bf16[16,96,128]{2,1,0:T(8,128)(2,1)} %get-tuple-element.70), channel_id=1, source_target_pairs={{0,1},{1,0},{2,3},{3,2},{4,5},{5,4},{6,7},{7,6},{8,9},{9,8},{10,11... | collective-permute-start | bytes 1179656 | tf_op jit(solution)/shard_map/ppermute | solution.py:54
  143.6 3.3 %collective-permute-start.5 = (bf16[8,64,128]{2,1,0:T(8,128)(2,1)S(1)}, bf16[8,64,128]{2,1,0:T(8,128)(2,1)S(1)}, u32[]{:S(2)}, u32[]{:S(2)}) collective-permute-start(bf16[8,64,128]{2,1,0:T(8,128)(2,1)S(1)} %get-tuple-element.83), channel_id=1, source_target_pairs={{0,1},{1,0},{2,3},{3,2},{4,5},{5,4},{6,7},{7,6},{8,9},{9,8},{10,11... | collective-permute-start | bytes 393224 | tf_op jit(solution)/shard_map/ppermute | solution.py:54
  168.1 3.8 %collective-permute-start.6 = (bf16[8,64,128]{2,1,0:T(8,128)(2,1)S(1)}, bf16[8,64,128]{2,1,0:T(8,128)(2,1)S(1)}, u32[]{:S(2)}, u32[]{:S(2)}) collective-permute-start(bf16[8,64,128]{2,1,0:T(8,128)(2,1)S(1)} %all_to_all.57.x_ref), channel_id=1, source_target_pairs={{0,1},{1,0},{2,3},{3,2},{4,5},{5,4},{6,7},{7,6},{8,9},{9,8},{10,11... | collective-permute-start | bytes 393224 | tf_op jit(solution)/shard_map/ppermute | solution.py:54
